TPU v7x, 512 devices: a whole 4x4x16 slice. The times are simulated.
512 devices in a mesh: sp: 32 (over z, core), tp: 16 (over y, x).
Axes of the slice: x: 4, y: 4, z: 16, core: 2. Of those that a mesh axis runs over, the one named last changes fastest.
Arguments:
- query_major: bfloat16 [4096, 3072], P('sp', 'tp'), may hold values from -256 to 256
- query_minor: bfloat16 [4096, 2048], P('sp', 'tp'), may hold values from -256 to 256
- latent_rows: bfloat16 [4096, 512], P('sp'), may hold values from -6 to 6
- rope_keys: bfloat16 [4096, 64], P('sp'), may hold values from -4 to 4
- key_up_major: bfloat16 [512, 2048], P(None, 'tp'), may hold values from -0.25 to 0.25
- value_up_major: bfloat16 [512, 2048], P(None, 'tp'), may hold values from -0.25 to 0.25
- key_up_minor: bfloat16 [512, 1024], P(None, 'tp'), may hold values from -0.25 to 0.25
- value_up_minor: bfloat16 [512, 1024], P(None, 'tp'), may hold values from -0.25 to 0.25
- out_major: bfloat16 [2048, 2048], P('tp'), may hold values from -0.625 to 0.625
- out_minor: bfloat16 [1024, 2048], P('tp'), may hold values from -0.625 to 0.625
- residual: bfloat16 [4096, 2048], P('sp', 'tp'), may hold values from -4 to 4
- norm_gain: float32 [2048], replicated, may hold values from 0.1 to 1.9
- expert_ids: int32 [4096, 2], P('sp'), may hold values from 0 to 31, all different within a row; in each aligned block of 128 rows (0 to 127, 128 to 255, ...) at most 16 rows name the same one
- expert_weights: float32 [4096, 2], P('sp'), may hold values from 0.2 to 1
- gate_proj: bfloat16 [32, 2048, 4096], P('sp', None, 'tp'), may hold values from -0.125 to 0.125
- up_proj: bfloat16 [32, 2048, 4096], P('sp', None, 'tp'), may hold values from -0.125 to 0.125
- down_proj: bfloat16 [32, 4096, 2048], P('sp', 'tp'), may hold values from -0.125 to 0.125
Outputs:
- mixed: bfloat16 [4096, 2048], P('sp', 'tp')
Inputs may be any that keep to these rules, and one draw needn't show every extreme that they name: `expert_ids`: each row names 2 different experts. In each aligned block of 128 rows (the rows of one index of sp) no expert is named by more than 16 rows, and in some blocks one expert is named by exactly 16 rows.
All inputs are finite; a program needn't handle non-finite values.
Results may differ from a plain program's by a relative error of at most 0.02.
Values may be sent and summed in bfloat16 or wider, within the bound.
No kernel may reach another device: no remote copies, remote signals or barrier semaphores. Data moves between devices by JAX's collectives and lax.ppermute only.
A program may use at most 64 MiB of HBM per device.

v0:
```python
import jax
import jax.numpy as jnp
from jax import lax
from jax.sharding import PartitionSpec as P

D = 2048
NOPE_MAJOR = 128
NOPE_MINOR = 64
TOP = 2


theta_base = 10000.0
norm_eps = 1e-06


def in_blocks(array, dim, size):
    before, after = (array.shape[:dim], array.shape[dim + 1 :])
    return jnp.moveaxis(array.reshape(*before, size, -1, *after), dim, 0)


def sent_and_summed(array, axis, dim):
    size = lax.axis_size(axis)
    parts = lax.all_to_all(in_blocks(array, dim, size), axis, 0, 0, tiled=True)
    return jnp.sum(parts.astype(jnp.float32), axis=0)


def side_by_side(arrays, axis, dim, along):
    ends, at = ([], 0)
    for a in arrays[:-1]:
        at += a.shape[along]
        ends.append(at)
    both = jnp.concatenate(arrays, axis=along)
    return tuple(jnp.split(lax.all_gather(both, axis, axis=dim, tiled=True), ends, axis=along))


def copy_for_each(array, axis):
    copies = jnp.broadcast_to(array, (lax.axis_size(axis), *array.shape))
    return lax.all_to_all(copies, axis, split_axis=0, concat_axis=0, tiled=True)


def of_everyone(array, axis):
    everything = copy_for_each(array, axis)
    return jnp.sum(everything, axis=0)


def in_order(parts, dim):
    parts = jnp.moveaxis(parts, 0, dim)
    dims = parts.shape
    return parts.reshape(*dims[:dim], dims[dim] * dims[dim + 1], *dims[dim + 2 :])


def collect(array, axis, dim):
    parts = copy_for_each(array, axis)
    return in_order(parts, dim)


def rotary(values, positions):
    half_width = values.shape[-1] // 2
    inverse_freq = 1.0 / theta_base ** (
        jnp.arange(half_width, dtype=jnp.float32) * (2.0 / values.shape[-1])
    )
    angles = positions.astype(jnp.float32)[:, None] * inverse_freq[None, :]
    view_shape = (angles.shape[0],) + (1,) * (values.ndim - 2) + (half_width,)
    cosine = jnp.cos(angles).reshape(view_shape)
    sine_table = jnp.sin(angles).reshape(view_shape)
    lower_half = values[..., :half_width].astype(jnp.float32)
    upper_half = values[..., half_width:].astype(jnp.float32)
    return jnp.concatenate(
        [
            lower_half * cosine - upper_half * sine_table,
            upper_half * cosine + lower_half * sine_table,
        ],
        axis=-1,
    )


def slot_ids(route_block, experts, capacity):
    pairs = route_block.reshape(-1)
    matches = (pairs[:, None] == jnp.arange(experts, dtype=jnp.int32)[None, :]).astype(jnp.int32)
    ranks = jnp.cumsum(matches, axis=0) - 1
    return pairs * capacity + jnp.sum(ranks * matches, axis=1)


def group_step(states, latent_part, rope_part, visible, q_nope, q_rope, key_up, value_up, scale):
    running, totals, summed = states
    key_count = latent_part.shape[0]
    head_count = q_nope.shape[1]
    key_rows = (
        jnp.dot(latent_part, key_up, preferred_element_type=jnp.float32)
        .astype(jnp.bfloat16)
        .reshape(key_count, head_count, -1)
    )
    value_rows = (
        jnp.dot(latent_part, value_up, preferred_element_type=jnp.float32)
        .astype(jnp.bfloat16)
        .reshape(key_count, head_count, -1)
    )
    scores = jnp.einsum("qhd,khd->hqk", q_nope, key_rows, preferred_element_type=jnp.float32)
    scores = scores + jnp.einsum(
        "qhd,kd->hqk", q_rope, rope_part, preferred_element_type=jnp.float32
    )
    scores = jnp.where(visible[None, :, :], scores * scale, -jnp.inf)
    newest = jnp.max(scores, axis=2)
    weights = jnp.exp(scores - newest[:, :, None])
    factor = jnp.exp(running - newest)
    totals = totals * factor + jnp.sum(weights, axis=2)
    summed = summed * factor[:, :, None] + jnp.einsum(
        "hqk,khv->hqv", weights.astype(jnp.bfloat16), value_rows, preferred_element_type=jnp.float32
    )
    return (newest, totals, summed)


def finish_heads(states, tok_rows):
    running, totals, summed = states
    return (
        (summed / totals[:, :, None]).astype(jnp.bfloat16).transpose(1, 0, 2).reshape(tok_rows, -1)
    )


def finish_expert(gate_pre, up_pre, down_weight, slot_count):
    hidden = (jax.nn.silu(gate_pre) * up_pre).astype(jnp.bfloat16)
    down_part = jnp.dot(hidden, down_weight, preferred_element_type=jnp.float32)
    expert_out = sent_and_summed(down_part.astype(jnp.bfloat16), "tp", 1).astype(jnp.bfloat16)
    return lax.all_to_all(
        expert_out.reshape(-1, slot_count, expert_out.shape[1]),
        "sp",
        split_axis=0,
        concat_axis=0,
        tiled=True,
    )


def per_device(
    query_major,
    query_minor,
    latent_rows,
    rope_keys,
    key_up_major,
    value_up_major,
    key_up_minor,
    value_up_minor,
    out_major,
    out_minor,
    residual,
    norm_gain,
    expert_ids,
    expert_weights,
    gate_proj,
    up_proj,
    down_proj,
):
    tok_rows = query_major.shape[0]
    row_start = lax.axis_index("sp") * tok_rows
    row_last = row_start + tok_rows - 1
    positions = row_start + jnp.arange(tok_rows, dtype=jnp.int32)
    rope_width = rope_keys.shape[1]
    rope_rot = rotary(rope_keys, positions).astype(jnp.bfloat16)
    heads_major = key_up_major.shape[1] // NOPE_MAJOR
    heads_minor = key_up_minor.shape[1] // NOPE_MINOR
    value_major = value_up_major.shape[1] // heads_major
    value_minor = value_up_minor.shape[1] // heads_minor
    shaped_major = query_major.reshape(tok_rows, heads_major, NOPE_MAJOR + rope_width)
    shaped_minor = query_minor.reshape(tok_rows, heads_minor, NOPE_MINOR + rope_width)
    nope_major = shaped_major[:, :, :NOPE_MAJOR]
    nope_minor = shaped_minor[:, :, :NOPE_MINOR]
    turned_major = rotary(shaped_major[:, :, NOPE_MAJOR:], positions).astype(jnp.bfloat16)
    turned_minor = rotary(shaped_minor[:, :, NOPE_MINOR:], positions).astype(jnp.bfloat16)
    scale_major = (NOPE_MAJOR + rope_width) ** (-0.5)
    scale_minor = (NOPE_MINOR + rope_width) ** (-0.5)

    def fresh(head_count, value_width):
        return (
            jnp.full((head_count, tok_rows), -jnp.inf, jnp.float32),
            jnp.zeros((head_count, tok_rows), jnp.float32),
            jnp.zeros((head_count, tok_rows, value_width), jnp.float32),
        )

    latent_part, rope_part = side_by_side((latent_rows, rope_rot), "sp", 0, 1)
    key_pos = jnp.arange(latent_part.shape[0], dtype=jnp.int32)
    visible = key_pos[None, :] <= positions[:, None]

    def compute(states):
        major_state = group_step(
            states[0],
            latent_part,
            rope_part,
            visible,
            nope_major,
            turned_major,
            key_up_major,
            value_up_major,
            scale_major,
        )
        minor_state = group_step(
            states[1],
            latent_part,
            rope_part,
            visible,
            nope_minor,
            turned_minor,
            key_up_minor,
            value_up_minor,
            scale_minor,
        )
        return (major_state, minor_state)

    def unchanged(states):
        return states

    state_major, state_minor = lax.cond(
        jnp.int32(0) <= row_last,
        compute,
        unchanged,
        (fresh(heads_major, value_major), fresh(heads_minor, value_minor)),
    )
    attn_major = finish_heads(state_major, tok_rows)
    attn_minor = finish_heads(state_minor, tok_rows)
    partial_value = jnp.dot(attn_major, out_major, preferred_element_type=jnp.float32)
    partial_value = partial_value + jnp.dot(
        attn_minor, out_minor, preferred_element_type=jnp.float32
    )
    head_total = sent_and_summed(partial_value.astype(jnp.bfloat16), "tp", 1)
    stream_mid = (residual.astype(jnp.float32) + head_total).astype(jnp.bfloat16)
    stream_f = stream_mid.astype(jnp.float32)
    feature_count = residual.shape[1]
    feature_start = lax.axis_index("tp") * feature_count
    experts = lax.axis_size("sp")
    capacity = 2 * tok_rows * TOP // experts
    slot_list = slot_ids(expert_ids, experts, capacity)
    matches = (
        slot_list[:, None] == jnp.arange(experts * capacity, dtype=jnp.int32)[None, :]
    ).astype(jnp.int32)
    select = jnp.sum(matches.reshape(tok_rows, TOP, experts * capacity), axis=1).astype(
        jnp.bfloat16
    )
    squares = of_everyone(jnp.sum(stream_f * stream_f, axis=1), "tp")
    gain_slice = lax.dynamic_slice_in_dim(norm_gain, feature_start, feature_count, 0)
    normed = (stream_f * lax.rsqrt(squares[:, None] / D + norm_eps) * gain_slice[None, :]).astype(
        jnp.bfloat16
    )
    placed = lax.dot_general(
        select, normed, (((0,), (0,)), ((), ())), preferred_element_type=jnp.float32
    )
    arrived = lax.all_to_all(
        placed.astype(jnp.bfloat16).reshape(experts, capacity, -1),
        "sp",
        split_axis=0,
        concat_axis=0,
        tiled=True,
    )
    slot_rows = arrived.reshape(-1, arrived.shape[2])
    portion = collect(slot_rows, "tp", 1)
    gate_part = gate_proj[0]
    up_part = up_proj[0]
    gate_pre = jnp.dot(portion, gate_part, preferred_element_type=jnp.float32)
    up_pre = jnp.dot(portion, up_part, preferred_element_type=jnp.float32)
    returned = finish_expert(gate_pre, up_pre, down_proj[0], arrived.shape[1])
    flat_out = returned.reshape(experts * capacity, -1)
    picked = jnp.take(flat_out, slot_list, axis=0).astype(jnp.float32)
    weighted = picked * expert_weights.reshape(-1)[:, None]
    moe_out = jnp.sum(weighted.reshape(tok_rows, TOP, -1), axis=1)
    return (stream_f + moe_out).astype(jnp.bfloat16)


def solution(mesh):
    in_specs = (
        P("sp", "tp"),
        P("sp", "tp"),
        P("sp", None),
        P("sp", None),
        P(None, "tp"),
        P(None, "tp"),
        P(None, "tp"),
        P(None, "tp"),
        P("tp", None),
        P("tp", None),
        P("sp", "tp"),
        P(),
        P("sp", None),
        P("sp", None),
        P("sp", None, "tp"),
        P("sp", None, "tp"),
        P("sp", "tp", None),
    )
    out_specs = P("sp", "tp")
    return jax.shard_map(
        per_device, mesh=mesh, in_specs=in_specs, out_specs=out_specs, check_vma=False
    )
```

profile of v0, /device:TPU:1, one launch (start us, length us, event | category | flops | bytes accessed | tf_op | source)
XLA Modules:
  0.0 278.1 jit_solution(13900231103439922564)
XLA Ops:
  6.6 0.9 fusion.88
  7.8 1.7 pad_maximum_fusion
  9.5 0.9 fusion.109
  10.6 0.8 copy.104
  11.4 0.1 eq.40
  11.5 0.9 fusion.96
  12.4 77.9 %all-gather.2.cloned.1.call-done = bf16[4096,576]{1,0:T(8,128)(2,1)} async-done(((bf16[128,576]{1,0:T(8,128)(2,1)}), bf16[4096,576]{1,0:T(8,128)(2,1)}) %all-gather.2.cloned.1.call-update) | async-done | bytes 4718608 | tf_op jit(solution)/shard_map/all_gather | solution.py:33
  90.3 0.1 le.34
  90.5 27.5 %conditional.1 = (f32[1,128]{1,0:T(1,128)S(1)}, f32[1,128,128]{2,1,0:T(8,128)S(1)}, f32[1,128]{1,0:T(1,128)S(1)}, f32[1,128,64]{1,2,0:T(8,128)S(1)}) conditional(s32[]{:T(128)} %convert_element_type.122, () %tuple.13, (s32[]{:T(128)}, s32[128,1]{0,1:T(1,128)S(1)}, s32[128,4096]{0,1:T(8,128)S(1)}, bf16[4096,576]{1,0:T(8,128)(2,1)}, ...), branch_computations={%region_0.0_spmd, %region_1.6_spmd} | conditional | flops 2157994496 | bytes 44526144 | solution.py:210
  90.5 1.6 convolution_bitcast_fusion.2
  92.1 1.1 broadcast_compare_fusion
  93.3 5.4 %fusion.103 = (f32[128]{0:T(128)S(1)}, f32[1,128,4096]{1,2,0:T(8,128)}) fusion(f32[1,128,4096]{1,2,0:T(8,128)S(1)} %convolution_bitcast_fusion.2, bf16[128,1,192]{2,0,1:T(8,128)(2,1)S(1)} %copy.99, bf16[512,128]{1,0:T(8,128)(2,1)} %get-tuple-element.63, bf16[4096,576]{1,0:T(8,128)(2,1)} %get-tuple-element.42, pred[128,4096]{0,1:T(32,128)(4,1)} %broadcast_compare_fusion), kind=kOutput, calls=%fused_computation.137 | convolution fusion | flops 673709952 | bytes 9077248 | tf_op jit(solution)/shard_map/cond/branch_1_fun/qhd,khd->hqk/dot_general | solution.py:98
  98.7 2.2 fusion.11
  100.8 3.0 %convolution_bitcast_fusion = f32[1,128,4096]{1,2,0:T(8,128)} fusion(bf16[4096,576]{1,0:T(8,128)(2,1)} %get-tuple-element.42, bf16[128,1,64]{0,2,1:T(8,128)(2,1)S(1)} %get-tuple-element.49), kind=kOutput, calls=%fused_computation.1 | convolution fusion | flops 67108864 | bytes 3162112 | tf_op jit(solution)/shard_map/cond/branch_1_fun/qhd,kd->hqk/dot_general | solution.py:99
  104.0 4.8 %fusion.106 = (f32[128]{0:T(128)S(1)}, f32[1,128,4096]{1,2,0:T(8,128)S(1)}) fusion(f32[1,128,4096]{1,2,0:T(8,128)} %convolution_bitcast_fusion, bf16[128,1,128]{0,2,1:T(8,128)(2,1)S(1)} %copy.101, bf16[512,64]{0,1:T(8,128)(2,1)S(1)} %get-tuple-element.135, bf16[4096,576]{1,0:T(8,128)(2,1)} %get-tuple-element.42, pred[128,4096]{0,1:T(32,128)(4,1)} %broadcast_compare_fusion), kind=kOutput, calls=%fused_computation.138 | convolution fusion | flops 337903488 | bytes 8995328 | tf_op jit(solution)/shard_map/cond/branch_1_fun/qhd,khd->hqk/dot_general | solution.py:98
  108.7 0.6 fusion.13
  109.3 0.3 copy-done.8
  109.6 3.8 %fusion.31 = f32[1,128,64]{1,2,0:T(8,128)S(1)} fusion(bf16[512,64]{0,1:T(8,128)(2,1)S(1)} %copy-done.8, bf16[4096,576]{1,0:T(8,128)(2,1)} %get-tuple-element.42, f32[1,128,4096]{1,2,0:T(8,128)S(1)} %get-tuple-element.150, f32[128]{0:T(128)S(1)} %get-tuple-element.149, f32[128]{0:T(128)S(1)} %get-tuple-element.143), kind=kOutput, calls=%fused_computation.30 | convolution fusion | flops 336863232 | bytes 6390784 | tf_op jit(solution)/shard_map/cond/branch_1_fun/hqk,khv->hqv/dot_general | solution.py:107
  113.4 4.6 %fusion.25 = f32[1,128,128]{2,1,0:T(8,128)S(1)} fusion(bf16[512,128]{1,0:T(8,128)(2,1)} %get-tuple-element.64, bf16[4096,576]{1,0:T(8,128)(2,1)} %get-tuple-element.42, f32[1,128,4096]{1,2,0:T(8,128)} %get-tuple-element.148, f32[128]{0:T(128)S(1)} %get-tuple-element.147, f32[128]{0:T(128)S(1)} %get-tuple-element.152), kind=kOutput, calls=%fused_computation.28 | convolution fusion | flops 672677888 | bytes 6489088 | tf_op jit(solution)/shard_map/cond/branch_1_fun/hqk,khv->hqv/dot_general | solution.py:107
  118.0 1.4 fusion.70
  119.4 1.3 fusion.48
  120.7 0.9 copy.125
  121.6 6.5 %all-to-all-start = ((bf16[16,128,128]{2,1,0:T(8,128)(2,1)}), bf16[16,128,128]{2,1,0:T(8,128)(2,1)S(1)}, u32[]{:S(2)}, u32[]{:S(2)}) async-start(bf16[16,128,128]{2,1,0:T(8,128)(2,1)} %bitcast.133), calls=%async_computation | async-start | bytes 1048576 | tf_op jit(solution)/shard_map/all_to_all | solution.py:23
  128.2 0.1 reshape.416
  128.3 0.6 reduce-window.6
  128.9 0.2 slice_reduce_fusion
  129.2 0.1 reduce_sum.90
  129.5 9.5 %all-to-all-done = bf16[16,128,128]{2,1,0:T(8,128)(2,1)S(1)} async-done(((bf16[16,128,128]{2,1,0:T(8,128)(2,1)}), bf16[16,128,128]{2,1,0:T(8,128)(2,1)S(1)}, u32[]{:S(2)}, u32[]{:S(2)}) %all-to-all-start) | async-done | bytes 524320 | tf_op jit(solution)/shard_map/all_to_all | solution.py:23
  139.2 0.6 broadcast_in_dim.33
  139.8 3.5 %all-to-all-start.1 = ((f32[16,1,128]{2,1,0:T(1,128)}), f32[16,1,128]{2,1,0:T(1,128)S(1)}, u32[]{:S(2)}, u32[]{:S(2)}) async-start(f32[16,1,128]{2,1,0:T(1,128)} %broadcast_in_dim.33), calls=%async_computation.1 | async-start | bytes 16384 | tf_op jit(solution)/shard_map/all_to_all | solution.py:38
  143.4 0.8 dynamic_slice.3
  144.1 5.4 %all-to-all-done.1 = f32[16,1,128]{2,1,0:T(1,128)S(1)} async-done(((f32[16,1,128]{2,1,0:T(1,128)}), f32[16,1,128]{2,1,0:T(1,128)S(1)}, u32[]{:S(2)}, u32[]{:S(2)}) %all-to-all-start.1) | async-done | bytes 8224 | tf_op jit(solution)/shard_map/all_to_all | solution.py:38
  149.6 0.3 convolution_convert_fusion.5
  149.8 26.1 %all_to_all.31 = bf16[32,16,128]{2,1,0:T(8,128)(2,1)S(1)} all-to-all(bf16[32,16,128]{2,1,0:T(8,128)(2,1)S(1)} %bitcast.138), channel_id=1, replica_groups=mesh['sp'=32,'tp'=16] {'sp'}, dimensions={0} | all-to-all | bytes 262144 | tf_op jit(solution)/shard_map/all_to_all | solution.py:244
  176.0 0.2 broadcast_in_dim.34
  176.2 29.7 %all_to_all.32 = bf16[16,512,128]{1,2,0:T(8,128)(2,1)S(1)} all-to-all(bf16[16,512,128]{1,2,0:T(8,128)(2,1)S(1)} %broadcast_in_dim.34), channel_id=1, replica_groups=mesh['sp'=32,'tp'=16] {'tp'}, dimensions={0} | all-to-all | bytes 4194304 | tf_op jit(solution)/shard_map/all_to_all | solution.py:38
  206.0 1.5 fusion.52
  207.5 5.0 %fusion.47 = bf16[64,16,8,128]{3,2,1,0:T(8,128)(2,1)} fusion(bf16[1,256,2048]{2,1,0:T(8,128)(2,1)S(1)} %copy-done, bf16[512,2048]{0,1:T(8,128)(2,1)S(1)} %bitcast.135, bf16[1,2048,256]{2,1,0:T(8,128)(2,1)} %param.34, f32[512,256]{1,0:T(8,128)} %fusion.52), kind=kOutput, calls=%fused_computation.51 | convolution fusion | flops 1075576832 | bytes 6815744 | tf_op jit(solution)/shard_map/dot_general | solution.py:122
  212.6 2.1 copy.124
  214.7 28.2 %all_to_all.33 = bf16[16,512,128]{2,1,0:T(8,128)(2,1)S(1)} all-to-all(bf16[16,512,128]{2,1,0:T(8,128)(2,1)S(1)} %bitcast.136), channel_id=1, replica_groups=mesh['sp'=32,'tp'=16] {'tp'}, dimensions={0} | all-to-all | bytes 4194304 | tf_op jit(solution)/shard_map/all_to_all | solution.py:23
  242.9 0.9 reduce_sum.94
  243.8 9.8 %all-to-all-start.5 = ((bf16[32,16,128]{2,1,0:T(8,128)(2,1)}), bf16[32,16,128]{2,1,0:T(8,128)(2,1)S(1)}, u32[]{:S(2)}, u32[]{:S(2)}) async-start(bf16[32,16,128]{2,1,0:T(8,128)(2,1)} %bitcast.38), calls=%async_computation.5 | async-start | bytes 262144 | tf_op jit(solution)/shard_map/all_to_all | solution.py:124
  253.7 0.1 mul.204
  253.9 0.1 copy.108
  254.2 15.3 %all-to-all-done.5 = bf16[32,16,128]{2,1,0:T(8,128)(2,1)S(1)} async-done(((bf16[32,16,128]{2,1,0:T(8,128)(2,1)}), bf16[32,16,128]{2,1,0:T(8,128)(2,1)S(1)}, u32[]{:S(2)}, u32[]{:S(2)}) %all-to-all-start.5) | async-done | bytes 131104 | tf_op jit(solution)/shard_map/all_to_all | solution.py:124
  269.5 0.9 gather_fusion
  270.3 0.3 multiply_reduce_fusion
  270.7 0.6 fusion.66
  (48 shorter events, 1.6 us)
Async XLA Ops:
  6.5 201.0 %copy-start = (bf16[1,256,2048]{2,1,0:T(8,128)(2,1)S(1)}, bf16[1,256,2048]{2,1,0:T(8,128)(2,1)}, u32[]{:S(2)}) copy-start(bf16[1,256,2048]{2,1,0:T(8,128)(2,1)} %param.35) | copy-start | bytes 3145732
  6.5 83.9 %copy-start.2 = (bf16[128,128]{1,0:T(8,128)(2,1)S(1)}, bf16[128,128]{1,0:T(8,128)(2,1)}, u32[]{:S(2)}) copy-start(bf16[128,128]{1,0:T(8,128)(2,1)} %param.20) | copy-start | bytes 98308
  6.5 83.9 %copy-start.3 = (bf16[128,192]{0,1:T(8,128)(2,1)S(1)}, bf16[128,192]{0,1:T(8,128)(2,1)}, u32[]{:S(2)}) copy-start(bf16[128,192]{0,1:T(8,128)(2,1)} %param.19) | copy-start | bytes 147460
  6.5 83.9 %copy-start.4 = (bf16[512,64]{0,1:T(8,128)(2,1)S(1)}, bf16[512,64]{0,1:T(8,128)(2,1)}, u32[]{:S(2)}) copy-start(bf16[512,64]{0,1:T(8,128)(2,1)} %param.25) | copy-start | bytes 196612
  6.5 83.7 %all-gather.2.cloned.1.call-start = ((), (), s32[]{:S(2)}) async-start(), calls=%async_computation.6 | async-start | bytes 5406720 | tf_op jit(solution)/shard_map/all_gather | solution.py:33
  108.7 0.8 copy-start.8
  119.4 10.1 %copy-start.6 = (s32[128,2]{0,1:T(2,128)S(1)}, s32[128,2]{0,1:T(2,128)}, u32[]{:S(2)}) copy-start(s32[128,2]{0,1:T(2,128)} %param.31) | copy-start | bytes 3076
  119.4 19.7 %copy-start.5 = (bf16[128,128]{1,0:T(8,128)(2,1)S(1)}, bf16[128,128]{1,0:T(8,128)(2,1)}, u32[]{:S(2)}) copy-start(bf16[128,128]{1,0:T(8,128)(2,1)} %param.29) | copy-start | bytes 98308
  121.6 17.3 %all-to-all-start = ((bf16[16,128,128]{2,1,0:T(8,128)(2,1)}), bf16[16,128,128]{2,1,0:T(8,128)(2,1)S(1)}, u32[]{:S(2)}, u32[]{:S(2)}) async-start(bf16[16,128,128]{2,1,0:T(8,128)(2,1)} %bitcast.133), calls=%async_computation | async-start | bytes 1048576 | tf_op jit(solution)/shard_map/all_to_all | solution.py:23
  139.8 9.8 %all-to-all-start.1 = ((f32[16,1,128]{2,1,0:T(1,128)}), f32[16,1,128]{2,1,0:T(1,128)S(1)}, u32[]{:S(2)}, u32[]{:S(2)}) async-start(f32[16,1,128]{2,1,0:T(1,128)} %broadcast_in_dim.33), calls=%async_computation.1 | async-start | bytes 16384 | tf_op jit(solution)/shard_map/all_to_all | solution.py:38
  176.2 29.7 %copy-start.1 = (bf16[1,2048,256]{2,1,0:T(8,128)(2,1)S(1)}, bf16[1,2048,256]{2,1,0:T(8,128)(2,1)}, u32[]{:S(2)}) copy-start(bf16[1,2048,256]{2,1,0:T(8,128)(2,1)} %param.33) | copy-start | bytes 3145732
  242.9 11.1 %copy-start.7 = (f32[128,2]{0,1:T(2,128)S(1)}, f32[128,2]{0,1:T(2,128)}, u32[]{:S(2)}) copy-start(f32[128,2]{0,1:T(2,128)} %param.32) | copy-start | bytes 3076
  243.8 25.6 %all-to-all-start.5 = ((bf16[32,16,128]{2,1,0:T(8,128)(2,1)}), bf16[32,16,128]{2,1,0:T(8,128)(2,1)S(1)}, u32[]{:S(2)}, u32[]{:S(2)}) async-start(bf16[32,16,128]{2,1,0:T(8,128)(2,1)} %bitcast.38), calls=%async_computation.5 | async-start | bytes 262144 | tf_op jit(solution)/shard_map/all_to_all | solution.py:124
Sparse Core Ops, SparseCore 0:
  9.6 80.6 all-gather.1
where the time goes:
time: 279 us; the launch traced here: 278 us
  waiting for transfers between devices  108 us (39%)
  blocking collectives  84 us (30%)
  matrix products  32.7 us (12%)
  starting transfers between devices  19.8 us (7%)
  between operations  13.7 us (5%)
  other arithmetic  10.3 us (4%)
  local copies, waits for them, and re-layouts  9.54 us (3%)
    all_gather x1, waiting for transfers between devices, side_by_side(): lax.all_gather(both, axis, axis=dim, tiled=True)  77.9 us
    all_to_all x1, blocking collectives, copy_for_each(): return lax.all_to_all(copies, axis, split_axis=0, concat_axis=0, tiled=True)  29.7 us
    all_to_all x1, blocking collectives, sent_and_summed(): parts = lax.all_to_all(in_blocks(array, dim, size), axis, 0, 0, tiled=True)  28.2 us
    all_to_all x1, blocking collectives, per_device(): lax.all_to_all(placed.astype(jnp.bfloat16).reshape(experts, capacity, -1)...  26.1 us
    all_to_all x1, waiting for transfers between devices, finish_expert(): lax.all_to_all(expert_out.reshape(-1, slot_count, expert_out.shape[1]), '...  15.3 us
    dot_general x2, matrix products, group_step(): jnp.einsum('qhd,khd->hqk', q_nope, key_rows, preferred_element_type=jnp.f...  10.1 us
    all_to_all x1, starting transfers between devices, finish_expert(): lax.all_to_all(expert_out.reshape(-1, slot_count, expert_out.shape[1]), '...  9.78 us
    all_to_all x1, waiting for transfers between devices, sent_and_summed(): parts = lax.all_to_all(in_blocks(array, dim, size), axis, 0, 0, tiled=True)  9.48 us
  transfers between devices with their start and end apart: 4, of which 4 were waited for; matrix products, arithmetic and copies ran while one was open for 2% of the time, Pallas kernels for 0%

commit v1 on v0

v1 whole, which is shorter than its diff:
```python
import jax
import jax.numpy as jnp
import numpy as np
from jax import lax
from jax.experimental import pallas as pl
from jax.experimental.pallas import tpu as pltpu
from jax.sharding import PartitionSpec as P

F32 = jnp.float32
BF16 = jnp.bfloat16
D = 2048
ROPE = 64
NOPE_MAJOR = 128
NOPE_MINOR = 64
LATENT = 512
TOK = 128
N_TP = 16
N_Z = 16
EXPERTS = 32
CAP = 16
SLOTS = EXPERTS * CAP
ROWS = TOK // N_TP
KEYS = N_Z * TOK
MASKED = -1e30
NORM_EPS = 1e-6
INV_FREQ = (1.0 / 10000.0 ** (np.arange(32, dtype=np.float64) / 32.0)).astype(np.float32)

SAME_CORE = [[z * 2 + c for z in range(N_Z)] for c in range(2)]
OTHER_CORE = [(i, i ^ 1) for i in range(2 * N_Z)]


def vmem(n):
    return [pl.BlockSpec(memory_space=pltpu.VMEM)] * n


def dot(a, b, dims=((1,), (0,))):
    return lax.dot_general(a, b, (dims, ((), ())), preferred_element_type=F32)


def turned(values, cosine, sine):
    low = values[:, :32].astype(F32)
    high = values[:, 32:].astype(F32)
    return jnp.concatenate(
        [low * cosine - high * sine, high * cosine + low * sine], axis=1
    ).astype(BF16)


def prepare_body(lat, rope, qmaj, qmin, cos_k, sin_k, cos_q, sin_q, rows_out, q_out):
    key = turned(rope[...], cos_k[...], sin_k[...])
    row = jnp.concatenate([lat[...], key, jnp.zeros((ROWS, 64), BF16)], axis=1)
    for z in range(N_Z):
        rows_out[z] = row
    c, s = cos_q[...], sin_q[...]
    maj, low = qmaj[...], qmin[...]
    q_out[...] = jnp.concatenate(
        [
            maj[:, :NOPE_MAJOR],
            turned(maj[:, NOPE_MAJOR:], c, s),
            low[:, :NOPE_MINOR],
            turned(low[:, NOPE_MINOR:], c, s),
        ],
        axis=1,
    )


def spread_body(got, out):
    flat = got[...].reshape(N_Z * ROWS, 640)
    rope = flat[:, 512:576]
    half = jnp.concatenate([rope[:64], rope[64:]], axis=1)
    for t in range(N_TP):
        for k in range(4):
            out[t, 128 * k : 128 * (k + 1), :] = flat[:, 128 * k : 128 * (k + 1)]
        out[t, 512:576, :] = half


CHUNK = 512
N_CHUNK = KEYS // CHUNK


def attend_body(where, keys, q_own, q_other, ku_maj, vu_maj, ku_min, vu_min, own, other, s_maj, s_min, v_all):
    me = where[0]
    core = me % 2
    weights = jnp.concatenate([ku_maj[...], vu_maj[...], ku_min[...], vu_min[...]], axis=1)
    q = jnp.concatenate([q_own[...], q_other[...]], axis=0)
    q_maj, q_min = q[:, :192], q[:, 192:320]
    row = lax.broadcasted_iota(jnp.int32, (2 * TOK, 1), 0)
    q_pos = jnp.where(row < TOK, me * TOK + row, (me + 1 - 2 * core) * TOK + row - TOK)
    scale_maj = (NOPE_MAJOR + ROPE) ** -0.5
    scale_min = (NOPE_MINOR + ROPE) ** -0.5
    top_maj = jnp.full((2 * TOK, 128), MASKED, F32)
    top_min = jnp.full((2 * TOK, 128), MASKED, F32)
    per = CHUNK // 128
    for n in range(N_CHUNK):
        lat_rows, rope_rows = [], []
        for t in range(n * per, (n + 1) * per):
            lat_rows.append(
                jnp.concatenate([keys[t, 128 * k : 128 * (k + 1), :] for k in range(4)], axis=1)
            )
            half = keys[t, 512:576, :]
            rope_rows.append(jnp.concatenate([half[:, :64], half[:, 64:]], axis=0))
        lat = jnp.concatenate(lat_rows, axis=0)
        rope = jnp.concatenate(rope_rows, axis=0)
        up = dot(lat, weights).astype(BF16)
        k_maj = jnp.concatenate([up[:, :128], rope], axis=1)
        k_min = jnp.concatenate([up[:, 256:320], rope], axis=1)
        v_all[CHUNK * n : CHUNK * (n + 1), :] = jnp.concatenate([up[:, 128:256], up[:, 320:384]], axis=1)
        col = lax.broadcasted_iota(jnp.int32, (1, CHUNK), 1) + CHUNK * n
        k_pos = (2 * ((col >> 3) & 15) + core) * TOK + 8 * (col >> 7) + (col & 7)
        seen = k_pos <= q_pos
        a = jnp.where(seen, dot(q_maj, k_maj, ((1,), (1,))) * scale_maj, MASKED)
        b = jnp.where(seen, dot(q_min, k_min, ((1,), (1,))) * scale_min, MASKED)
        s_maj[:, CHUNK * n : CHUNK * (n + 1)] = a
        s_min[:, CHUNK * n : CHUNK * (n + 1)] = b
        for k in range(CHUNK // 128):
            top_maj = jnp.maximum(top_maj, a[:, 128 * k : 128 * (k + 1)])
            top_min = jnp.maximum(top_min, b[:, 128 * k : 128 * (k + 1)])
    m_maj = jnp.max(top_maj, axis=1, keepdims=True)
    m_min = jnp.max(top_min, axis=1, keepdims=True)
    sum_maj = jnp.zeros((2 * TOK, 128), F32)
    sum_min = jnp.zeros((2 * TOK, 128), F32)
    o_maj = jnp.zeros((2 * TOK, 128), F32)
    o_min = jnp.zeros((2 * TOK, 64), F32)
    for n in range(N_CHUNK):
        p = jnp.exp(s_maj[:, CHUNK * n : CHUNK * (n + 1)] - m_maj)
        r = jnp.exp(s_min[:, CHUNK * n : CHUNK * (n + 1)] - m_min)
        for k in range(CHUNK // 128):
            sum_maj = sum_maj + p[:, 128 * k : 128 * (k + 1)]
            sum_min = sum_min + r[:, 128 * k : 128 * (k + 1)]
        v = v_all[CHUNK * n : CHUNK * (n + 1), :]
        o_maj = o_maj + dot(p.astype(BF16), v[:, :128])
        o_min = o_min + dot(r.astype(BF16), v[:, 128:192])
    l_maj = jnp.sum(sum_maj, axis=1, keepdims=True)
    l_min = jnp.sum(sum_min, axis=1, keepdims=True)
    lane = lax.broadcasted_iota(jnp.int32, (2 * TOK, 64), 1)
    stats = jnp.where(
        lane == 0, m_maj, jnp.where(lane == 1, l_maj, jnp.where(lane == 2, m_min, l_min))
    )
    result = jnp.concatenate([o_maj, o_min, stats], axis=1)
    own[...] = result[:TOK]
    other[...] = result[TOK:]


def project_body(a, b, out_maj, out_min, parts):
    a, b = a[...], b[...]

    def joined(m_at, lo, hi):
        m_a, m_b = a[:, m_at : m_at + 1], b[:, m_at : m_at + 1]
        l_a, l_b = a[:, m_at + 1 : m_at + 2], b[:, m_at + 1 : m_at + 2]
        top = jnp.maximum(m_a, m_b)
        f_a, f_b = jnp.exp(m_a - top), jnp.exp(m_b - top)
        total = l_a * f_a + l_b * f_b
        return ((a[:, lo:hi] * f_a + b[:, lo:hi] * f_b) / total).astype(BF16)

    attn_maj = joined(192, 0, 128)
    attn_min = joined(194, 128, 192)
    value = dot(attn_maj, out_maj[...]) + dot(attn_min, out_min[...])
    for t in range(N_TP):
        parts[t] = value[:, 128 * t : 128 * (t + 1)].astype(BF16)


def slot_columns(ids):
    lane = lax.broadcasted_iota(jnp.int32, (TOK, EXPERTS), 1)
    first = (ids[:, 0:1] == lane).astype(F32)
    second = (ids[:, 1:2] == lane).astype(F32)
    below = (
        lax.broadcasted_iota(jnp.int32, (TOK, TOK), 1) < lax.broadcasted_iota(jnp.int32, (TOK, TOK), 0)
    ).astype(BF16)
    earlier = dot(below, (first + second).astype(BF16))
    rank_0 = jnp.sum(first * earlier, axis=1, keepdims=True).astype(jnp.int32)
    rank_1 = jnp.sum(second * earlier, axis=1, keepdims=True).astype(jnp.int32)
    return ids[:, 0:1] * CAP + rank_0, ids[:, 1:2] * CAP + rank_1


def place_body(parts, residual, ids, stream, placed):
    total = residual[...].astype(F32)
    summed = parts[0].astype(F32)
    for t in range(1, N_TP):
        summed = summed + parts[t].astype(F32)
    rows = (total + summed).astype(BF16)
    stream[...] = rows
    slot_0, slot_1 = slot_columns(ids[...])
    lane = lax.broadcasted_iota(jnp.int32, (TOK, SLOTS), 1)
    select = ((lane == slot_0) | (lane == slot_1)).astype(BF16)
    placed[...] = dot(select, rows, ((0,), (0,))).astype(BF16)


def expert_body(got, gain, gate_hbm, up_hbm, down_hbm, parts, x, gate_w, up_w, down_w, sems):
    copies = [
        pltpu.make_async_copy(src, dst, sems.at[i])
        for i, (src, dst) in enumerate(((gate_hbm, gate_w), (up_hbm, up_w), (down_hbm, down_w)))
    ]
    for c in copies:
        c.start()
    squares = jnp.zeros((SLOTS, 128), F32)
    for t in range(N_TP):
        v = got[t].astype(F32)
        squares = squares + v * v
    factor = lax.rsqrt(jnp.sum(squares, axis=1, keepdims=True) / D + NORM_EPS)
    for t in range(N_TP):
        x[:, 128 * t : 128 * (t + 1)] = (
            got[t].astype(F32) * factor * gain[:, 128 * t : 128 * (t + 1)]
        ).astype(BF16)
    copies[0].wait()
    gate = dot(x[...], gate_w[...])
    copies[1].wait()
    up = dot(x[...], up_w[...])
    hidden = (gate / (1.0 + jnp.exp(-gate)) * up).astype(BF16)
    copies[2].wait()
    for t in range(N_TP):
        parts[t] = dot(hidden, down_w[:, 128 * t : 128 * (t + 1)]).astype(BF16)


def mix_body(returned, stream, ids, weights, out):
    slot_0, slot_1 = slot_columns(ids[...])
    lane = lax.broadcasted_iota(jnp.int32, (TOK, SLOTS), 1)
    rows = returned[...]
    w = weights[...]
    first = dot((lane == slot_0).astype(BF16), rows) * w[:, 0:1]
    second = dot((lane == slot_1).astype(BF16), rows) * w[:, 1:2]
    out[...] = (stream[...].astype(F32) + (first + second)).astype(BF16)


def shape(dims, kind=BF16):
    return jax.ShapeDtypeStruct(dims, kind)


def to_each(array, axis, groups=None):
    return lax.all_to_all(array, axis, 0, 0, tiled=True, axis_index_groups=groups)


def per_device(
    query_major,
    query_minor,
    latent_rows,
    rope_keys,
    key_up_major,
    value_up_major,
    key_up_minor,
    value_up_minor,
    out_major,
    out_minor,
    residual,
    norm_gain,
    expert_ids,
    expert_weights,
    gate_proj,
    up_proj,
    down_proj,
):
    block = lax.axis_index("sp").astype(jnp.int32)
    part = lax.axis_index("tp").astype(jnp.int32)
    angles = (block * TOK + jnp.arange(TOK, dtype=jnp.int32)).astype(F32)[:, None] * INV_FREQ[None, :]
    cosine, sine = jnp.cos(angles), jnp.sin(angles)
    mine = part * ROWS

    def my_rows(a):
        return lax.dynamic_slice_in_dim(a, mine, ROWS, 0)

    rows, q_own = pl.pallas_call(
        prepare_body,
        out_shape=(shape((N_Z, ROWS, 640)), shape((TOK, 320))),
        in_specs=vmem(8),
        out_specs=tuple(vmem(2)),
        name="prepare",
    )(
        my_rows(latent_rows),
        my_rows(rope_keys),
        query_major,
        query_minor,
        my_rows(cosine),
        my_rows(sine),
        cosine,
        sine,
    )
    q_other = lax.ppermute(q_own, "sp", OTHER_CORE)
    got_rows = to_each(rows, "sp", SAME_CORE)
    spread = pl.pallas_call(
        spread_body,
        out_shape=shape((N_TP, 576, 128)),
        in_specs=vmem(1),
        out_specs=vmem(1)[0],
        name="spread",
    )(got_rows)
    keys = to_each(spread, "tp")
    own, other = pl.pallas_call(
        attend_body,
        out_shape=(shape((TOK, 256), F32), shape((TOK, 256), F32)),
        in_specs=[pl.BlockSpec(memory_space=pltpu.SMEM)] + vmem(7),
        out_specs=tuple(vmem(2)),
        scratch_shapes=[
            pltpu.VMEM((2 * TOK, KEYS), F32),
            pltpu.VMEM((2 * TOK, KEYS), F32),
            pltpu.VMEM((KEYS, 192), BF16),
        ],
        name="attend",
    )(
        block.reshape(1),
        keys,
        q_own,
        q_other,
        key_up_major,
        value_up_major,
        key_up_minor,
        value_up_minor,
    )
    from_other = lax.ppermute(other, "sp", OTHER_CORE)
    head_parts = pl.pallas_call(
        project_body,
        out_shape=shape((N_TP, TOK, 128)),
        in_specs=vmem(4),
        out_specs=vmem(1)[0],
        name="project",
    )(own, from_other, out_major, out_minor)
    head_parts = to_each(head_parts, "tp")
    stream, placed = pl.pallas_call(
        place_body,
        out_shape=(shape((TOK, 128)), shape((SLOTS, 128))),
        in_specs=vmem(3),
        out_specs=tuple(vmem(2)),
        name="place",
    )(head_parts, residual, expert_ids)
    arrived = to_each(placed.reshape(EXPERTS, CAP, 128), "sp").reshape(SLOTS, 128)
    everyone = to_each(jnp.broadcast_to(arrived, (N_TP, SLOTS, 128)), "tp")
    any_spec = pl.BlockSpec(memory_space=pl.ANY)
    down_parts = pl.pallas_call(
        expert_body,
        out_shape=shape((N_TP, SLOTS, 128)),
        in_specs=vmem(2) + [any_spec] * 3,
        out_specs=vmem(1)[0],
        scratch_shapes=[
            pltpu.VMEM((SLOTS, D), BF16),
            pltpu.VMEM((D, 256), BF16),
            pltpu.VMEM((D, 256), BF16),
            pltpu.VMEM((256, D), BF16),
            pltpu.SemaphoreType.DMA((3,)),
        ],
        name="expert",
    )(everyone, norm_gain.reshape(1, D), gate_proj[0], up_proj[0], down_proj[0])
    down_parts = to_each(down_parts, "tp")
    expert_out = jnp.sum(down_parts.astype(F32), axis=0).astype(BF16)
    returned = to_each(expert_out.reshape(EXPERTS, CAP, 128), "sp").reshape(SLOTS, 128)
    return pl.pallas_call(
        mix_body,
        out_shape=shape((TOK, 128)),
        in_specs=vmem(4),
        out_specs=vmem(1)[0],
        name="mix",
    )(returned, stream, expert_ids, expert_weights)


def solution(mesh):
    in_specs = (
        P("sp", "tp"),
        P("sp", "tp"),
        P("sp", None),
        P("sp", None),
        P(None, "tp"),
        P(None, "tp"),
        P(None, "tp"),
        P(None, "tp"),
        P("tp", None),
        P("tp", None),
        P("sp", "tp"),
        P(),
        P("sp", None),
        P("sp", None),
        P("sp", None, "tp"),
        P("sp", None, "tp"),
        P("sp", "tp", None),
    )
    return jax.shard_map(
        per_device, mesh=mesh, in_specs=in_specs, out_specs=P("sp", "tp"), check_vma=False
    )
```

time: 279 us -> 237 us (0.85)
  waiting for transfers between devices: 108 us -> 46.5 us
  blocking collectives: 84 us -> 117 us
  matrix products: 32.7 us -> 0 us
  Pallas kernels: 0 us -> 25.8 us
  between operations: 13.7 us -> 0.13 us
  starting transfers between devices: 19.8 us -> 32.5 us
  other arithmetic: 10.3 us -> 1.92 us
    all_gather x1 -> x0, waiting for transfers between devices: 77.9 us -> none  [side_by_side(): lax.all_gather(both, axis, axis=dim, tiled=True)]
    all_to_all x3 -> x4, blocking collectives: 84 us -> 117 us  [to_each(): lax.all_to_all(array, axis, 0, 0, tiled=True, axis_index_groups=groups)]
    dot_general x11 -> x0, matrix products: 32.7 us -> none  [the longest x2 10.1 us: group_step(): jnp.einsum('qhd,khd->hqk', q_nope, key_rows, preferred_element_type=jnp.f...]
    pallas_call x0 -> x7, Pallas kernels: none -> 25.8 us  [the longest x1 7.86 us: per_device(): pl.pallas_call(expert_body, out_shape=shape((N_TP, SLOTS, 128)), in_specs...]
    ppermute x0 -> x2, starting transfers between devices: none -> 15.4 us  [the longest x1 8.9 us: per_device(): from_other = lax.ppermute(other, 'sp', OTHER_CORE)]
    all_to_all x3, waiting for transfers between devices: 30.2 us -> 45.3 us  [to_each(): lax.all_to_all(array, axis, 0, 0, tiled=True, axis_index_groups=groups)]
    unnamed x20 -> x32, local copies, waits for them, and re-layouts: 1.12 us -> 9.64 us
    reduce_sum x9 -> x1, other arithmetic: 4.41 us -> 0.96 us  [per_device(): expert_out = jnp.sum(down_parts.astype(F32), axis=0).astype(BF16)]
  transfers between devices with their start and end apart: 4 -> 5, of which waited for: 4 -> 4; matrix products, arithmetic and copies ran while one was open for 2% -> 1% of each run, Pallas kernels for 0% -> 0%
where the time goes in v1:
time: 237 us; the launch traced here: 236 us
  blocking collectives  117 us (49%)
  waiting for transfers between devices  46.5 us (20%)
  starting transfers between devices  32.5 us (14%)
  Pallas kernels  25.8 us (11%)
  local copies, waits for them, and re-layouts  12.1 us (5%)
    all_to_all x4, blocking collectives, to_each(): lax.all_to_all(array, axis, 0, 0, tiled=True, axis_index_groups=groups)  117 us
    all_to_all x3, waiting for transfers between devices, to_each(): lax.all_to_all(array, axis, 0, 0, tiled=True, axis_index_groups=groups)  45.3 us
    all_to_all x3, starting transfers between devices, to_each(): lax.all_to_all(array, axis, 0, 0, tiled=True, axis_index_groups=groups)  17.1 us
    unnamed x32, local copies, waits for them, and re-layouts  9.64 us
    ppermute x1, starting transfers between devices, per_device(): from_other = lax.ppermute(other, 'sp', OTHER_CORE)  8.9 us
    pallas_call x1, Pallas kernels, per_device(): pl.pallas_call(expert_body, out_shape=shape((N_TP, SLOTS, 128)), in_specs...  7.86 us
    ppermute x1, starting transfers between devices, per_device(): q_other = lax.ppermute(q_own, 'sp', OTHER_CORE)  6.53 us
    pallas_call x1, Pallas kernels, per_device(): pl.pallas_call(attend_body, out_shape=(shape((TOK, 256), F32), shape((TOK...  6.1 us
  transfers between devices with their start and end apart: 5, of which 4 were waited for; matrix products, arithmetic and copies ran while one was open for 1% of the time, Pallas kernels for 0%

profile of v1, /device:TPU:1, one launch (start us, length us, event | category | flops | bytes accessed | tf_op | source)
XLA Modules:
  0.0 235.7 jit_solution(15102885325500324807)
XLA Ops:
  0.0 0.0 copy-start
  0.0 0.9 copy-done
  0.9 0.6 constant_dynamic-slice_fusion.3.lat
  1.5 0.8 constant_dynamic-slice_fusion.2
  2.3 0.7 copy.26.rope
  3.0 1.5 copy.20.qmaj
  4.5 1.0 multiply_sine_fusion
  5.5 0.0 copy-start.4
  5.5 0.0 copy-start.5
  5.5 0.6 constant_dynamic-slice_fusion
  6.1 0.0 copy-done.4
  6.1 0.0 copy-done.5
  6.1 1.9 prepare.1
  8.0 28.0 %all_to_all.35.got = bf16[16,8,640]{2,1,0:T(8,128)(2,1)} all-to-all(bf16[16,8,640]{2,1,0:T(8,128)(2,1)} %get-tuple-element.11), channel_id=1, replica_groups={{0,32,64,96,128,160,192,224,256,288,320,352,384,416,448,480},{16,48,80,..., dimensions={0} | all-to-all | bytes 327680 | tf_op jit(solution)/shard_map/all_to_all | solution.py:228
  36.0 2.7 %spread.1 = bf16[16,576,128]{2,1,0:T(8,128)(2,1)} custom-call(bf16[16,8,640]{2,1,0:T(8,128)(2,1)} %all_to_all.35.got), custom_call_target="tpu_custom_call" | custom-call | tf_op jit(solution)/shard_map/spread/pallas_call | solution.py:277
  38.7 6.9 %all-to-all-start.1 = ((bf16[16,576,128]{2,1,0:T(8,128)(2,1)}), bf16[16,576,128]{2,1,0:T(8,128)(2,1)S(1)}, u32[]{:S(2)}, u32[]{:S(2)}) async-start(bf16[16,576,128]{2,1,0:T(8,128)(2,1)} %spread.1), calls=%async_computation.1 | async-start | bytes 4718592 | tf_op jit(solution)/shard_map/all_to_all | solution.py:228
  45.6 0.0 copy-done.7
  45.6 6.5 %collective-permute-start = (bf16[128,320]{1,0:T(8,128)(2,1)S(1)}, bf16[128,320]{1,0:T(8,128)(2,1)S(1)}, u32[]{:S(2)}, u32[]{:S(2)}) collective-permute-start(bf16[128,320]{1,0:T(8,128)(2,1)S(1)} %copy-done.7), channel_id=1, source_target_pairs={{0,16},{16,0},{32,48},{48,32},{64,80},{80,64},{96,112},{112,96},{1... | collective-permute-start | bytes 245768 | tf_op jit(solution)/shard_map/ppermute | solution.py:275
  52.2 0.0 copy-done.9
  52.2 0.8 copy.21.ku_min
  52.9 0.0 copy-done.10
  52.9 0.8 copy.22.vu_min
  53.7 0.0 collective-permute-done.q_other
  53.7 19.6 %all-to-all-done.1.keys = bf16[16,576,128]{2,1,0:T(8,128)(2,1)S(1)} async-done(((bf16[16,576,128]{2,1,0:T(8,128)(2,1)}), bf16[16,576,128]{2,1,0:T(8,128)(2,1)S(1)}, u32[]{:S(2)}, u32[]{:S(2)}) %all-to-all-start.1) | async-done | bytes 2359328 | tf_op jit(solution)/shard_map/all_to_all | solution.py:228
  73.3 0.0 copy-done.8
  73.3 1.4 copy-done.1
  74.8 6.1 %attend.1 = (f32[128,256]{1,0:T(8,128)}, f32[128,256]{1,0:T(8,128)}) custom-call(s32[1]{0:T(128)} %bitcast.where, bf16[16,576,128]{2,1,0:T(8,128)(2,1)} %copy-done.1, bf16[128,320]{1,0:T(8,128)(2,1)} %get-tuple-element.12.q_own, bf16[128,320]{1,0:T(8,128)(2,1)} %copy-done.8, bf16[512,128]{1,0:T(8,128)(2,1)} %ku_maj.1, bf16[512,128]{1,0:T(8,128)(2,1)} %vu_maj.1, ...), custom_call_target="tpu_custom_call" | custom-call | tf_op jit(solution)/shard_map/attend/pallas_call | solution.py:285
  80.9 8.9 %collective-permute-start.1 = (f32[128,256]{1,0:T(8,128)}, f32[128,256]{1,0:T(8,128)S(1)}, u32[]{:S(2)}, u32[]{:S(2)}) collective-permute-start(f32[128,256]{1,0:T(8,128)} %get-tuple-element.14), channel_id=1, source_target_pairs={{0,16},{16,0},{32,48},{48,32},{64,80},{80,64},{96,112},{112,96},{1... | collective-permute-start | bytes 393224 | tf_op jit(solution)/shard_map/ppermute | solution.py:306
  89.8 1.2 collective-permute-done.1.b
  91.0 0.7 copy-done.6
  91.6 2.6 %project.1 = bf16[16,128,128]{2,1,0:T(8,128)(2,1)} custom-call(f32[128,256]{1,0:T(8,128)} %get-tuple-element.13.a, f32[128,256]{1,0:T(8,128)} %copy-done.6, bf16[128,2048]{1,0:T(8,128)(2,1)} %out_maj.1, bf16[64,2048]{1,0:T(8,128)(2,1)} %out_min.1), custom_call_target="tpu_custom_call" | custom-call | tf_op jit(solution)/shard_map/project/pallas_call | solution.py:307
  94.2 3.6 %all-to-all-start.2 = ((bf16[16,128,128]{2,1,0:T(8,128)(2,1)}), bf16[16,128,128]{2,1,0:T(8,128)(2,1)S(1)}, u32[]{:S(2)}, u32[]{:S(2)}) async-start(bf16[16,128,128]{2,1,0:T(8,128)(2,1)} %project.1), calls=%async_computation.2 | async-start | bytes 1048576 | tf_op jit(solution)/shard_map/all_to_all | solution.py:228
  97.8 0.0 copy-done.11
  97.8 0.7 copy.23.ids
  98.6 10.2 %all-to-all-done.2.parts = bf16[16,128,128]{2,1,0:T(8,128)(2,1)S(1)} async-done(((bf16[16,128,128]{2,1,0:T(8,128)(2,1)}), bf16[16,128,128]{2,1,0:T(8,128)(2,1)S(1)}, u32[]{:S(2)}, u32[]{:S(2)}) %all-to-all-start.2) | async-done | bytes 524320 | tf_op jit(solution)/shard_map/all_to_all | solution.py:228
  108.8 0.8 copy-done.2
  109.6 2.4 %place.1 = (bf16[128,128]{1,0:T(8,128)(2,1)}, bf16[512,128]{1,0:T(8,128)(2,1)}) custom-call(bf16[16,128,128]{2,1,0:T(8,128)(2,1)} %copy-done.2, bf16[128,128]{1,0:T(8,128)(2,1)} %residual.1, s32[128,2]{1,0:T(8,128)} %copy.23.ids), custom_call_target="tpu_custom_call" | custom-call | tf_op jit(solution)/shard_map/place/pallas_call | solution.py:315
  112.0 27.4 %all_to_all.36 = bf16[32,16,128]{2,1,0:T(8,128)(2,1)S(1)} all-to-all(bf16[32,16,128]{2,1,0:T(8,128)(2,1)} %bitcast.14), channel_id=1, replica_groups=mesh['sp'=32,'tp'=16] {'sp'}, dimensions={0} | all-to-all | bytes 262144 | tf_op jit(solution)/shard_map/all_to_all | solution.py:228
  139.4 0.4 broadcast_in_dim.4
  139.8 30.4 %all_to_all.37.got = bf16[16,512,128]{2,1,0:T(8,128)(2,1)} all-to-all(bf16[16,512,128]{2,1,0:T(8,128)(2,1)S(1)} %broadcast_in_dim.4), channel_id=1, replica_groups=mesh['sp'=32,'tp'=16] {'tp'}, dimensions={0} | all-to-all | bytes 4194304 | tf_op jit(solution)/shard_map/all_to_all | solution.py:228
  170.2 7.9 %expert.1 = bf16[16,512,128]{2,1,0:T(8,128)(2,1)} custom-call(bf16[16,512,128]{2,1,0:T(8,128)(2,1)} %all_to_all.37.got, f32[1,2048]{1,0:T(1,128)} %bitcast.15, bf16[2048,256]{1,0:T(8,128)(2,1)} %bitcast.9, bf16[2048,256]{1,0:T(8,128)(2,1)} %bitcast.10, bf16[256,2048]{1,0:T(8,128)(2,1)} %bitcast.11), custom_call_target="tpu_custom_call" | custom-call | tf_op jit(solution)/shard_map/expert/pallas_call | solution.py:325
  178.1 30.9 %all_to_all.38 = bf16[16,512,128]{2,1,0:T(8,128)(2,1)S(1)} all-to-all(bf16[16,512,128]{2,1,0:T(8,128)(2,1)} %expert.1), channel_id=1, replica_groups=mesh['sp'=32,'tp'=16] {'tp'}, dimensions={0} | all-to-all | bytes 4194304 | tf_op jit(solution)/shard_map/all_to_all | solution.py:228
  209.0 1.0 reduce_sum.12
  210.0 6.6 %all-to-all-start.6 = ((bf16[32,16,128]{2,1,0:T(8,128)(2,1)}), bf16[32,16,128]{2,1,0:T(8,128)(2,1)S(1)}, u32[]{:S(2)}, u32[]{:S(2)}) async-start(bf16[32,16,128]{2,1,0:T(8,128)(2,1)} %bitcast.7), calls=%async_computation.6 | async-start | bytes 262144 | tf_op jit(solution)/shard_map/all_to_all | solution.py:228
  216.6 0.7 copy.25.weights
  217.3 15.5 %all-to-all-done.6 = bf16[32,16,128]{2,1,0:T(8,128)(2,1)S(1)} async-done(((bf16[32,16,128]{2,1,0:T(8,128)(2,1)}), bf16[32,16,128]{2,1,0:T(8,128)(2,1)S(1)}, u32[]{:S(2)}, u32[]{:S(2)}) %all-to-all-start.6) | async-done | bytes 131104 | tf_op jit(solution)/shard_map/all_to_all | solution.py:228
  232.8 0.6 copy-done.3
  233.5 2.2 mix.1
  (12 shorter events, 0.0 us)
Async XLA Ops:
  0.0 0.9 copy-start
  5.5 0.7 copy-start.4
  5.5 0.6 copy-start.5
  38.7 6.9 %copy-start.7 = (bf16[128,320]{1,0:T(8,128)(2,1)S(1)}, bf16[128,320]{1,0:T(8,128)(2,1)}, u32[]{:S(2)}) copy-start(bf16[128,320]{1,0:T(8,128)(2,1)} %get-tuple-element.12.q_own) | copy-start | bytes 245764
  38.7 13.5 %copy-start.9 = (bf16[512,64]{0,1:T(8,128)(2,1)S(1)}, bf16[512,64]{0,1:T(8,128)(2,1)}, u32[]{:S(2)}) copy-start(bf16[512,64]{0,1:T(8,128)(2,1)} %param.24) | copy-start | bytes 196612
  38.7 14.2 %copy-start.10 = (bf16[512,64]{0,1:T(8,128)(2,1)S(1)}, bf16[512,64]{0,1:T(8,128)(2,1)}, u32[]{:S(2)}) copy-start(bf16[512,64]{0,1:T(8,128)(2,1)} %param.25) | copy-start | bytes 196612
  38.7 34.6 %all-to-all-start.1 = ((bf16[16,576,128]{2,1,0:T(8,128)(2,1)}), bf16[16,576,128]{2,1,0:T(8,128)(2,1)S(1)}, u32[]{:S(2)}, u32[]{:S(2)}) async-start(bf16[16,576,128]{2,1,0:T(8,128)(2,1)} %spread.1), calls=%async_computation.1 | async-start | bytes 4718592 | tf_op jit(solution)/shard_map/all_to_all | solution.py:228
  45.6 8.1 %collective-permute-start = (bf16[128,320]{1,0:T(8,128)(2,1)S(1)}, bf16[128,320]{1,0:T(8,128)(2,1)S(1)}, u32[]{:S(2)}, u32[]{:S(2)}) collective-permute-start(bf16[128,320]{1,0:T(8,128)(2,1)S(1)} %copy-done.7), channel_id=1, source_target_pairs={{0,16},{16,0},{32,48},{48,32},{64,80},{80,64},{96,112},{112,96},{1... | collective-permute-start | bytes 245768 | tf_op jit(solution)/shard_map/ppermute | solution.py:275
  53.7 19.6 %copy-start.8 = (bf16[128,320]{1,0:T(8,128)(2,1)}, bf16[128,320]{1,0:T(8,128)(2,1)S(1)}, u32[]{:S(2)}) copy-start(bf16[128,320]{1,0:T(8,128)(2,1)S(1)} %collective-permute-done.q_other) | copy-start | bytes 245764
  73.3 1.4 copy-start.1
  74.8 23.1 %copy-start.11 = (s32[128,2]{0,1:T(2,128)S(1)}, s32[128,2]{0,1:T(2,128)}, u32[]{:S(2)}) copy-start(s32[128,2]{0,1:T(2,128)} %param.30) | copy-start | bytes 3076
  80.9 10.1 %collective-permute-start.1 = (f32[128,256]{1,0:T(8,128)}, f32[128,256]{1,0:T(8,128)S(1)}, u32[]{:S(2)}, u32[]{:S(2)}) collective-permute-start(f32[128,256]{1,0:T(8,128)} %get-tuple-element.14), channel_id=1, source_target_pairs={{0,16},{16,0},{32,48},{48,32},{64,80},{80,64},{96,112},{112,96},{1... | collective-permute-start | bytes 393224 | tf_op jit(solution)/shard_map/ppermute | solution.py:306
  91.0 0.7 copy-start.6
  94.2 14.5 %all-to-all-start.2 = ((bf16[16,128,128]{2,1,0:T(8,128)(2,1)}), bf16[16,128,128]{2,1,0:T(8,128)(2,1)S(1)}, u32[]{:S(2)}, u32[]{:S(2)}) async-start(bf16[16,128,128]{2,1,0:T(8,128)(2,1)} %project.1), calls=%async_computation.2 | async-start | bytes 1048576 | tf_op jit(solution)/shard_map/all_to_all | solution.py:228
  108.8 0.8 copy-start.2
  209.0 7.6 %copy-start.12 = (f32[128,2]{0,1:T(2,128)S(1)}, f32[128,2]{0,1:T(2,128)}, u32[]{:S(2)}) copy-start(f32[128,2]{0,1:T(2,128)} %param.31) | copy-start | bytes 3076
  210.0 22.8 %all-to-all-start.6 = ((bf16[32,16,128]{2,1,0:T(8,128)(2,1)}), bf16[32,16,128]{2,1,0:T(8,128)(2,1)S(1)}, u32[]{:S(2)}, u32[]{:S(2)}) async-start(bf16[32,16,128]{2,1,0:T(8,128)(2,1)} %bitcast.7), calls=%async_computation.6 | async-start | bytes 262144 | tf_op jit(solution)/shard_map/all_to_all | solution.py:228
  232.8 0.7 copy-start.3

commit v2 on v1

--- a/solution.py
+++ b/solution.py
@@ -5,6 +5,7 @@
 from jax.experimental import pallas as pl
 from jax.experimental.pallas import tpu as pltpu
 from jax.sharding import PartitionSpec as P
+
 
 F32 = jnp.float32
 BF16 = jnp.bfloat16
@@ -23,18 +24,46 @@
 KEYS = N_Z * TOK
 MASKED = -1e30
 NORM_EPS = 1e-6
-INV_FREQ = (1.0 / 10000.0 ** (np.arange(32, dtype=np.float64) / 32.0)).astype(np.float32)
+HALF = SLOTS // 2
+
+
+def turns(positions):
+    angles = positions[:, None] * (1.0 / 10000.0 ** (np.arange(32) / 32.0))[None, :]
+    return np.concatenate([np.cos(angles), np.sin(angles), np.zeros((len(positions), 64))], axis=1)
+
+
+TABLE = np.concatenate([turns(np.arange(2 * N_Z) * float(TOK)), turns(np.arange(TOK) * 1.0)]).astype(
+    np.float32
+)
 
 SAME_CORE = [[z * 2 + c for z in range(N_Z)] for c in range(2)]
 OTHER_CORE = [(i, i ^ 1) for i in range(2 * N_Z)]
+PARTNER = [(s * N_TP + t, s * N_TP + (t ^ (4 if s % 2 else 1))) for s in range(2 * N_Z) for t in range(N_TP)]
+
+
+ANY = pl.BlockSpec(memory_space=pl.ANY)
 
 
 def vmem(n):
     return [pl.BlockSpec(memory_space=pltpu.VMEM)] * n
 
 
+def fetch(pairs, sems):
+    copies = [pltpu.make_async_copy(src, dst, sems.at[i]) for i, (src, dst) in enumerate(pairs)]
+    for c in copies:
+        c.start()
+    return copies
+
+
 def dot(a, b, dims=((1,), (0,))):
     return lax.dot_general(a, b, (dims, ((), ())), preferred_element_type=F32)
+
+
+def turn_at(table, block, rows):
+    first = table[pl.ds(block, 1), :]
+    c_0, s_0 = first[:, :32], first[:, 32:64]
+    c_1, s_1 = rows[:, :32], rows[:, 32:64]
+    return c_0 * c_1 - s_0 * s_1, s_0 * c_1 + c_0 * s_1
 
 
 def turned(values, cosine, sine):
@@ -45,14 +74,24 @@
     ).astype(BF16)
 
 
-def prepare_body(lat, rope, qmaj, qmin, cos_k, sin_k, cos_q, sin_q, rows_out, q_out):
-    key = turned(rope[...], cos_k[...], sin_k[...])
+def rows_body(lat_in, rope_in, table_in, out, lat, rope, table, by_row, sems):
+    block, part = lax.axis_index("sp"), lax.axis_index("tp")
+    mine = pl.ds(pl.multiple_of(part * ROWS, ROWS), ROWS)
+    for c in fetch(((lat_in.at[mine], lat), (rope_in, rope), (table_in, table)), sems):
+        c.wait()
+    at = pl.ds(pl.multiple_of(2 * N_Z + part * ROWS, ROWS), ROWS)
+    cosine, sine = turn_at(table, block, table[at, :])
+    by_row[...] = rope[...].astype(F32).T
+    key = turned(by_row[pl.ds(pl.multiple_of(part * ROWS, ROWS), ROWS), :], cosine, sine)
     row = jnp.concatenate([lat[...], key, jnp.zeros((ROWS, 64), BF16)], axis=1)
     for z in range(N_Z):
-        rows_out[z] = row
-    c, s = cos_q[...], sin_q[...]
-    maj, low = qmaj[...], qmin[...]
-    q_out[...] = jnp.concatenate(
+        out[z] = row
+
+
+def queries_body(maj, low, table, after, ku_maj, vu_maj, ku_min, vu_min, out, weights):
+    weights[...] = jnp.concatenate([ku_maj[...], vu_maj[...], ku_min[...], vu_min[...]], axis=1)
+    c, s = turn_at(table, lax.axis_index("sp"), table[2 * N_Z :, :])
+    out[...] = jnp.concatenate(
         [
             maj[:, :NOPE_MAJOR],
             turned(maj[:, NOPE_MAJOR:], c, s),
@@ -63,24 +102,15 @@
     )
 
 
-def spread_body(got, out):
-    flat = got[...].reshape(N_Z * ROWS, 640)
-    rope = flat[:, 512:576]
-    half = jnp.concatenate([rope[:64], rope[64:]], axis=1)
-    for t in range(N_TP):
-        for k in range(4):
-            out[t, 128 * k : 128 * (k + 1), :] = flat[:, 128 * k : 128 * (k + 1)]
-        out[t, 512:576, :] = half
-
-
 CHUNK = 512
 N_CHUNK = KEYS // CHUNK
 
 
-def attend_body(where, keys, q_own, q_other, ku_maj, vu_maj, ku_min, vu_min, own, other, s_maj, s_min, v_all):
-    me = where[0]
+def attend_body(keys, q_own, q_other, up_weights, own, other, s_maj, s_min, v_all):
+    per = CHUNK // 128
+    me = lax.axis_index("sp")
     core = me % 2
-    weights = jnp.concatenate([ku_maj[...], vu_maj[...], ku_min[...], vu_min[...]], axis=1)
+    weights = up_weights[...]
     q = jnp.concatenate([q_own[...], q_other[...]], axis=0)
     q_maj, q_min = q[:, :192], q[:, 192:320]
     row = lax.broadcasted_iota(jnp.int32, (2 * TOK, 1), 0)
@@ -89,7 +119,6 @@
     scale_min = (NOPE_MINOR + ROPE) ** -0.5
     top_maj = jnp.full((2 * TOK, 128), MASKED, F32)
     top_min = jnp.full((2 * TOK, 128), MASKED, F32)
-    per = CHUNK // 128
     for n in range(N_CHUNK):
         lat_rows, rope_rows = [], []
         for t in range(n * per, (n + 1) * per):
@@ -172,26 +201,34 @@
 
 
 def place_body(parts, residual, ids, stream, placed):
-    total = residual[...].astype(F32)
+    slot_0, slot_1 = slot_columns(ids[...])
+    lane = lax.broadcasted_iota(jnp.int32, (TOK, SLOTS), 1)
+    select = ((lane == slot_0) | (lane == slot_1)).astype(BF16)
     summed = parts[0].astype(F32)
     for t in range(1, N_TP):
         summed = summed + parts[t].astype(F32)
-    rows = (total + summed).astype(BF16)
+    rows = (residual[...].astype(F32) + summed).astype(BF16)
     stream[...] = rows
-    slot_0, slot_1 = slot_columns(ids[...])
-    lane = lax.broadcasted_iota(jnp.int32, (TOK, SLOTS), 1)
-    select = ((lane == slot_0) | (lane == slot_1)).astype(BF16)
     placed[...] = dot(select, rows, ((0,), (0,))).astype(BF16)
 
 
-def expert_body(got, gain, gate_hbm, up_hbm, down_hbm, parts, x, gate_w, up_w, down_w, sems):
-    copies = [
-        pltpu.make_async_copy(src, dst, sems.at[i])
-        for i, (src, dst) in enumerate(((gate_hbm, gate_w), (up_hbm, up_w), (down_hbm, down_w)))
-    ]
-    for c in copies:
-        c.start()
-    squares = jnp.zeros((SLOTS, 128), F32)
+def expert_body(
+    got, gain, gate_a, up_a, down_a, gate_b, up_b, down_b,
+    parts,
+    gate_w, up_w, down_w, x, sems,
+):
+    copies = fetch(
+        (
+            (gate_a.at[0], gate_w.at[0]),
+            (gate_b.at[0], gate_w.at[1]),
+            (up_a.at[0], up_w.at[0]),
+            (up_b.at[0], up_w.at[1]),
+            (down_a.at[0], down_w.at[0]),
+            (down_b.at[0], down_w.at[1]),
+        ),
+        sems,
+    )
+    squares = jnp.zeros((HALF, 128), F32)
     for t in range(N_TP):
         v = got[t].astype(F32)
         squares = squares + v * v
@@ -200,14 +237,31 @@
         x[:, 128 * t : 128 * (t + 1)] = (
             got[t].astype(F32) * factor * gain[:, 128 * t : 128 * (t + 1)]
         ).astype(BF16)
-    copies[0].wait()
-    gate = dot(x[...], gate_w[...])
-    copies[1].wait()
-    up = dot(x[...], up_w[...])
-    hidden = (gate / (1.0 + jnp.exp(-gate)) * up).astype(BF16)
-    copies[2].wait()
-    for t in range(N_TP):
-        parts[t] = dot(hidden, down_w[:, 128 * t : 128 * (t + 1)]).astype(BF16)
+    hidden = []
+    for i in range(2):
+        copies[i].wait()
+        copies[2 + i].wait()
+        gate = dot(x[...], gate_w[i])
+        up = dot(x[...], up_w[i])
+        hidden.append((gate / (1.0 + jnp.exp(-gate)) * up).astype(BF16))
+    copies[4].wait()
+    copies[5].wait()
+    for t in range(0, N_TP, 2):
+        cols = slice(128 * t, 128 * (t + 2))
+        value = dot(hidden[0], down_w[0, :, cols]) + dot(hidden[1], down_w[1, :, cols])
+        parts[t] = value[:, :128].astype(BF16)
+        parts[t + 1] = value[:, 128:].astype(BF16)
+
+
+def gather_sum_body(parts, out):
+    core = lax.axis_index("sp") % 2
+    for half in range(2):
+        total = jnp.zeros((HALF, 128), F32)
+        for k in range(N_TP // 2):
+            by_x = 2 * k + half
+            by_y = (k // 4) * 8 + half * 4 + k % 4
+            total = total + parts[jnp.where(core == 0, by_x, by_y)].astype(F32)
+        out[half * HALF : (half + 1) * HALF, :] = total.astype(BF16)
 
 
 def mix_body(returned, stream, ids, weights, out):
@@ -221,7 +275,25 @@
 
 
 def shape(dims, kind=BF16):
-    return jax.ShapeDtypeStruct(dims, kind)
+    return pltpu.VMEM(dims, kind)
+
+
+def room(dims, kind=BF16):
+    return pltpu.VMEM(dims, kind)
+
+
+def kernel(body, outs, rooms, sems, operands, near=()):
+    single = not isinstance(outs, tuple)
+    places = [pltpu.VMEM if i in near else pltpu.HBM for i in range(len(operands))]
+    operands = [pltpu.with_memory_space_constraint(x, m) for x, m in zip(operands, places)]
+    return pl.pallas_call(
+        body,
+        out_shape=outs,
+        in_specs=[pl.BlockSpec(memory_space=m) for m in places],
+        out_specs=vmem(1)[0] if single else tuple(vmem(len(outs))),
+        scratch_shapes=rooms + ([pltpu.SemaphoreType.DMA((sems,))] if sems else []),
+        compiler_params=pltpu.CompilerParams(vmem_limit_bytes=24 * 2**20),
+    )(*operands)
 
 
 def to_each(array, axis, groups=None):
@@ -247,105 +319,98 @@
     up_proj,
     down_proj,
 ):
-    block = lax.axis_index("sp").astype(jnp.int32)
-    part = lax.axis_index("tp").astype(jnp.int32)
-    angles = (block * TOK + jnp.arange(TOK, dtype=jnp.int32)).astype(F32)[:, None] * INV_FREQ[None, :]
-    cosine, sine = jnp.cos(angles), jnp.sin(angles)
-    mine = part * ROWS
-
-    def my_rows(a):
-        return lax.dynamic_slice_in_dim(a, mine, ROWS, 0)
-
-    rows, q_own = pl.pallas_call(
-        prepare_body,
-        out_shape=(shape((N_Z, ROWS, 640)), shape((TOK, 320))),
-        in_specs=vmem(8),
-        out_specs=tuple(vmem(2)),
-        name="prepare",
-    )(
-        my_rows(latent_rows),
-        my_rows(rope_keys),
-        query_major,
-        query_minor,
-        my_rows(cosine),
-        my_rows(sine),
-        cosine,
-        sine,
+    table = jnp.asarray(TABLE)
+    rows = kernel(
+        rows_body,
+        shape((N_Z, ROWS, 640)),
+        [room((ROWS, LATENT)), room((ROPE, TOK)), room((160, 128), F32), room((TOK, ROPE), F32)],
+        3,
+        (latent_rows, rope_keys.T, table),
+    )
+    flat = to_each(rows, "sp", SAME_CORE).reshape(N_Z * ROWS, 640)
+    rope = flat[:, 512:576]
+    packed = jnp.concatenate(
+        [flat[:, 128 * k : 128 * (k + 1)] for k in range(4)]
+        + [jnp.concatenate([rope[:64], rope[64:]], axis=1)],
+        axis=0,
+    )
+    spread = jnp.broadcast_to(packed, (N_TP, 576, 128))
+    keys = to_each(spread, "tp")
+    q_own, up_weights = kernel(
+        queries_body,
+        (shape((TOK, 320)), shape((LATENT, 384))),
+        [],
+        0,
+        (
+            query_major,
+            query_minor,
+            table,
+            packed,
+            key_up_major,
+            value_up_major,
+            key_up_minor,
+            value_up_minor,
+        ),
+        range(8),
     )
     q_other = lax.ppermute(q_own, "sp", OTHER_CORE)
-    got_rows = to_each(rows, "sp", SAME_CORE)
-    spread = pl.pallas_call(
-        spread_body,
-        out_shape=shape((N_TP, 576, 128)),
-        in_specs=vmem(1),
-        out_specs=vmem(1)[0],
-        name="spread",
-    )(got_rows)
-    keys = to_each(spread, "tp")
-    own, other = pl.pallas_call(
+    gate_b = lax.ppermute(gate_proj, ("sp", "tp"), PARTNER)
+    up_b = lax.ppermute(up_proj, ("sp", "tp"), PARTNER)
+    down_b = lax.ppermute(down_proj, ("sp", "tp"), PARTNER)
+    own, other = kernel(
         attend_body,
-        out_shape=(shape((TOK, 256), F32), shape((TOK, 256), F32)),
-        in_specs=[pl.BlockSpec(memory_space=pltpu.SMEM)] + vmem(7),
-        out_specs=tuple(vmem(2)),
-        scratch_shapes=[
-            pltpu.VMEM((2 * TOK, KEYS), F32),
-            pltpu.VMEM((2 * TOK, KEYS), F32),
-            pltpu.VMEM((KEYS, 192), BF16),
+        (shape((TOK, 256), F32), shape((TOK, 256), F32)),
+        [
+            room((2 * TOK, KEYS), F32),
+            room((2 * TOK, KEYS), F32),
+            room((KEYS, 192)),
         ],
-        name="attend",
-    )(
-        block.reshape(1),
-        keys,
-        q_own,
-        q_other,
-        key_up_major,
-        value_up_major,
-        key_up_minor,
-        value_up_minor,
+        0,
+        (keys, q_own, q_other, up_weights),
+        range(4),
     )
     from_other = lax.ppermute(other, "sp", OTHER_CORE)
-    head_parts = pl.pallas_call(
+    head_parts = kernel(
         project_body,
-        out_shape=shape((N_TP, TOK, 128)),
-        in_specs=vmem(4),
-        out_specs=vmem(1)[0],
-        name="project",
-    )(own, from_other, out_major, out_minor)
+        shape((N_TP, TOK, 128)),
+        [],
+        0,
+        (own, from_other, out_major, out_minor),
+        range(4),
+    )
     head_parts = to_each(head_parts, "tp")
-    stream, placed = pl.pallas_call(
+    stream, placed = kernel(
         place_body,
-        out_shape=(shape((TOK, 128)), shape((SLOTS, 128))),
-        in_specs=vmem(3),
-        out_specs=tuple(vmem(2)),
-        name="place",
-    )(head_parts, residual, expert_ids)
-    arrived = to_each(placed.reshape(EXPERTS, CAP, 128), "sp").reshape(SLOTS, 128)
-    everyone = to_each(jnp.broadcast_to(arrived, (N_TP, SLOTS, 128)), "tp")
-    any_spec = pl.BlockSpec(memory_space=pl.ANY)
-    down_parts = pl.pallas_call(
+        (shape((TOK, 128)), shape((SLOTS, 128))),
+        [],
+        0,
+        (head_parts, residual, expert_ids),
+        range(3),
+    )
+    arrived = to_each(placed.reshape(EXPERTS, CAP, 128), "sp").reshape(2, 1, HALF, 128)
+    peers = jnp.arange(N_TP, dtype=jnp.int32)
+    half_of = jnp.where(lax.axis_index("sp") % 2 == 0, peers % 2, (peers // 4) % 2)
+    half_rows = jnp.where(half_of[:, None, None] == 0, arrived[0], arrived[1])
+    everyone = to_each(half_rows, "tp")
+    down_parts = kernel(
         expert_body,
-        out_shape=shape((N_TP, SLOTS, 128)),
-        in_specs=vmem(2) + [any_spec] * 3,
-        out_specs=vmem(1)[0],
-        scratch_shapes=[
-            pltpu.VMEM((SLOTS, D), BF16),
-            pltpu.VMEM((D, 256), BF16),
-            pltpu.VMEM((D, 256), BF16),
-            pltpu.VMEM((256, D), BF16),
-            pltpu.SemaphoreType.DMA((3,)),
+        shape((N_TP, HALF, 128)),
+        [
+            room((2, D, 256)),
+            room((2, D, 256)),
+            room((2, 256, D)),
+            room((HALF, D)),
         ],
-        name="expert",
-    )(everyone, norm_gain.reshape(1, D), gate_proj[0], up_proj[0], down_proj[0])
+        6,
+        (everyone, norm_gain.reshape(1, D), gate_proj, up_proj, down_proj, gate_b, up_b, down_b),
+        (0, 1),
+    )
     down_parts = to_each(down_parts, "tp")
-    expert_out = jnp.sum(down_parts.astype(F32), axis=0).astype(BF16)
+    expert_out = kernel(gather_sum_body, shape((SLOTS, 128)), [], 0, (down_parts,), (0,))
     returned = to_each(expert_out.reshape(EXPERTS, CAP, 128), "sp").reshape(SLOTS, 128)
-    return pl.pallas_call(
-        mix_body,
-        out_shape=shape((TOK, 128)),
-        in_specs=vmem(4),
-        out_specs=vmem(1)[0],
-        name="mix",
-    )(returned, stream, expert_ids, expert_weights)
+    return kernel(
+        mix_body, shape((TOK, 128)), [], 0, (returned, stream, expert_ids, expert_weights), range(4)
+    )
 
 
 def solution(mesh):
@@ -368,6 +433,7 @@
         P("sp", None, "tp"),
         P("sp", "tp", None),
     )
+
     return jax.shard_map(
         per_device, mesh=mesh, in_specs=in_specs, out_specs=P("sp", "tp"), check_vma=False
     )

time: 237 us -> 215 us (0.907)
  blocking collectives: 117 us -> 46.3 us
  waiting for transfers between devices: 46.5 us -> 81.1 us
  starting transfers between devices: 32.5 us -> 63.2 us
  Pallas kernels: 25.8 us -> 13.5 us
  local copies, waits for them, and re-layouts: 12.1 us -> 8.27 us
    all_to_all x4 -> x2, blocking collectives: 117 us -> 46.3 us  [to_each(): lax.all_to_all(array, axis, 0, 0, tiled=True, axis_index_groups=groups)]
    ppermute x0 -> x3, waiting for transfers between devices: none -> 27.5 us  [the longest x1 13.9 us: per_device(): down_b = lax.ppermute(down_proj, ('sp', 'tp'), PARTNER)]
    all_to_all x3 -> x5, starting transfers between devices: 17.1 us -> 40.4 us  [to_each(): lax.all_to_all(array, axis, 0, 0, tiled=True, axis_index_groups=groups)]
    pallas_call x7 -> x8, Pallas kernels: 25.8 us -> 13.5 us  [kernel(): pl.pallas_call(body, out_shape=outs, in_specs=[pl.BlockSpec(memory_space=...]
    ppermute x0 -> x3, starting transfers between devices: none -> 7.21 us  [the longest x1 3.36 us: per_device(): up_b = lax.ppermute(up_proj, ('sp', 'tp'), PARTNER)]
    all_to_all x3 -> x5, waiting for transfers between devices: 45.3 us -> 51.7 us  [to_each(): lax.all_to_all(array, axis, 0, 0, tiled=True, axis_index_groups=groups)]
    unnamed x32 -> x42, local copies, waits for them, and re-layouts: 9.64 us -> 6.38 us
  transfers between devices with their start and end apart: 5 -> 10, of which waited for: 4 -> 9; matrix products, arithmetic and copies ran while one was open for 1% -> 1% of each run, Pallas kernels for 0% -> 0%
where the time goes in v2:
time: 215 us; the launch traced here: 214 us
  waiting for transfers between devices  81.1 us (38%)
  starting transfers between devices  63.2 us (29%)
  blocking collectives  46.3 us (22%)
  Pallas kernels  13.5 us (6%)
  local copies, waits for them, and re-layouts  8.27 us (4%)
    all_to_all x5, waiting for transfers between devices, to_each(): lax.all_to_all(array, axis, 0, 0, tiled=True, axis_index_groups=groups)  51.7 us
    all_to_all x2, blocking collectives, to_each(): lax.all_to_all(array, axis, 0, 0, tiled=True, axis_index_groups=groups)  46.3 us
    all_to_all x5, starting transfers between devices, to_each(): lax.all_to_all(array, axis, 0, 0, tiled=True, axis_index_groups=groups)  40.4 us
    ppermute x1, waiting for transfers between devices, per_device(): down_b = lax.ppermute(down_proj, ('sp', 'tp'), PARTNER)  13.9 us
    ppermute x1, waiting for transfers between devices, per_device(): up_b = lax.ppermute(up_proj, ('sp', 'tp'), PARTNER)  13.6 us
    pallas_call x8, Pallas kernels, kernel(): pl.pallas_call(body, out_shape=outs, in_specs=[pl.BlockSpec(memory_space=...  13.5 us
    ppermute x1, starting transfers between devices, per_device(): from_other = lax.ppermute(other, 'sp', OTHER_CORE)  9.04 us
    ppermute x1, starting transfers between devices, per_device(): q_other = lax.ppermute(q_own, 'sp', OTHER_CORE)  6.52 us
  transfers between devices with their start and end apart: 10, of which 9 were waited for; matrix products, arithmetic and copies ran while one was open for 1% of the time, Pallas kernels for 0%

profile of v2, /device:TPU:1, one launch (start us, length us, event | category | flops | bytes accessed | tf_op | source)
XLA Modules:
  0.0 213.9 jit_solution(15484322054245600995)
XLA Ops:
  0.0 1.2 shard_map.172
  1.2 27.7 %all_to_all.35 = bf16[16,8,640]{2,1,0:T(8,128)(2,1)S(1)} all-to-all(bf16[16,8,640]{2,1,0:T(8,128)(2,1)S(1)} %shard_map.172), channel_id=1, replica_groups={{0,32,64,96,128,160,192,224,256,288,320,352,384,416,448,480},{16,48,80,..., dimensions={0} | all-to-all | bytes 327680 | tf_op jit(solution)/shard_map/all_to_all | solution.py:300
  29.0 0.1 maximum_dynamic-update-slice_fusion.after
  29.1 1.9 broadcast_in_dim.33
  31.0 6.9 %all-to-all-start.1 = ((bf16[16,576,128]{2,1,0:T(8,128)(2,1)}), bf16[16,576,128]{2,1,0:T(8,128)(2,1)S(1)}, u32[]{:S(2)}, u32[]{:S(2)}) async-start(bf16[16,576,128]{2,1,0:T(8,128)(2,1)} %broadcast_in_dim.33), calls=%async_computation.1 | async-start | bytes 4718592 | tf_op jit(solution)/shard_map/all_to_all | solution.py:300
  37.9 0.0 copy-start
  37.9 0.1 copy.20.ku_min
  38.0 0.1 copy.21.vu_min
  38.1 0.9 copy.19.maj
  39.0 0.0 copy-start.5
  39.1 0.9 copy-done.5
  40.0 0.9 copy-done.6
  40.9 0.8 copy-done.8
  41.6 0.6 shard_map.173
  42.2 0.7 copy-done.1
  42.9 6.5 %collective-permute-start = (bf16[128,320]{1,0:T(8,128)(2,1)S(1)}, bf16[128,320]{1,0:T(8,128)(2,1)S(1)}, u32[]{:S(2)}, u32[]{:S(2)}) collective-permute-start(bf16[128,320]{1,0:T(8,128)(2,1)S(1)} %get-tuple-element.11.q_own), channel_id=1, source_target_pairs={{0,16},{16,0},{32,48},{48,32},{64,80},{80,64},{96,112},{112,96},{1... | collective-permute-start | bytes 245768 | tf_op jit(solution)/shard_map/ppermute | solution.py:356
  49.5 0.9 collective-permute-done.q_other
  50.4 15.2 %all-to-all-done.1.keys = bf16[16,576,128]{2,1,0:T(8,128)(2,1)S(1)} async-done(((bf16[16,576,128]{2,1,0:T(8,128)(2,1)}), bf16[16,576,128]{2,1,0:T(8,128)(2,1)S(1)}, u32[]{:S(2)}, u32[]{:S(2)}) %all-to-all-start.1) | async-done | bytes 2359328 | tf_op jit(solution)/shard_map/all_to_all | solution.py:300
  65.6 1.0 copy-done.2
  66.6 3.6 %shard_map.174 = (f32[128,256]{1,0:T(8,128)S(1)}, f32[128,256]{1,0:T(8,128)S(1)}) custom-call(bf16[16,576,128]{2,1,0:T(8,128)(2,1)S(1)} %all-to-all-done.1.keys, bf16[128,320]{1,0:T(8,128)(2,1)S(1)} %get-tuple-element.11.q_own, bf16[128,320]{1,0:T(8,128)(2,1)S(1)} %collective-permute-done.q_other, bf16[512,384]{1,0:T(8,128)(2,1)S(1)} %copy-done.2), custom_call_target="tpu_custom_call" | custom-call | tf_op jit(solution)/shard_map/pallas_call | solution.py:289
  70.1 0.0 copy-start.10
  70.1 0.0 copy-start.11
  70.2 9.0 %collective-permute-start.1 = (f32[128,256]{1,0:T(8,128)S(1)}, f32[128,256]{1,0:T(8,128)S(1)}, u32[]{:S(2)}, u32[]{:S(2)}) collective-permute-start(f32[128,256]{1,0:T(8,128)S(1)} %get-tuple-element.14), channel_id=1, source_target_pairs={{0,16},{16,0},{32,48},{48,32},{64,80},{80,64},{96,112},{112,96},{1... | collective-permute-start | bytes 393224 | tf_op jit(solution)/shard_map/ppermute | solution.py:372
  79.2 1.0 collective-permute-done.1.b
  80.2 1.4 shard_map.175
  81.5 3.6 %all-to-all-start.2 = ((bf16[16,128,128]{2,1,0:T(8,128)(2,1)}), bf16[16,128,128]{2,1,0:T(8,128)(2,1)S(1)}, u32[]{:S(2)}, u32[]{:S(2)}) async-start(bf16[16,128,128]{2,1,0:T(8,128)(2,1)} %shard_map.175), calls=%async_computation.2 | async-start | bytes 1048576 | tf_op jit(solution)/shard_map/all_to_all | solution.py:300
  85.1 0.0 copy-start.9
  85.1 0.1 copy.22.ids
  85.2 10.8 %all-to-all-done.2.parts = bf16[16,128,128]{2,1,0:T(8,128)(2,1)S(1)} async-done(((bf16[16,128,128]{2,1,0:T(8,128)(2,1)}), bf16[16,128,128]{2,1,0:T(8,128)(2,1)S(1)}, u32[]{:S(2)}, u32[]{:S(2)}) %all-to-all-start.2) | async-done | bytes 524320 | tf_op jit(solution)/shard_map/all_to_all | solution.py:300
  96.1 1.3 shard_map.176
  97.4 11.6 %all-to-all-start.3 = ((bf16[32,16,128]{2,1,0:T(8,128)(2,1)}), bf16[32,16,128]{2,1,0:T(8,128)(2,1)S(1)}, u32[]{:S(2)}, u32[]{:S(2)}) async-start(bf16[32,16,128]{2,1,0:T(8,128)(2,1)} %bitcast.2), calls=%async_computation.3 | async-start | bytes 262144 | tf_op jit(solution)/shard_map/all_to_all | solution.py:300
  109.0 1.9 collective-permute-start.2
  110.9 3.4 %collective-permute-start.3 = (bf16[1,2048,256]{2,1,0:T(8,128)(2,1)S(1)}, bf16[1,2048,256]{2,1,0:T(8,128)(2,1)}, u32[]{:S(2)}, u32[]{:S(2)}) collective-permute-start(bf16[1,2048,256]{2,1,0:T(8,128)(2,1)S(1)} %copy-done.11), channel_id=1, source_target_pairs={{0,1},{1,0},{2,3},{3,2},{4,5},{5,4},{6,7},{7,6},{8,9},{9,8},{10,11... | collective-permute-start | bytes 3145736 | tf_op jit(solution)/shard_map/ppermute | solution.py:358
  114.3 1.9 collective-permute-start.4
  116.3 8.6 %all-to-all-done.3 = bf16[32,16,128]{2,1,0:T(8,128)(2,1)S(1)} async-done(((bf16[32,16,128]{2,1,0:T(8,128)(2,1)}), bf16[32,16,128]{2,1,0:T(8,128)(2,1)S(1)}, u32[]{:S(2)}, u32[]{:S(2)}) %all-to-all-start.3) | async-done | bytes 131104 | tf_op jit(solution)/shard_map/all_to_all | solution.py:300
  124.8 1.1 broadcast_select_fusion
  126.0 3.7 %all-to-all-start.4 = ((bf16[16,256,128]{2,1,0:T(8,128)(2,1)}), bf16[16,256,128]{2,1,0:T(8,128)(2,1)S(1)}, u32[]{:S(2)}, u32[]{:S(2)}) async-start(bf16[16,256,128]{2,1,0:T(8,128)(2,1)} %broadcast_select_fusion), calls=%async_computation.4 | async-start | bytes 2097152 | tf_op jit(solution)/shard_map/all_to_all | solution.py:300
  129.6 13.6 %collective-permute-done.3.up_b = bf16[1,2048,256]{2,1,0:T(8,128)(2,1)} collective-permute-done((bf16[1,2048,256]{2,1,0:T(8,128)(2,1)S(1)}, bf16[1,2048,256]{2,1,0:T(8,128)(2,1)}, u32[]{:S(2)}, u32[]{:S(2)}) %collective-permute-start.3) | collective-permute-done | bytes 1048608 | tf_op jit(solution)/shard_map/ppermute | solution.py:358
  143.2 13.9 %collective-permute-done.4.down_b = bf16[1,256,2048]{2,1,0:T(8,128)(2,1)} collective-permute-done((bf16[1,256,2048]{2,1,0:T(8,128)(2,1)}, bf16[1,256,2048]{2,1,0:T(8,128)(2,1)}, u32[]{:S(2)}, u32[]{:S(2)}) %collective-permute-start.4) | collective-permute-done | bytes 1048608 | tf_op jit(solution)/shard_map/ppermute | solution.py:359
  157.1 1.4 all-to-all-done.4.got
  158.5 4.1 %shard_map.177 = bf16[16,256,128]{2,1,0:T(8,128)(2,1)S(1)} custom-call(bf16[16,256,128]{2,1,0:T(8,128)(2,1)S(1)} %all-to-all-done.4.got, f32[1,2048]{1,0:T(1,128)S(1)} %bitcast.9, bf16[1,2048,256]{2,1,0:T(8,128)(2,1)} %gate_a.1, bf16[1,2048,256]{2,1,0:T(8,128)(2,1)} %up_a.1, bf16[1,256,2048]{2,1,0:T(8,128)(2,1)} %down_a.1, ...), custom_call_target="tpu_custom_call" | custom-call | tf_op jit(solution)/shard_map/pallas_call | solution.py:289
  162.6 18.7 %all_to_all.36.parts = bf16[16,256,128]{2,1,0:T(8,128)(2,1)S(1)} all-to-all(bf16[16,256,128]{2,1,0:T(8,128)(2,1)S(1)} %shard_map.177), channel_id=1, replica_groups=mesh['sp'=32,'tp'=16] {'tp'}, dimensions={0} | all-to-all | bytes 2097152 | tf_op jit(solution)/shard_map/all_to_all | solution.py:300
  181.3 0.8 shard_map.178
  182.1 14.7 %all-to-all-start.6 = ((bf16[32,16,128]{2,1,0:T(8,128)(2,1)}), bf16[32,16,128]{2,1,0:T(8,128)(2,1)S(1)}, u32[]{:S(2)}, u32[]{:S(2)}) async-start(bf16[32,16,128]{2,1,0:T(8,128)(2,1)} %bitcast.6), calls=%async_computation.6 | async-start | bytes 262144 | tf_op jit(solution)/shard_map/all_to_all | solution.py:300
  196.8 0.1 copy.24.weights
  196.9 15.7 %all-to-all-done.6 = bf16[32,16,128]{2,1,0:T(8,128)(2,1)S(1)} async-done(((bf16[32,16,128]{2,1,0:T(8,128)(2,1)}), bf16[32,16,128]{2,1,0:T(8,128)(2,1)S(1)}, u32[]{:S(2)}, u32[]{:S(2)}) %all-to-all-start.6) | async-done | bytes 131104 | tf_op jit(solution)/shard_map/all_to_all | solution.py:300
  212.6 0.6 shard_map.179
  213.3 0.6 copy.29
  (30 shorter events, 0.1 us)
Async XLA Ops:
  30.9 6.9 %copy-start.12 = (bf16[512,64]{0,1:T(8,128)(2,1)S(1)}, bf16[512,64]{0,1:T(8,128)(2,1)}, u32[]{:S(2)}) copy-start(bf16[512,64]{0,1:T(8,128)(2,1)} %param.24) | copy-start | bytes 196612
  30.9 7.0 %copy-start.13 = (bf16[512,64]{0,1:T(8,128)(2,1)S(1)}, bf16[512,64]{0,1:T(8,128)(2,1)}, u32[]{:S(2)}) copy-start(bf16[512,64]{0,1:T(8,128)(2,1)} %param.25) | copy-start | bytes 196612
  30.9 8.1 %copy-start.3 = (f32[160,128]{1,0:T(8,128)S(1)}, f32[160,128]{1,0:T(8,128)}, u32[]{:S(2)}) copy-start(f32[160,128]{1,0:T(8,128)} %constant.52.clone.table_in.table) | copy-start | bytes 245764
  31.0 34.6 %all-to-all-start.1 = ((bf16[16,576,128]{2,1,0:T(8,128)(2,1)}), bf16[16,576,128]{2,1,0:T(8,128)(2,1)S(1)}, u32[]{:S(2)}, u32[]{:S(2)}) async-start(bf16[16,576,128]{2,1,0:T(8,128)(2,1)} %broadcast_in_dim.33), calls=%async_computation.1 | async-start | bytes 4718592 | tf_op jit(solution)/shard_map/all_to_all | solution.py:300
  37.9 42.3 %copy-start = (bf16[128,2048]{1,0:T(8,128)(2,1)S(1)}, bf16[128,2048]{1,0:T(8,128)(2,1)}, u32[]{:S(2)}) copy-start(bf16[128,2048]{1,0:T(8,128)(2,1)} %out_maj.1) | copy-start | bytes 1572868
  39.0 0.9 copy-start.5
  40.0 0.9 copy-start.6
  40.9 0.8 copy-start.8
  42.2 0.8 copy-start.1
  42.9 7.5 %collective-permute-start = (bf16[128,320]{1,0:T(8,128)(2,1)S(1)}, bf16[128,320]{1,0:T(8,128)(2,1)S(1)}, u32[]{:S(2)}, u32[]{:S(2)}) collective-permute-start(bf16[128,320]{1,0:T(8,128)(2,1)S(1)} %get-tuple-element.11.q_own), channel_id=1, source_target_pairs={{0,16},{16,0},{32,48},{48,32},{64,80},{80,64},{96,112},{112,96},{1... | collective-permute-start | bytes 245768 | tf_op jit(solution)/shard_map/ppermute | solution.py:356
  65.6 1.0 copy-start.2
  66.6 13.6 %copy-start.4 = (bf16[64,2048]{1,0:T(8,128)(2,1)S(1)}, bf16[64,2048]{1,0:T(8,128)(2,1)}, u32[]{:S(2)}) copy-start(bf16[64,2048]{1,0:T(8,128)(2,1)} %out_min.1) | copy-start | bytes 786436
  66.6 18.5 %copy-start.14 = (s32[128,2]{0,1:T(2,128)S(1)}, s32[128,2]{0,1:T(2,128)}, u32[]{:S(2)}) copy-start(s32[128,2]{0,1:T(2,128)} %param.30) | copy-start | bytes 3076
  66.6 29.5 %copy-start.7 = (bf16[128,128]{1,0:T(8,128)(2,1)S(1)}, bf16[128,128]{1,0:T(8,128)(2,1)}, u32[]{:S(2)}) copy-start(bf16[128,128]{1,0:T(8,128)(2,1)} %residual.1) | copy-start | bytes 98308
  70.1 38.8 %copy-start.10 = (bf16[1,2048,256]{2,1,0:T(8,128)(2,1)S(1)}, bf16[1,2048,256]{2,1,0:T(8,128)(2,1)}, u32[]{:S(2)}) copy-start(bf16[1,2048,256]{2,1,0:T(8,128)(2,1)} %gate_a.1) | copy-start | bytes 3145732
  70.1 40.8 %copy-start.11 = (bf16[1,2048,256]{2,1,0:T(8,128)(2,1)S(1)}, bf16[1,2048,256]{2,1,0:T(8,128)(2,1)}, u32[]{:S(2)}) copy-start(bf16[1,2048,256]{2,1,0:T(8,128)(2,1)} %up_a.1) | copy-start | bytes 3145732
  70.2 10.0 %collective-permute-start.1 = (f32[128,256]{1,0:T(8,128)S(1)}, f32[128,256]{1,0:T(8,128)S(1)}, u32[]{:S(2)}, u32[]{:S(2)}) collective-permute-start(f32[128,256]{1,0:T(8,128)S(1)} %get-tuple-element.14), channel_id=1, source_target_pairs={{0,16},{16,0},{32,48},{48,32},{64,80},{80,64},{96,112},{112,96},{1... | collective-permute-start | bytes 393224 | tf_op jit(solution)/shard_map/ppermute | solution.py:372
  81.5 14.5 %all-to-all-start.2 = ((bf16[16,128,128]{2,1,0:T(8,128)(2,1)}), bf16[16,128,128]{2,1,0:T(8,128)(2,1)S(1)}, u32[]{:S(2)}, u32[]{:S(2)}) async-start(bf16[16,128,128]{2,1,0:T(8,128)(2,1)} %shard_map.175), calls=%async_computation.2 | async-start | bytes 1048576 | tf_op jit(solution)/shard_map/all_to_all | solution.py:300
  85.1 73.4 %copy-start.9 = (f32[2048]{0:T(1024)S(1)}, f32[2048]{0:T(1024)}, u32[]{:S(2)}) copy-start(f32[2048]{0:T(1024)} %param.29) | copy-start | bytes 24580
  97.4 27.5 %all-to-all-start.3 = ((bf16[32,16,128]{2,1,0:T(8,128)(2,1)}), bf16[32,16,128]{2,1,0:T(8,128)(2,1)S(1)}, u32[]{:S(2)}, u32[]{:S(2)}) async-start(bf16[32,16,128]{2,1,0:T(8,128)(2,1)} %bitcast.2), calls=%async_computation.3 | async-start | bytes 262144 | tf_op jit(solution)/shard_map/all_to_all | solution.py:300
  109.0 20.6 %collective-permute-start.2 = (bf16[1,2048,256]{2,1,0:T(8,128)(2,1)S(1)}, bf16[1,2048,256]{2,1,0:T(8,128)(2,1)}, u32[]{:S(2)}, u32[]{:S(2)}) collective-permute-start(bf16[1,2048,256]{2,1,0:T(8,128)(2,1)S(1)} %copy-done.10), channel_id=1, source_target_pairs={{0,1},{1,0},{2,3},{3,2},{4,5},{5,4},{6,7},{7,6},{8,9},{9,8},{10,11... | collective-permute-start | bytes 3145736 | tf_op jit(solution)/shard_map/ppermute | solution.py:357
  110.9 32.3 %collective-permute-start.3 = (bf16[1,2048,256]{2,1,0:T(8,128)(2,1)S(1)}, bf16[1,2048,256]{2,1,0:T(8,128)(2,1)}, u32[]{:S(2)}, u32[]{:S(2)}) collective-permute-start(bf16[1,2048,256]{2,1,0:T(8,128)(2,1)S(1)} %copy-done.11), channel_id=1, source_target_pairs={{0,1},{1,0},{2,3},{3,2},{4,5},{5,4},{6,7},{7,6},{8,9},{9,8},{10,11... | collective-permute-start | bytes 3145736 | tf_op jit(solution)/shard_map/ppermute | solution.py:358
  114.3 42.8 %collective-permute-start.4 = (bf16[1,256,2048]{2,1,0:T(8,128)(2,1)}, bf16[1,256,2048]{2,1,0:T(8,128)(2,1)}, u32[]{:S(2)}, u32[]{:S(2)}) collective-permute-start(bf16[1,256,2048]{2,1,0:T(8,128)(2,1)} %down_a.1), channel_id=1, source_target_pairs={{0,1},{1,0},{2,3},{3,2},{4,5},{5,4},{6,7},{7,6},{8,9},{9,8},{10,11... | collective-permute-start | bytes 3145736 | tf_op jit(solution)/shard_map/ppermute | solution.py:359
  126.0 32.6 %all-to-all-start.4 = ((bf16[16,256,128]{2,1,0:T(8,128)(2,1)}), bf16[16,256,128]{2,1,0:T(8,128)(2,1)S(1)}, u32[]{:S(2)}, u32[]{:S(2)}) async-start(bf16[16,256,128]{2,1,0:T(8,128)(2,1)} %broadcast_select_fusion), calls=%async_computation.4 | async-start | bytes 2097152 | tf_op jit(solution)/shard_map/all_to_all | solution.py:300
  162.6 34.2 %copy-start.15 = (f32[128,2]{0,1:T(2,128)S(1)}, f32[128,2]{0,1:T(2,128)}, u32[]{:S(2)}) copy-start(f32[128,2]{0,1:T(2,128)} %param.31) | copy-start | bytes 3076
  182.1 30.6 %all-to-all-start.6 = ((bf16[32,16,128]{2,1,0:T(8,128)(2,1)}), bf16[32,16,128]{2,1,0:T(8,128)(2,1)S(1)}, u32[]{:S(2)}, u32[]{:S(2)}) async-start(bf16[32,16,128]{2,1,0:T(8,128)(2,1)} %bitcast.6), calls=%async_computation.6 | async-start | bytes 262144 | tf_op jit(solution)/shard_map/all_to_all | solution.py:300

commit v3 on v2

--- a/solution.py
+++ b/solution.py
@@ -38,7 +38,32 @@
 
 SAME_CORE = [[z * 2 + c for z in range(N_Z)] for c in range(2)]
 OTHER_CORE = [(i, i ^ 1) for i in range(2 * N_Z)]
-PARTNER = [(s * N_TP + t, s * N_TP + (t ^ (4 if s % 2 else 1))) for s in range(2 * N_Z) for t in range(N_TP)]
+
+
+def ring(step):
+    moves = []
+    for s in range(2 * N_Z):
+        for t in range(N_TP):
+            y, x = divmod(t, 4)
+            to = (y + step) % 4 * 4 + x if s % 2 else y * 4 + (x + step) % 4
+            moves.append((s * N_TP + t, s * N_TP + to))
+    return moves
+
+
+HALF = SLOTS // 2
+
+
+def turns(positions):
+    angles = positions[:, None] * (1.0 / 10000.0 ** (np.arange(32) / 32.0))[None, :]
+    return np.concatenate([np.cos(angles), np.sin(angles), np.zeros((len(positions), 64))], axis=1)
+
+
+TABLE = np.concatenate([turns(np.arange(2 * N_Z) * float(TOK)), turns(np.arange(TOK) * 1.0)]).astype(
+    np.float32
+)
+
+SAME_CORE = [[z * 2 + c for z in range(N_Z)] for c in range(2)]
+OTHER_CORE = [(i, i ^ 1) for i in range(2 * N_Z)]
 
 
 ANY = pl.BlockSpec(memory_space=pl.ANY)
@@ -106,13 +131,18 @@
 N_CHUNK = KEYS // CHUNK
 
 
-def attend_body(keys, q_own, q_other, up_weights, own, other, s_maj, s_min, v_all):
+def attend_body(
+    keys, q_own_in, q_other_in, up_in, own, other, s_maj, s_min, v_all, q_all, up_weights, sems
+):
+    copies = fetch(
+        ((up_in, up_weights), (q_own_in, q_all.at[pl.ds(0, TOK)]), (q_other_in, q_all.at[pl.ds(TOK, TOK)])),
+        sems,
+    )
     per = CHUNK // 128
+    copies[0].wait()
+    weights = up_weights[...]
     me = lax.axis_index("sp")
     core = me % 2
-    weights = up_weights[...]
-    q = jnp.concatenate([q_own[...], q_other[...]], axis=0)
-    q_maj, q_min = q[:, :192], q[:, 192:320]
     row = lax.broadcasted_iota(jnp.int32, (2 * TOK, 1), 0)
     q_pos = jnp.where(row < TOK, me * TOK + row, (me + 1 - 2 * core) * TOK + row - TOK)
     scale_maj = (NOPE_MAJOR + ROPE) ** -0.5
@@ -130,6 +160,10 @@
         lat = jnp.concatenate(lat_rows, axis=0)
         rope = jnp.concatenate(rope_rows, axis=0)
         up = dot(lat, weights).astype(BF16)
+        if n == 0:
+            copies[1].wait()
+            copies[2].wait()
+            q_maj, q_min = q_all[:, :192], q_all[:, 192:320]
         k_maj = jnp.concatenate([up[:, :128], rope], axis=1)
         k_min = jnp.concatenate([up[:, 256:320], rope], axis=1)
         v_all[CHUNK * n : CHUNK * (n + 1), :] = jnp.concatenate([up[:, 128:256], up[:, 320:384]], axis=1)
@@ -212,22 +246,38 @@
     placed[...] = dot(select, rows, ((0,), (0,))).astype(BF16)
 
 
+def pack_body(gate, up, down, low, high, sems):
+    pairs = []
+    for i, out in enumerate((low, high)):
+        mine = pl.ds(128 * i, 128)
+        pairs.append((gate.at[0, :, mine], out.at[pl.ds(0, D)]))
+        pairs.append((up.at[0, :, mine], out.at[pl.ds(D, D)]))
+        for t in range(N_TP):
+            pairs.append((down.at[0, mine, pl.ds(128 * t, 128)], out.at[pl.ds(2 * D + 128 * t, 128)]))
+    for c in fetch(pairs, sems):
+        c.wait()
+
+
 def expert_body(
-    got, gain, gate_a, up_a, down_a, gate_b, up_b, down_b,
+    got, gain, gate_a, up_a, down_a, low, high,
     parts,
     gate_w, up_w, down_w, x, sems,
 ):
-    copies = fetch(
-        (
-            (gate_a.at[0], gate_w.at[0]),
-            (gate_b.at[0], gate_w.at[1]),
-            (up_a.at[0], up_w.at[0]),
-            (up_b.at[0], up_w.at[1]),
-            (down_a.at[0], down_w.at[0]),
-            (down_b.at[0], down_w.at[1]),
-        ),
-        sems,
-    )
+    pairs = [(gate_a.at[0], gate_w.at[0]), (up_a.at[0], up_w.at[0])]
+    for i, packed in enumerate((low, high)):
+        mine = pl.ds(128 * i, 128)
+        pairs.append((packed.at[pl.ds(0, D)], gate_w.at[1, :, mine]))
+        pairs.append((packed.at[pl.ds(D, D)], up_w.at[1, :, mine]))
+    pairs.append((down_a.at[0], down_w.at[0]))
+    for i, packed in enumerate((low, high)):
+        for t in range(N_TP):
+            pairs.append(
+                (
+                    packed.at[pl.ds(2 * D + 128 * t, 128)],
+                    down_w.at[1, pl.ds(128 * i, 128), pl.ds(128 * t, 128)],
+                )
+            )
+    copies = fetch(pairs, sems)
     squares = jnp.zeros((HALF, 128), F32)
     for t in range(N_TP):
         v = got[t].astype(F32)
@@ -239,13 +289,13 @@
         ).astype(BF16)
     hidden = []
     for i in range(2):
-        copies[i].wait()
-        copies[2 + i].wait()
+        for c in copies[2 * i : 2 + 4 * i]:
+            c.wait()
         gate = dot(x[...], gate_w[i])
         up = dot(x[...], up_w[i])
         hidden.append((gate / (1.0 + jnp.exp(-gate)) * up).astype(BF16))
-    copies[4].wait()
-    copies[5].wait()
+    for c in copies[6:]:
+        c.wait()
     for t in range(0, N_TP, 2):
         cols = slice(128 * t, 128 * (t + 2))
         value = dot(hidden[0], down_w[0, :, cols]) + dot(hidden[1], down_w[1, :, cols])
@@ -327,7 +377,15 @@
         3,
         (latent_rows, rope_keys.T, table),
     )
-    flat = to_each(rows, "sp", SAME_CORE).reshape(N_Z * ROWS, 640)
+    got_rows = to_each(rows, "sp", SAME_CORE)
+    low, high = kernel(
+        pack_body,
+        (shape((3 * D, 128)), shape((3 * D, 128))),
+        [],
+        4 + 2 * N_TP,
+        (gate_proj, up_proj, down_proj),
+    )
+    flat = got_rows.reshape(N_Z * ROWS, 640)
     rope = flat[:, 512:576]
     packed = jnp.concatenate(
         [flat[:, 128 * k : 128 * (k + 1)] for k in range(4)]
@@ -354,9 +412,8 @@
         range(8),
     )
     q_other = lax.ppermute(q_own, "sp", OTHER_CORE)
-    gate_b = lax.ppermute(gate_proj, ("sp", "tp"), PARTNER)
-    up_b = lax.ppermute(up_proj, ("sp", "tp"), PARTNER)
-    down_b = lax.ppermute(down_proj, ("sp", "tp"), PARTNER)
+    from_low = lax.ppermute(low, ("sp", "tp"), ring(1))
+    from_high = lax.ppermute(high, ("sp", "tp"), ring(-1))
     own, other = kernel(
         attend_body,
         (shape((TOK, 256), F32), shape((TOK, 256), F32)),
@@ -364,10 +421,12 @@
             room((2 * TOK, KEYS), F32),
             room((2 * TOK, KEYS), F32),
             room((KEYS, 192)),
+            room((2 * TOK, 320)),
+            room((LATENT, 384)),
         ],
-        0,
+        3,
         (keys, q_own, q_other, up_weights),
-        range(4),
+        (0,),
     )
     from_other = lax.ppermute(other, "sp", OTHER_CORE)
     head_parts = kernel(
@@ -401,8 +460,8 @@
             room((2, 256, D)),
             room((HALF, D)),
         ],
-        6,
-        (everyone, norm_gain.reshape(1, D), gate_proj, up_proj, down_proj, gate_b, up_b, down_b),
+        7 + 2 * N_TP,
+        (everyone, norm_gain.reshape(1, D), gate_proj, up_proj, down_proj, from_low, from_high),
         (0, 1),
     )
     down_parts = to_each(down_parts, "tp")

time: 215 us -> 205 us (0.953)
  waiting for transfers between devices: 81.1 us -> 70.7 us
  Pallas kernels: 13.5 us -> 17.9 us
  local copies, waits for them, and re-layouts: 8.27 us -> 3.93 us
    ppermute x3 -> x2, waiting for transfers between devices: 27.5 us -> 16.9 us  [the longest x1 10.4 us: per_device(): from_high = lax.ppermute(high, ('sp', 'tp'), ring(-1))]
    pallas_call x8 -> x9, Pallas kernels: 13.5 us -> 17.9 us  [kernel(): pl.pallas_call(body, out_shape=outs, in_specs=[pl.BlockSpec(memory_space=...]
    unnamed x42, local copies, waits for them, and re-layouts: 6.38 us -> 2.05 us
    ppermute x3 -> x2, starting transfers between devices: 7.21 us -> 6.5 us  [the longest x1 4.57 us: per_device(): from_high = lax.ppermute(high, ('sp', 'tp'), ring(-1))]
  transfers between devices with their start and end apart: 10 -> 9, of which waited for: 9 -> 9; matrix products, arithmetic and copies ran while one was open for 1% -> 1% of each run, Pallas kernels for 0% -> 2%
where the time goes in v3:
time: 205 us; the launch traced here: 204 us
  waiting for transfers between devices  70.7 us (34%)
  starting transfers between devices  64.6 us (32%)
  blocking collectives  45.4 us (22%)
  Pallas kernels  17.9 us (9%)
  local copies, waits for them, and re-layouts  3.93 us (2%)
    all_to_all x5, waiting for transfers between devices, to_each(): lax.all_to_all(array, axis, 0, 0, tiled=True, axis_index_groups=groups)  51.8 us
    all_to_all x2, blocking collectives, to_each(): lax.all_to_all(array, axis, 0, 0, tiled=True, axis_index_groups=groups)  45.4 us
    all_to_all x5, starting transfers between devices, to_each(): lax.all_to_all(array, axis, 0, 0, tiled=True, axis_index_groups=groups)  42.5 us
    pallas_call x9, Pallas kernels, kernel(): pl.pallas_call(body, out_shape=outs, in_specs=[pl.BlockSpec(memory_space=...  17.9 us
    ppermute x1, waiting for transfers between devices, per_device(): from_high = lax.ppermute(high, ('sp', 'tp'), ring(-1))  10.4 us
    ppermute x1, starting transfers between devices, per_device(): from_other = lax.ppermute(other, 'sp', OTHER_CORE)  8.92 us
    ppermute x1, starting transfers between devices, per_device(): q_other = lax.ppermute(q_own, 'sp', OTHER_CORE)  6.65 us
    ppermute x1, waiting for transfers between devices, per_device(): from_low = lax.ppermute(low, ('sp', 'tp'), ring(1))  6.5 us
  transfers between devices with their start and end apart: 9, of which 9 were waited for; matrix products, arithmetic and copies ran while one was open for 1% of the time, Pallas kernels for 2%

profile of v3, /device:TPU:1, one launch (start us, length us, event | category | flops | bytes accessed | tf_op | source)
XLA Modules:
  0.0 204.1 jit_solution(7003979937862458226)
XLA Ops:
  0.0 1.2 shard_map.172
  1.2 27.7 %all_to_all.35 = bf16[16,8,640]{2,1,0:T(8,128)(2,1)S(1)} all-to-all(bf16[16,8,640]{2,1,0:T(8,128)(2,1)S(1)} %shard_map.172), channel_id=1, replica_groups={{0,32,64,96,128,160,192,224,256,288,320,352,384,416,448,480},{16,48,80,..., dimensions={0} | all-to-all | bytes 327680 | tf_op jit(solution)/shard_map/all_to_all | solution.py:350
  29.0 0.1 maximum_dynamic-update-slice_fusion.after
  29.1 1.9 broadcast_in_dim.33
  31.0 0.0 copy-start.4
  31.0 0.0 copy-start.5
  31.0 0.0 copy-start.8
  31.0 6.9 %all-to-all-start.1 = ((bf16[16,576,128]{2,1,0:T(8,128)(2,1)}), bf16[16,576,128]{2,1,0:T(8,128)(2,1)S(1)}, u32[]{:S(2)}, u32[]{:S(2)}) async-start(bf16[16,576,128]{2,1,0:T(8,128)(2,1)} %broadcast_in_dim.33), calls=%async_computation.1 | async-start | bytes 4718592 | tf_op jit(solution)/shard_map/all_to_all | solution.py:350
  37.9 0.1 copy.20.ku_min
  38.0 0.0 copy-done.12
  38.0 0.1 copy.21.vu_min
  38.2 0.1 copy.19.maj
  38.3 0.6 shard_map.173
  38.9 0.0 copy-start.1
  38.9 0.7 copy-done.1
  39.7 6.7 %collective-permute-start = (bf16[128,320]{1,0:T(8,128)(2,1)S(1)}, bf16[128,320]{1,0:T(8,128)(2,1)S(1)}, u32[]{:S(2)}, u32[]{:S(2)}) collective-permute-start(bf16[128,320]{1,0:T(8,128)(2,1)S(1)} %get-tuple-element.13.q_own_in), channel_id=1, source_target_pairs={{0,16},{16,0},{32,48},{48,32},{64,80},{80,64},{96,112},{112,96},{1... | collective-permute-start | bytes 245768 | tf_op jit(solution)/shard_map/ppermute | solution.py:414
  46.3 0.9 collective-permute-done.q_other_in
  47.2 18.4 %all-to-all-done.1.keys = bf16[16,576,128]{2,1,0:T(8,128)(2,1)S(1)} async-done(((bf16[16,576,128]{2,1,0:T(8,128)(2,1)}), bf16[16,576,128]{2,1,0:T(8,128)(2,1)S(1)}, u32[]{:S(2)}, u32[]{:S(2)}) %all-to-all-start.1) | async-done | bytes 2359328 | tf_op jit(solution)/shard_map/all_to_all | solution.py:350
  65.6 4.8 %shard_map.174 = (f32[128,256]{1,0:T(8,128)S(1)}, f32[128,256]{1,0:T(8,128)S(1)}) custom-call(bf16[16,576,128]{2,1,0:T(8,128)(2,1)S(1)} %all-to-all-done.1.keys, bf16[128,320]{1,0:T(8,128)(2,1)} %copy-done.6, bf16[128,320]{1,0:T(8,128)(2,1)} %copy-done.10, bf16[512,384]{1,0:T(8,128)(2,1)} %copy-done.1), custom_call_target="tpu_custom_call" | custom-call | tf_op jit(solution)/shard_map/pallas_call | solution.py:339
  70.4 0.0 copy-start.14
  70.4 0.0 copy-start.7
  70.4 8.9 %collective-permute-start.1 = (f32[128,256]{1,0:T(8,128)S(1)}, f32[128,256]{1,0:T(8,128)S(1)}, u32[]{:S(2)}, u32[]{:S(2)}) collective-permute-start(f32[128,256]{1,0:T(8,128)S(1)} %get-tuple-element.16), channel_id=1, source_target_pairs={{0,16},{16,0},{32,48},{48,32},{64,80},{80,64},{96,112},{112,96},{1... | collective-permute-start | bytes 393224 | tf_op jit(solution)/shard_map/ppermute | solution.py:431
  79.3 1.0 collective-permute-done.1.b
  80.3 1.4 shard_map.175
  81.7 3.6 %all-to-all-start.2 = ((bf16[16,128,128]{2,1,0:T(8,128)(2,1)}), bf16[16,128,128]{2,1,0:T(8,128)(2,1)S(1)}, u32[]{:S(2)}, u32[]{:S(2)}) async-start(bf16[16,128,128]{2,1,0:T(8,128)(2,1)} %shard_map.175), calls=%async_computation.2 | async-start | bytes 1048576 | tf_op jit(solution)/shard_map/all_to_all | solution.py:350
  85.3 0.1 copy.22.ids
  85.4 10.8 %all-to-all-done.2.parts = bf16[16,128,128]{2,1,0:T(8,128)(2,1)S(1)} async-done(((bf16[16,128,128]{2,1,0:T(8,128)(2,1)}), bf16[16,128,128]{2,1,0:T(8,128)(2,1)S(1)}, u32[]{:S(2)}, u32[]{:S(2)}) %all-to-all-start.2) | async-done | bytes 524320 | tf_op jit(solution)/shard_map/all_to_all | solution.py:350
  96.2 1.3 shard_map.176
  97.5 11.6 %all-to-all-start.3 = ((bf16[32,16,128]{2,1,0:T(8,128)(2,1)}), bf16[32,16,128]{2,1,0:T(8,128)(2,1)S(1)}, u32[]{:S(2)}, u32[]{:S(2)}) async-start(bf16[32,16,128]{2,1,0:T(8,128)(2,1)} %bitcast.2), calls=%async_computation.3 | async-start | bytes 262144 | tf_op jit(solution)/shard_map/all_to_all | solution.py:350
  109.1 3.2 %shard_map.177 = (bf16[6144,128]{1,0:T(8,128)(2,1)}, bf16[6144,128]{1,0:T(8,128)(2,1)S(1)}) custom-call(bf16[1,2048,256]{2,1,0:T(8,128)(2,1)} %gate_a.1, bf16[1,2048,256]{2,1,0:T(8,128)(2,1)} %up_a.1, bf16[1,256,2048]{2,1,0:T(8,128)(2,1)} %down_a.1), custom_call_target="tpu_custom_call" | custom-call | tf_op jit(solution)/shard_map/pallas_call | solution.py:339
  112.3 1.9 collective-permute-start.2
  114.2 4.6 %collective-permute-start.3 = (bf16[6144,128]{1,0:T(8,128)(2,1)S(1)}, bf16[6144,128]{1,0:T(8,128)(2,1)}, u32[]{:S(2)}, u32[]{:S(2)}) collective-permute-start(bf16[6144,128]{1,0:T(8,128)(2,1)S(1)} %get-tuple-element.19), channel_id=1, source_target_pairs={{0,3},{1,0},{2,1},{3,2},{4,7},{5,4},{6,5},{7,6},{8,11},{9,8},{10,9... | collective-permute-start | bytes 4718600 | tf_op jit(solution)/shard_map/ppermute | solution.py:416
  118.8 6.1 %all-to-all-done.3 = bf16[32,16,128]{2,1,0:T(8,128)(2,1)S(1)} async-done(((bf16[32,16,128]{2,1,0:T(8,128)(2,1)}), bf16[32,16,128]{2,1,0:T(8,128)(2,1)S(1)}, u32[]{:S(2)}, u32[]{:S(2)}) %all-to-all-start.3) | async-done | bytes 131104 | tf_op jit(solution)/shard_map/all_to_all | solution.py:350
  124.9 0.0 copy-start.9
  125.0 1.1 broadcast_select_fusion
  126.1 3.7 %all-to-all-start.4 = ((bf16[16,256,128]{2,1,0:T(8,128)(2,1)}), bf16[16,256,128]{2,1,0:T(8,128)(2,1)S(1)}, u32[]{:S(2)}, u32[]{:S(2)}) async-start(bf16[16,256,128]{2,1,0:T(8,128)(2,1)} %broadcast_select_fusion), calls=%async_computation.4 | async-start | bytes 2097152 | tf_op jit(solution)/shard_map/all_to_all | solution.py:350
  129.8 6.5 %collective-permute-done.2.low = bf16[6144,128]{1,0:T(8,128)(2,1)} collective-permute-done((bf16[6144,128]{1,0:T(8,128)(2,1)}, bf16[6144,128]{1,0:T(8,128)(2,1)}, u32[]{:S(2)}, u32[]{:S(2)}) %collective-permute-start.2) | collective-permute-done | bytes 1572896 | tf_op jit(solution)/shard_map/ppermute | solution.py:415
  136.3 10.4 %collective-permute-done.3.high = bf16[6144,128]{1,0:T(8,128)(2,1)} collective-permute-done((bf16[6144,128]{1,0:T(8,128)(2,1)S(1)}, bf16[6144,128]{1,0:T(8,128)(2,1)}, u32[]{:S(2)}, u32[]{:S(2)}) %collective-permute-start.3) | collective-permute-done | bytes 1572896 | tf_op jit(solution)/shard_map/ppermute | solution.py:416
  146.7 0.8 all-to-all-done.4.got
  147.5 4.1 %shard_map.178 = bf16[16,256,128]{2,1,0:T(8,128)(2,1)S(1)} custom-call(bf16[16,256,128]{2,1,0:T(8,128)(2,1)S(1)} %all-to-all-done.4.got, f32[1,2048]{1,0:T(1,128)S(1)} %bitcast.9, bf16[1,2048,256]{2,1,0:T(8,128)(2,1)} %gate_a.1, bf16[1,2048,256]{2,1,0:T(8,128)(2,1)} %up_a.1, bf16[1,256,2048]{2,1,0:T(8,128)(2,1)} %down_a.1, ...), custom_call_target="tpu_custom_call" | custom-call | tf_op jit(solution)/shard_map/pallas_call | solution.py:339
  151.7 0.0 copy-start.15
  151.7 17.7 %all_to_all.36.parts = bf16[16,256,128]{2,1,0:T(8,128)(2,1)S(1)} all-to-all(bf16[16,256,128]{2,1,0:T(8,128)(2,1)S(1)} %shard_map.178), channel_id=1, replica_groups=mesh['sp'=32,'tp'=16] {'tp'}, dimensions={0} | all-to-all | bytes 2097152 | tf_op jit(solution)/shard_map/all_to_all | solution.py:350
  169.4 0.8 shard_map.179
  170.2 16.8 %all-to-all-start.6 = ((bf16[32,16,128]{2,1,0:T(8,128)(2,1)}), bf16[32,16,128]{2,1,0:T(8,128)(2,1)S(1)}, u32[]{:S(2)}, u32[]{:S(2)}) async-start(bf16[32,16,128]{2,1,0:T(8,128)(2,1)} %bitcast.6), calls=%async_computation.6 | async-start | bytes 262144 | tf_op jit(solution)/shard_map/all_to_all | solution.py:350
  187.0 0.1 copy.24.weights
  187.1 15.7 %all-to-all-done.6 = bf16[32,16,128]{2,1,0:T(8,128)(2,1)S(1)} async-done(((bf16[32,16,128]{2,1,0:T(8,128)(2,1)}), bf16[32,16,128]{2,1,0:T(8,128)(2,1)S(1)}, u32[]{:S(2)}, u32[]{:S(2)}) %all-to-all-start.6) | async-done | bytes 131104 | tf_op jit(solution)/shard_map/all_to_all | solution.py:350
  202.8 0.6 shard_map.180
  203.5 0.6 copy.29
  (29 shorter events, 0.1 us)
Async XLA Ops:
  30.9 7.0 %copy-start.11 = (bf16[512,64]{0,1:T(8,128)(2,1)S(1)}, bf16[512,64]{0,1:T(8,128)(2,1)}, u32[]{:S(2)}) copy-start(bf16[512,64]{0,1:T(8,128)(2,1)} %param.24) | copy-start | bytes 196612
  30.9 7.1 %copy-start.12 = (bf16[512,64]{0,1:T(8,128)(2,1)S(1)}, bf16[512,64]{0,1:T(8,128)(2,1)}, u32[]{:S(2)}) copy-start(bf16[512,64]{0,1:T(8,128)(2,1)} %param.25) | copy-start | bytes 196612
  30.9 7.2 %copy-start.13 = (bf16[128,192]{0,1:T(8,128)(2,1)S(1)}, bf16[128,192]{0,1:T(8,128)(2,1)}, u32[]{:S(2)}) copy-start(bf16[128,192]{0,1:T(8,128)(2,1)} %param.18) | copy-start | bytes 147460
  31.0 7.3 %copy-start.2 = (f32[160,128]{1,0:T(8,128)S(1)}, f32[160,128]{1,0:T(8,128)}, u32[]{:S(2)}) copy-start(f32[160,128]{1,0:T(8,128)} %constant.52.clone.table_in.table) | copy-start | bytes 245764
  31.0 7.3 %copy-start.4 = (bf16[512,128]{1,0:T(8,128)(2,1)S(1)}, bf16[512,128]{1,0:T(8,128)(2,1)}, u32[]{:S(2)}) copy-start(bf16[512,128]{1,0:T(8,128)(2,1)} %ku_maj.1) | copy-start | bytes 393220
  31.0 7.3 %copy-start.5 = (bf16[512,128]{1,0:T(8,128)(2,1)S(1)}, bf16[512,128]{1,0:T(8,128)(2,1)}, u32[]{:S(2)}) copy-start(bf16[512,128]{1,0:T(8,128)(2,1)} %vu_maj.1) | copy-start | bytes 393220
  31.0 7.3 %copy-start.8 = (bf16[128,128]{1,0:T(8,128)(2,1)S(1)}, bf16[128,128]{1,0:T(8,128)(2,1)}, u32[]{:S(2)}) copy-start(bf16[128,128]{1,0:T(8,128)(2,1)} %low.1) | copy-start | bytes 98308
  31.0 34.6 %all-to-all-start.1 = ((bf16[16,576,128]{2,1,0:T(8,128)(2,1)}), bf16[16,576,128]{2,1,0:T(8,128)(2,1)S(1)}, u32[]{:S(2)}, u32[]{:S(2)}) async-start(bf16[16,576,128]{2,1,0:T(8,128)(2,1)} %broadcast_in_dim.33), calls=%async_computation.1 | async-start | bytes 4718592 | tf_op jit(solution)/shard_map/all_to_all | solution.py:350
  38.9 0.8 copy-start.1
  39.7 26.0 %copy-start.6 = (bf16[128,320]{1,0:T(8,128)(2,1)}, bf16[128,320]{1,0:T(8,128)(2,1)S(1)}, u32[]{:S(2)}) copy-start(bf16[128,320]{1,0:T(8,128)(2,1)S(1)} %get-tuple-element.13.q_own_in) | copy-start | bytes 245764
  39.7 40.6 %copy-start = (bf16[128,2048]{1,0:T(8,128)(2,1)S(1)}, bf16[128,2048]{1,0:T(8,128)(2,1)}, u32[]{:S(2)}) copy-start(bf16[128,2048]{1,0:T(8,128)(2,1)} %out_maj.1) | copy-start | bytes 1572868
  39.7 40.7 %copy-start.3 = (bf16[64,2048]{1,0:T(8,128)(2,1)S(1)}, bf16[64,2048]{1,0:T(8,128)(2,1)}, u32[]{:S(2)}) copy-start(bf16[64,2048]{1,0:T(8,128)(2,1)} %out_min.1) | copy-start | bytes 786436
  39.7 7.6 %collective-permute-start = (bf16[128,320]{1,0:T(8,128)(2,1)S(1)}, bf16[128,320]{1,0:T(8,128)(2,1)S(1)}, u32[]{:S(2)}, u32[]{:S(2)}) collective-permute-start(bf16[128,320]{1,0:T(8,128)(2,1)S(1)} %get-tuple-element.13.q_own_in), channel_id=1, source_target_pairs={{0,16},{16,0},{32,48},{48,32},{64,80},{80,64},{96,112},{112,96},{1... | collective-permute-start | bytes 245768 | tf_op jit(solution)/shard_map/ppermute | solution.py:414
  47.2 18.4 %copy-start.10 = (bf16[128,320]{1,0:T(8,128)(2,1)}, bf16[128,320]{1,0:T(8,128)(2,1)S(1)}, u32[]{:S(2)}) copy-start(bf16[128,320]{1,0:T(8,128)(2,1)S(1)} %collective-permute-done.q_other_in) | copy-start | bytes 245764
  70.4 14.9 %copy-start.14 = (s32[128,2]{0,1:T(2,128)S(1)}, s32[128,2]{0,1:T(2,128)}, u32[]{:S(2)}) copy-start(s32[128,2]{0,1:T(2,128)} %param.30) | copy-start | bytes 3076
  70.4 25.8 %copy-start.7 = (bf16[128,128]{1,0:T(8,128)(2,1)S(1)}, bf16[128,128]{1,0:T(8,128)(2,1)}, u32[]{:S(2)}) copy-start(bf16[128,128]{1,0:T(8,128)(2,1)} %residual.1) | copy-start | bytes 98308
  70.4 9.9 %collective-permute-start.1 = (f32[128,256]{1,0:T(8,128)S(1)}, f32[128,256]{1,0:T(8,128)S(1)}, u32[]{:S(2)}, u32[]{:S(2)}) collective-permute-start(f32[128,256]{1,0:T(8,128)S(1)} %get-tuple-element.16), channel_id=1, source_target_pairs={{0,16},{16,0},{32,48},{48,32},{64,80},{80,64},{96,112},{112,96},{1... | collective-permute-start | bytes 393224 | tf_op jit(solution)/shard_map/ppermute | solution.py:431
  81.7 14.5 %all-to-all-start.2 = ((bf16[16,128,128]{2,1,0:T(8,128)(2,1)}), bf16[16,128,128]{2,1,0:T(8,128)(2,1)S(1)}, u32[]{:S(2)}, u32[]{:S(2)}) async-start(bf16[16,128,128]{2,1,0:T(8,128)(2,1)} %shard_map.175), calls=%async_computation.2 | async-start | bytes 1048576 | tf_op jit(solution)/shard_map/all_to_all | solution.py:350
  97.5 27.4 %all-to-all-start.3 = ((bf16[32,16,128]{2,1,0:T(8,128)(2,1)}), bf16[32,16,128]{2,1,0:T(8,128)(2,1)S(1)}, u32[]{:S(2)}, u32[]{:S(2)}) async-start(bf16[32,16,128]{2,1,0:T(8,128)(2,1)} %bitcast.2), calls=%async_computation.3 | async-start | bytes 262144 | tf_op jit(solution)/shard_map/all_to_all | solution.py:350
  112.3 23.9 %collective-permute-start.2 = (bf16[6144,128]{1,0:T(8,128)(2,1)}, bf16[6144,128]{1,0:T(8,128)(2,1)}, u32[]{:S(2)}, u32[]{:S(2)}) collective-permute-start(bf16[6144,128]{1,0:T(8,128)(2,1)} %get-tuple-element.18), channel_id=1, source_target_pairs={{0,1},{1,2},{2,3},{3,0},{4,5},{5,6},{6,7},{7,4},{8,9},{9,10},{10,1... | collective-permute-start | bytes 4718600 | tf_op jit(solution)/shard_map/ppermute | solution.py:415
  114.2 32.5 %collective-permute-start.3 = (bf16[6144,128]{1,0:T(8,128)(2,1)S(1)}, bf16[6144,128]{1,0:T(8,128)(2,1)}, u32[]{:S(2)}, u32[]{:S(2)}) collective-permute-start(bf16[6144,128]{1,0:T(8,128)(2,1)S(1)} %get-tuple-element.19), channel_id=1, source_target_pairs={{0,3},{1,0},{2,1},{3,2},{4,7},{5,4},{6,5},{7,6},{8,11},{9,8},{10,9... | collective-permute-start | bytes 4718600 | tf_op jit(solution)/shard_map/ppermute | solution.py:416
  124.9 22.6 %copy-start.9 = (f32[2048]{0:T(1024)S(1)}, f32[2048]{0:T(1024)}, u32[]{:S(2)}) copy-start(f32[2048]{0:T(1024)} %param.29) | copy-start | bytes 24580
  126.1 21.4 %all-to-all-start.4 = ((bf16[16,256,128]{2,1,0:T(8,128)(2,1)}), bf16[16,256,128]{2,1,0:T(8,128)(2,1)S(1)}, u32[]{:S(2)}, u32[]{:S(2)}) async-start(bf16[16,256,128]{2,1,0:T(8,128)(2,1)} %broadcast_select_fusion), calls=%async_computation.4 | async-start | bytes 2097152 | tf_op jit(solution)/shard_map/all_to_all | solution.py:350
  151.7 35.3 %copy-start.15 = (f32[128,2]{0,1:T(2,128)S(1)}, f32[128,2]{0,1:T(2,128)}, u32[]{:S(2)}) copy-start(f32[128,2]{0,1:T(2,128)} %param.31) | copy-start | bytes 3076
  170.2 32.7 %all-to-all-start.6 = ((bf16[32,16,128]{2,1,0:T(8,128)(2,1)}), bf16[32,16,128]{2,1,0:T(8,128)(2,1)S(1)}, u32[]{:S(2)}, u32[]{:S(2)}) async-start(bf16[32,16,128]{2,1,0:T(8,128)(2,1)} %bitcast.6), calls=%async_computation.6 | async-start | bytes 262144 | tf_op jit(solution)/shard_map/all_to_all | solution.py:350

commit v4 on v3

--- a/solution.py
+++ b/solution.py
@@ -25,6 +25,14 @@
 MASKED = -1e30
 NORM_EPS = 1e-6
 HALF = SLOTS // 2
+NEAR = (-2, -1, 0, 1)
+FAR = N_Z - len(NEAR)
+FAR_ROWS = FAR * ROWS
+PACKED = 4 * FAR_ROWS + FAR_ROWS // 2
+
+
+def along_z(step):
+    return [(z * 2 + c, (z + step) % N_Z * 2 + c) for z in range(N_Z) for c in range(2)]
 
 
 def turns(positions):
@@ -51,6 +59,14 @@
 
 
 HALF = SLOTS // 2
+NEAR = (-2, -1, 0, 1)
+FAR = N_Z - len(NEAR)
+FAR_ROWS = FAR * ROWS
+PACKED = 4 * FAR_ROWS + FAR_ROWS // 2
+
+
+def along_z(step):
+    return [(z * 2 + c, (z + step) % N_Z * 2 + c) for z in range(N_Z) for c in range(2)]
 
 
 def turns(positions):
@@ -113,9 +129,11 @@
         out[z] = row
 
 
-def queries_body(maj, low, table, after, ku_maj, vu_maj, ku_min, vu_min, out, weights):
+def queries_body(maj, low, table, after, ku_maj, vu_maj, ku_min, vu_min, lat, rope, out, weights, block):
     weights[...] = jnp.concatenate([ku_maj[...], vu_maj[...], ku_min[...], vu_min[...]], axis=1)
     c, s = turn_at(table, lax.axis_index("sp"), table[2 * N_Z :, :])
+    key = turned(rope[...].astype(F32).T, c, s)
+    block[...] = jnp.concatenate([lat[...], key, jnp.zeros((TOK, 64), BF16)], axis=1)
     out[...] = jnp.concatenate(
         [
             maj[:, :NOPE_MAJOR],
@@ -127,69 +145,99 @@
     )
 
 
-CHUNK = 512
-N_CHUNK = KEYS // CHUNK
-
-
-def attend_body(
-    keys, q_own_in, q_other_in, up_in, own, other, s_maj, s_min, v_all, q_all, up_weights, sems
-):
+def choose_body(got, out, flat):
+    z = lax.axis_index("sp") // 2
+    for o in range(FAR):
+        flat[ROWS * o : ROWS * (o + 1), :] = got[(z + NEAR[-1] + 1 + o) % N_Z]
+    for k in range(4):
+        out[FAR_ROWS * k : FAR_ROWS * (k + 1), :] = flat[:, 128 * k : 128 * (k + 1)]
+    rope = flat[:, 512:576]
+    out[4 * FAR_ROWS :, :] = jnp.concatenate([rope[: FAR_ROWS // 2], rope[FAR_ROWS // 2 :]], axis=1)
+
+
+PER = 4
+CHUNK = PER * FAR_ROWS
+N_CHUNK = N_TP // PER
+
+
+def attend_body(keys, q_own_in, q_other_in, up_in, *refs):
+    near_in = refs[: len(NEAR)]
+    own, other, s_maj, s_min, v_all, q_all, up_weights, near, sems = refs[len(NEAR) :]
     copies = fetch(
-        ((up_in, up_weights), (q_own_in, q_all.at[pl.ds(0, TOK)]), (q_other_in, q_all.at[pl.ds(TOK, TOK)])),
+        (
+            (up_in, up_weights),
+            (q_own_in, q_all.at[pl.ds(0, TOK)]),
+            (q_other_in, q_all.at[pl.ds(TOK, TOK)]),
+        )
+        + tuple((b, near.at[pl.ds(TOK * i, TOK)]) for i, b in enumerate(near_in)),
         sems,
     )
-    per = CHUNK // 128
-    copies[0].wait()
-    weights = up_weights[...]
     me = lax.axis_index("sp")
-    core = me % 2
+    core, z = me % 2, me // 2
     row = lax.broadcasted_iota(jnp.int32, (2 * TOK, 1), 0)
     q_pos = jnp.where(row < TOK, me * TOK + row, (me + 1 - 2 * core) * TOK + row - TOK)
     scale_maj = (NOPE_MAJOR + ROPE) ** -0.5
     scale_min = (NOPE_MINOR + ROPE) ** -0.5
-    top_maj = jnp.full((2 * TOK, 128), MASKED, F32)
-    top_min = jnp.full((2 * TOK, 128), MASKED, F32)
+    tops = [jnp.full((2 * TOK, 128), MASKED, F32)] * 2
+    for c in copies:
+        c.wait()
+    weights = up_weights[...]
+    q_maj, q_min = q_all[:, :192], q_all[:, 192:320]
+
+    def scored(at, width, lat, rope, k_pos, tops):
+        up = dot(lat, weights).astype(BF16)
+        k_maj = jnp.concatenate([up[:, :128], rope], axis=1)
+        k_min = jnp.concatenate([up[:, 256:320], rope], axis=1)
+        v_all[at : at + width, :] = jnp.concatenate([up[:, 128:256], up[:, 320:384]], axis=1)
+        seen = k_pos <= q_pos
+        found = []
+        for q, k, scale, store, top in (
+            (q_maj, k_maj, scale_maj, s_maj, tops[0]),
+            (q_min, k_min, scale_min, s_min, tops[1]),
+        ):
+            s = jnp.where(seen, dot(q, k, ((1,), (1,))) * scale, MASKED)
+            store[:, at : at + width] = s
+            for i in range(width // 128):
+                top = jnp.maximum(top, s[:, 128 * i : 128 * (i + 1)])
+            found.append(top)
+        return found
+
+    col = lax.broadcasted_iota(jnp.int32, (1, len(NEAR) * TOK), 1)
+    k_pos = (2 * ((z + NEAR[0] + N_Z + col // TOK) % N_Z) + core) * TOK + col % TOK
+    tops = scored(0, len(NEAR) * TOK, near[:, :512], near[:, 512:576], k_pos, tops)
+    first = len(NEAR) * TOK
+    col = lax.broadcasted_iota(jnp.int32, (1, CHUNK), 1)
     for n in range(N_CHUNK):
         lat_rows, rope_rows = [], []
-        for t in range(n * per, (n + 1) * per):
+        for t in range(n * PER, (n + 1) * PER):
             lat_rows.append(
-                jnp.concatenate([keys[t, 128 * k : 128 * (k + 1), :] for k in range(4)], axis=1)
+                jnp.concatenate(
+                    [keys[t, FAR_ROWS * k : FAR_ROWS * (k + 1), :] for k in range(4)], axis=1
+                )
             )
-            half = keys[t, 512:576, :]
+            half = keys[t, 4 * FAR_ROWS :, :]
             rope_rows.append(jnp.concatenate([half[:, :64], half[:, 64:]], axis=0))
         lat = jnp.concatenate(lat_rows, axis=0)
         rope = jnp.concatenate(rope_rows, axis=0)
-        up = dot(lat, weights).astype(BF16)
-        if n == 0:
-            copies[1].wait()
-            copies[2].wait()
-            q_maj, q_min = q_all[:, :192], q_all[:, 192:320]
-        k_maj = jnp.concatenate([up[:, :128], rope], axis=1)
-        k_min = jnp.concatenate([up[:, 256:320], rope], axis=1)
-        v_all[CHUNK * n : CHUNK * (n + 1), :] = jnp.concatenate([up[:, 128:256], up[:, 320:384]], axis=1)
-        col = lax.broadcasted_iota(jnp.int32, (1, CHUNK), 1) + CHUNK * n
-        k_pos = (2 * ((col >> 3) & 15) + core) * TOK + 8 * (col >> 7) + (col & 7)
-        seen = k_pos <= q_pos
-        a = jnp.where(seen, dot(q_maj, k_maj, ((1,), (1,))) * scale_maj, MASKED)
-        b = jnp.where(seen, dot(q_min, k_min, ((1,), (1,))) * scale_min, MASKED)
-        s_maj[:, CHUNK * n : CHUNK * (n + 1)] = a
-        s_min[:, CHUNK * n : CHUNK * (n + 1)] = b
-        for k in range(CHUNK // 128):
-            top_maj = jnp.maximum(top_maj, a[:, 128 * k : 128 * (k + 1)])
-            top_min = jnp.maximum(top_min, b[:, 128 * k : 128 * (k + 1)])
+        inner = col % FAR_ROWS
+        k_z = (z + NEAR[-1] + 1 + inner // ROWS) % N_Z
+        k_pos = (2 * k_z + core) * TOK + ROWS * (n * PER + col // FAR_ROWS) + inner % ROWS
+        tops = scored(first + CHUNK * n, CHUNK, lat, rope, k_pos, tops)
+    top_maj, top_min = tops
     m_maj = jnp.max(top_maj, axis=1, keepdims=True)
     m_min = jnp.max(top_min, axis=1, keepdims=True)
     sum_maj = jnp.zeros((2 * TOK, 128), F32)
     sum_min = jnp.zeros((2 * TOK, 128), F32)
     o_maj = jnp.zeros((2 * TOK, 128), F32)
     o_min = jnp.zeros((2 * TOK, 64), F32)
-    for n in range(N_CHUNK):
-        p = jnp.exp(s_maj[:, CHUNK * n : CHUNK * (n + 1)] - m_maj)
-        r = jnp.exp(s_min[:, CHUNK * n : CHUNK * (n + 1)] - m_min)
-        for k in range(CHUNK // 128):
+    step = 512
+    for at in range(0, KEYS, step):
+        p = jnp.exp(s_maj[:, at : at + step] - m_maj)
+        r = jnp.exp(s_min[:, at : at + step] - m_min)
+        for k in range(step // 128):
             sum_maj = sum_maj + p[:, 128 * k : 128 * (k + 1)]
             sum_min = sum_min + r[:, 128 * k : 128 * (k + 1)]
-        v = v_all[CHUNK * n : CHUNK * (n + 1), :]
+        v = v_all[at : at + step, :]
         o_maj = o_maj + dot(p.astype(BF16), v[:, :128])
         o_min = o_min + dot(r.astype(BF16), v[:, 128:192])
     l_maj = jnp.sum(sum_maj, axis=1, keepdims=True)
@@ -385,18 +433,14 @@
         4 + 2 * N_TP,
         (gate_proj, up_proj, down_proj),
     )
-    flat = got_rows.reshape(N_Z * ROWS, 640)
-    rope = flat[:, 512:576]
-    packed = jnp.concatenate(
-        [flat[:, 128 * k : 128 * (k + 1)] for k in range(4)]
-        + [jnp.concatenate([rope[:64], rope[64:]], axis=1)],
-        axis=0,
-    )
-    spread = jnp.broadcast_to(packed, (N_TP, 576, 128))
+    packed = kernel(
+        choose_body, shape((PACKED, 128)), [room((FAR_ROWS, 640))], 0, (got_rows,), (0,)
+    )
+    spread = jnp.broadcast_to(packed, (N_TP, PACKED, 128))
     keys = to_each(spread, "tp")
-    q_own, up_weights = kernel(
+    q_own, up_weights, own_block = kernel(
         queries_body,
-        (shape((TOK, 320)), shape((LATENT, 384))),
+        (shape((TOK, 320)), shape((LATENT, 384)), shape((TOK, 640))),
         [],
         0,
         (
@@ -408,10 +452,13 @@
             value_up_major,
             key_up_minor,
             value_up_minor,
+            latent_rows,
+            rope_keys.T,
         ),
-        range(8),
+        range(10),
     )
     q_other = lax.ppermute(q_own, "sp", OTHER_CORE)
+    blocks = [lax.ppermute(own_block, "sp", along_z(-step)) if step else own_block for step in NEAR]
     from_low = lax.ppermute(low, ("sp", "tp"), ring(1))
     from_high = lax.ppermute(high, ("sp", "tp"), ring(-1))
     own, other = kernel(
@@ -423,9 +470,10 @@
             room((KEYS, 192)),
             room((2 * TOK, 320)),
             room((LATENT, 384)),
+            room((len(NEAR) * TOK, 640)),
         ],
-        3,
-        (keys, q_own, q_other, up_weights),
+        3 + len(NEAR),
+        (keys, q_own, q_other, up_weights, *blocks),
         (0,),
     )
     from_other = lax.ppermute(other, "sp", OTHER_CORE)
@@ -468,7 +516,12 @@
     expert_out = kernel(gather_sum_body, shape((SLOTS, 128)), [], 0, (down_parts,), (0,))
     returned = to_each(expert_out.reshape(EXPERTS, CAP, 128), "sp").reshape(SLOTS, 128)
     return kernel(
-        mix_body, shape((TOK, 128)), [], 0, (returned, stream, expert_ids, expert_weights), range(4)
+        mix_body,
+        jax.ShapeDtypeStruct((TOK, 128), BF16),
+        [],
+        0,
+        (returned, stream, expert_ids, expert_weights),
+        range(4),
     )
 
 

time: 205 us -> 196 us (0.956)
  waiting for transfers between devices: 70.7 us -> 52.3 us
  starting transfers between devices: 64.6 us -> 73.3 us
    all_to_all x5, waiting for transfers between devices: 51.8 us -> 33.5 us  [to_each(): lax.all_to_all(array, axis, 0, 0, tiled=True, axis_index_groups=groups)]
    ppermute x0 -> x3, starting transfers between devices: none -> 11.6 us  [per_device(): lax.ppermute(own_block, 'sp', along_z(-step))]
    pallas_call x9 -> x10, Pallas kernels: 17.9 us -> 19.3 us  [kernel(): pl.pallas_call(body, out_shape=outs, in_specs=[pl.BlockSpec(memory_space=...]
  transfers between devices with their start and end apart: 9 -> 12, of which waited for: 9 -> 8; matrix products, arithmetic and copies ran while one was open for 1% -> 1% of each run, Pallas kernels for 2% -> 2%
where the time goes in v4:
time: 196 us; the launch traced here: 195 us
  starting transfers between devices  73.3 us (37%)
  waiting for transfers between devices  52.3 us (27%)
  blocking collectives  45.4 us (23%)
  Pallas kernels  19.3 us (10%)
  local copies, waits for them, and re-layouts  3.63 us (2%)
    all_to_all x2, blocking collectives, to_each(): lax.all_to_all(array, axis, 0, 0, tiled=True, axis_index_groups=groups)  45.4 us
    all_to_all x5, starting transfers between devices, to_each(): lax.all_to_all(array, axis, 0, 0, tiled=True, axis_index_groups=groups)  40.9 us
    all_to_all x5, waiting for transfers between devices, to_each(): lax.all_to_all(array, axis, 0, 0, tiled=True, axis_index_groups=groups)  33.5 us
    pallas_call x10, Pallas kernels, kernel(): pl.pallas_call(body, out_shape=outs, in_specs=[pl.BlockSpec(memory_space=...  19.3 us
    ppermute x3, starting transfers between devices, per_device(): lax.ppermute(own_block, 'sp', along_z(-step))  11.6 us
    ppermute x1, waiting for transfers between devices, per_device(): from_high = lax.ppermute(high, ('sp', 'tp'), ring(-1))  10.5 us
    ppermute x1, starting transfers between devices, per_device(): from_other = lax.ppermute(other, 'sp', OTHER_CORE)  8.06 us
    ppermute x1, waiting for transfers between devices, per_device(): from_low = lax.ppermute(low, ('sp', 'tp'), ring(1))  6.47 us
  transfers between devices with their start and end apart: 12, of which 8 were waited for; matrix products, arithmetic and copies ran while one was open for 1% of the time, Pallas kernels for 2%

profile of v4, /device:TPU:1, one launch (start us, length us, event | category | flops | bytes accessed | tf_op | source)
XLA Modules:
  0.0 195.4 jit_solution(15644038465651182201)
XLA Ops:
  0.0 1.2 shard_map.172
  1.2 27.7 %all_to_all.35.got = bf16[16,8,640]{2,1,0:T(8,128)(2,1)S(1)} all-to-all(bf16[16,8,640]{2,1,0:T(8,128)(2,1)S(1)} %shard_map.172), channel_id=1, replica_groups={{0,32,64,96,128,160,192,224,256,288,320,352,384,416,448,480},{16,48,80,..., dimensions={0} | all-to-all | bytes 327680 | tf_op jit(solution)/shard_map/all_to_all | solution.py:398
  28.9 0.1 shard_map.173.after
  29.0 1.5 broadcast_in_dim.33
  30.5 0.0 copy-start.3
  30.5 0.0 copy-start.7
  30.5 0.0 copy-start.9
  30.5 6.9 %all-to-all-start.1 = ((bf16[16,432,128]{2,1,0:T(8,128)(2,1)}), bf16[16,432,128]{2,1,0:T(8,128)(2,1)S(1)}, u32[]{:S(2)}, u32[]{:S(2)}) async-start(bf16[16,432,128]{2,1,0:T(8,128)(2,1)} %broadcast_in_dim.33), calls=%async_computation.1 | async-start | bytes 3538944 | tf_op jit(solution)/shard_map/all_to_all | solution.py:398
  37.5 0.1 copy.20.ku_min
  37.6 0.1 copy.21.vu_min
  37.7 0.1 copy.19.maj
  37.9 0.8 shard_map.174
  38.7 0.7 copy-done.2
  39.4 5.1 %collective-permute-start.1 = (bf16[128,640]{1,0:T(8,128)(2,1)S(1)}, bf16[128,640]{1,0:T(8,128)(2,1)S(1)}, u32[]{:S(2)}, u32[]{:S(2)}) collective-permute-start(bf16[128,640]{1,0:T(8,128)(2,1)S(1)} %get-tuple-element.16.refs_2_), channel_id=1, source_target_pairs={{0,64},{16,80},{32,96},{48,112},{64,128},{80,144},{96,160},{112,17... | collective-permute-start | bytes 491528 | tf_op jit(solution)/shard_map/ppermute | solution.py:461
  44.5 3.9 %collective-permute-start.2 = (bf16[128,640]{1,0:T(8,128)(2,1)S(1)}, bf16[128,640]{1,0:T(8,128)(2,1)S(1)}, u32[]{:S(2)}, u32[]{:S(2)}) collective-permute-start(bf16[128,640]{1,0:T(8,128)(2,1)S(1)} %get-tuple-element.16.refs_2_), channel_id=1, source_target_pairs={{0,32},{16,48},{32,64},{48,80},{64,96},{80,112},{96,128},{112,144}... | collective-permute-start | bytes 491528 | tf_op jit(solution)/shard_map/ppermute | solution.py:461
  48.5 2.6 %collective-permute-start.3 = (bf16[128,640]{1,0:T(8,128)(2,1)S(1)}, bf16[128,640]{1,0:T(8,128)(2,1)S(1)}, u32[]{:S(2)}, u32[]{:S(2)}) collective-permute-start(bf16[128,640]{1,0:T(8,128)(2,1)S(1)} %get-tuple-element.16.refs_2_), channel_id=1, source_target_pairs={{0,480},{16,496},{32,0},{48,16},{64,32},{80,48},{96,64},{112,80},{... | collective-permute-start | bytes 491528 | tf_op jit(solution)/shard_map/ppermute | solution.py:461
  51.1 6.2 %collective-permute-start = (bf16[128,320]{1,0:T(8,128)(2,1)S(1)}, bf16[128,320]{1,0:T(8,128)(2,1)S(1)}, u32[]{:S(2)}, u32[]{:S(2)}) collective-permute-start(bf16[128,320]{1,0:T(8,128)(2,1)S(1)} %get-tuple-element.14.q_own_in), channel_id=1, source_target_pairs={{0,16},{16,0},{32,48},{48,32},{64,80},{80,64},{96,112},{112,96},{1... | collective-permute-start | bytes 245768 | tf_op jit(solution)/shard_map/ppermute | solution.py:460
  57.3 0.9 collective-permute-done.q_other_in
  58.2 0.0 all-to-all-done.1.keys
  58.3 0.5 copy-done.16
  58.8 0.1 copy-done.13
  58.9 0.1 copy-done.14
  59.0 0.1 copy-done.15
  59.0 5.2 %shard_map.175 = (f32[128,256]{1,0:T(8,128)S(1)}, f32[128,256]{1,0:T(8,128)S(1)}) custom-call(bf16[16,432,128]{2,1,0:T(8,128)(2,1)S(1)} %all-to-all-done.1.keys, bf16[128,320]{1,0:T(8,128)(2,1)} %copy-done.8, bf16[128,320]{1,0:T(8,128)(2,1)} %copy-done.16, bf16[512,384]{1,0:T(8,128)(2,1)} %copy-done.2, bf16[128,640]{1,0:T(8,128)(2,1)} %copy-done.13, ...), custom_call_target="tpu_custom_call" | custom-call | tf_op jit(solution)/shard_map/pallas_call | solution.py:387
  64.3 8.1 %collective-permute-start.4 = (f32[128,256]{1,0:T(8,128)S(1)}, f32[128,256]{1,0:T(8,128)S(1)}, u32[]{:S(2)}, u32[]{:S(2)}) collective-permute-start(f32[128,256]{1,0:T(8,128)S(1)} %get-tuple-element.18), channel_id=1, source_target_pairs={{0,16},{16,0},{32,48},{48,32},{64,80},{80,64},{96,112},{112,96},{1... | collective-permute-start | bytes 393224 | tf_op jit(solution)/shard_map/ppermute | solution.py:479
  72.3 1.0 collective-permute-done.4.b
  73.3 1.4 shard_map.176
  74.7 3.6 %all-to-all-start.2 = ((bf16[16,128,128]{2,1,0:T(8,128)(2,1)}), bf16[16,128,128]{2,1,0:T(8,128)(2,1)S(1)}, u32[]{:S(2)}, u32[]{:S(2)}) async-start(bf16[16,128,128]{2,1,0:T(8,128)(2,1)} %shard_map.176), calls=%async_computation.2 | async-start | bytes 1048576 | tf_op jit(solution)/shard_map/all_to_all | solution.py:398
  78.2 0.1 copy.22.ids
  78.4 10.8 %all-to-all-done.2.parts = bf16[16,128,128]{2,1,0:T(8,128)(2,1)S(1)} async-done(((bf16[16,128,128]{2,1,0:T(8,128)(2,1)}), bf16[16,128,128]{2,1,0:T(8,128)(2,1)S(1)}, u32[]{:S(2)}, u32[]{:S(2)}) %all-to-all-start.2) | async-done | bytes 524320 | tf_op jit(solution)/shard_map/all_to_all | solution.py:398
  89.2 1.3 shard_map.177
  90.5 10.0 %all-to-all-start.3 = ((bf16[32,16,128]{2,1,0:T(8,128)(2,1)}), bf16[32,16,128]{2,1,0:T(8,128)(2,1)S(1)}, u32[]{:S(2)}, u32[]{:S(2)}) async-start(bf16[32,16,128]{2,1,0:T(8,128)(2,1)} %bitcast.1), calls=%async_computation.3 | async-start | bytes 262144 | tf_op jit(solution)/shard_map/all_to_all | solution.py:398
  100.5 3.2 %shard_map.178 = (bf16[6144,128]{1,0:T(8,128)(2,1)}, bf16[6144,128]{1,0:T(8,128)(2,1)S(1)}) custom-call(bf16[1,2048,256]{2,1,0:T(8,128)(2,1)} %gate_a.1, bf16[1,2048,256]{2,1,0:T(8,128)(2,1)} %up_a.1, bf16[1,256,2048]{2,1,0:T(8,128)(2,1)} %down_a.1), custom_call_target="tpu_custom_call" | custom-call | tf_op jit(solution)/shard_map/pallas_call | solution.py:387
  103.7 1.9 collective-permute-start.5
  105.6 4.6 %collective-permute-start.6 = (bf16[6144,128]{1,0:T(8,128)(2,1)S(1)}, bf16[6144,128]{1,0:T(8,128)(2,1)}, u32[]{:S(2)}, u32[]{:S(2)}) collective-permute-start(bf16[6144,128]{1,0:T(8,128)(2,1)S(1)} %get-tuple-element.21), channel_id=1, source_target_pairs={{0,3},{1,0},{2,1},{3,2},{4,7},{5,4},{6,5},{7,6},{8,11},{9,8},{10,9... | collective-permute-start | bytes 4718600 | tf_op jit(solution)/shard_map/ppermute | solution.py:463
  110.2 6.1 %all-to-all-done.3 = bf16[32,16,128]{2,1,0:T(8,128)(2,1)S(1)} async-done(((bf16[32,16,128]{2,1,0:T(8,128)(2,1)}), bf16[32,16,128]{2,1,0:T(8,128)(2,1)S(1)}, u32[]{:S(2)}, u32[]{:S(2)}) %all-to-all-start.3) | async-done | bytes 131104 | tf_op jit(solution)/shard_map/all_to_all | solution.py:398
  116.3 1.1 broadcast_select_fusion
  117.5 3.7 %all-to-all-start.4 = ((bf16[16,256,128]{2,1,0:T(8,128)(2,1)}), bf16[16,256,128]{2,1,0:T(8,128)(2,1)S(1)}, u32[]{:S(2)}, u32[]{:S(2)}) async-start(bf16[16,256,128]{2,1,0:T(8,128)(2,1)} %broadcast_select_fusion), calls=%async_computation.4 | async-start | bytes 2097152 | tf_op jit(solution)/shard_map/all_to_all | solution.py:398
  121.1 6.5 %collective-permute-done.5.low = bf16[6144,128]{1,0:T(8,128)(2,1)} collective-permute-done((bf16[6144,128]{1,0:T(8,128)(2,1)}, bf16[6144,128]{1,0:T(8,128)(2,1)}, u32[]{:S(2)}, u32[]{:S(2)}) %collective-permute-start.5) | collective-permute-done | bytes 1572896 | tf_op jit(solution)/shard_map/ppermute | solution.py:462
  127.6 10.5 %collective-permute-done.6.high = bf16[6144,128]{1,0:T(8,128)(2,1)} collective-permute-done((bf16[6144,128]{1,0:T(8,128)(2,1)S(1)}, bf16[6144,128]{1,0:T(8,128)(2,1)}, u32[]{:S(2)}, u32[]{:S(2)}) %collective-permute-start.6) | collective-permute-done | bytes 1572896 | tf_op jit(solution)/shard_map/ppermute | solution.py:463
  138.1 0.8 all-to-all-done.4.got
  138.9 4.1 %shard_map.179 = bf16[16,256,128]{2,1,0:T(8,128)(2,1)S(1)} custom-call(bf16[16,256,128]{2,1,0:T(8,128)(2,1)S(1)} %all-to-all-done.4.got, f32[1,2048]{1,0:T(1,128)S(1)} %bitcast.10, bf16[1,2048,256]{2,1,0:T(8,128)(2,1)} %gate_a.1, bf16[1,2048,256]{2,1,0:T(8,128)(2,1)} %up_a.1, bf16[1,256,2048]{2,1,0:T(8,128)(2,1)} %down_a.1, ...), custom_call_target="tpu_custom_call" | custom-call | tf_op jit(solution)/shard_map/pallas_call | solution.py:387
  143.0 17.7 %all_to_all.36.parts = bf16[16,256,128]{2,1,0:T(8,128)(2,1)S(1)} all-to-all(bf16[16,256,128]{2,1,0:T(8,128)(2,1)S(1)} %shard_map.179), channel_id=1, replica_groups=mesh['sp'=32,'tp'=16] {'tp'}, dimensions={0} | all-to-all | bytes 2097152 | tf_op jit(solution)/shard_map/all_to_all | solution.py:398
  160.7 0.8 shard_map.180
  161.5 16.8 %all-to-all-start.6 = ((bf16[32,16,128]{2,1,0:T(8,128)(2,1)}), bf16[32,16,128]{2,1,0:T(8,128)(2,1)S(1)}, u32[]{:S(2)}, u32[]{:S(2)}) async-start(bf16[32,16,128]{2,1,0:T(8,128)(2,1)} %bitcast.5), calls=%async_computation.6 | async-start | bytes 262144 | tf_op jit(solution)/shard_map/all_to_all | solution.py:398
  178.4 0.1 copy.24.weights
  178.5 15.7 %all-to-all-done.6 = bf16[32,16,128]{2,1,0:T(8,128)(2,1)S(1)} async-done(((bf16[32,16,128]{2,1,0:T(8,128)(2,1)}), bf16[32,16,128]{2,1,0:T(8,128)(2,1)S(1)}, u32[]{:S(2)}, u32[]{:S(2)}) %all-to-all-start.6) | async-done | bytes 131104 | tf_op jit(solution)/shard_map/all_to_all | solution.py:398
  194.2 1.2 shard_map.181
  (41 shorter events, 0.1 us)
Async XLA Ops:
  30.5 7.0 %copy-start.17 = (bf16[512,64]{0,1:T(8,128)(2,1)S(1)}, bf16[512,64]{0,1:T(8,128)(2,1)}, u32[]{:S(2)}) copy-start(bf16[512,64]{0,1:T(8,128)(2,1)} %param.24) | copy-start | bytes 196612
  30.5 7.1 %copy-start.18 = (bf16[512,64]{0,1:T(8,128)(2,1)S(1)}, bf16[512,64]{0,1:T(8,128)(2,1)}, u32[]{:S(2)}) copy-start(bf16[512,64]{0,1:T(8,128)(2,1)} %param.25) | copy-start | bytes 196612
  30.5 7.2 %copy-start.19 = (bf16[128,192]{0,1:T(8,128)(2,1)S(1)}, bf16[128,192]{0,1:T(8,128)(2,1)}, u32[]{:S(2)}) copy-start(bf16[128,192]{0,1:T(8,128)(2,1)} %param.18) | copy-start | bytes 147460
  30.5 7.4 %copy-start.1 = (bf16[128,512]{1,0:T(8,128)(2,1)S(1)}, bf16[128,512]{1,0:T(8,128)(2,1)}, u32[]{:S(2)}) copy-start(bf16[128,512]{1,0:T(8,128)(2,1)} %lat.1) | copy-start | bytes 393220
  30.5 7.4 %copy-start.3 = (f32[160,128]{1,0:T(8,128)S(1)}, f32[160,128]{1,0:T(8,128)}, u32[]{:S(2)}) copy-start(f32[160,128]{1,0:T(8,128)} %constant.52.clone.table_in.table) | copy-start | bytes 245764
  30.5 7.4 %copy-start.6 = (bf16[512,128]{1,0:T(8,128)(2,1)S(1)}, bf16[512,128]{1,0:T(8,128)(2,1)}, u32[]{:S(2)}) copy-start(bf16[512,128]{1,0:T(8,128)(2,1)} %ku_maj.1) | copy-start | bytes 393220
  30.5 7.4 %copy-start.7 = (bf16[512,128]{1,0:T(8,128)(2,1)S(1)}, bf16[512,128]{1,0:T(8,128)(2,1)}, u32[]{:S(2)}) copy-start(bf16[512,128]{1,0:T(8,128)(2,1)} %vu_maj.1) | copy-start | bytes 393220
  30.5 7.4 %copy-start.9 = (bf16[128,64]{0,1:T(8,128)(2,1)S(1)}, bf16[128,64]{0,1:T(8,128)(2,1)}, u32[]{:S(2)}) copy-start(bf16[128,64]{0,1:T(8,128)(2,1)} %param.21) | copy-start | bytes 49156
  30.5 7.4 %copy-start.11 = (bf16[128,128]{1,0:T(8,128)(2,1)S(1)}, bf16[128,128]{1,0:T(8,128)(2,1)}, u32[]{:S(2)}) copy-start(bf16[128,128]{1,0:T(8,128)(2,1)} %low.1) | copy-start | bytes 98308
  30.5 27.7 %all-to-all-start.1 = ((bf16[16,432,128]{2,1,0:T(8,128)(2,1)}), bf16[16,432,128]{2,1,0:T(8,128)(2,1)S(1)}, u32[]{:S(2)}, u32[]{:S(2)}) async-start(bf16[16,432,128]{2,1,0:T(8,128)(2,1)} %broadcast_in_dim.33), calls=%async_computation.1 | async-start | bytes 3538944 | tf_op jit(solution)/shard_map/all_to_all | solution.py:398
  38.7 0.7 copy-start.2
  39.4 18.9 %copy-start.5 = (bf16[128,640]{1,0:T(8,128)(2,1)}, bf16[128,640]{1,0:T(8,128)(2,1)S(1)}, u32[]{:S(2)}) copy-start(bf16[128,640]{1,0:T(8,128)(2,1)S(1)} %get-tuple-element.16.refs_2_) | copy-start | bytes 491524
  39.4 18.9 %copy-start.8 = (bf16[128,320]{1,0:T(8,128)(2,1)}, bf16[128,320]{1,0:T(8,128)(2,1)S(1)}, u32[]{:S(2)}) copy-start(bf16[128,320]{1,0:T(8,128)(2,1)S(1)} %get-tuple-element.14.q_own_in) | copy-start | bytes 245764
  39.4 33.9 %copy-start = (bf16[128,2048]{1,0:T(8,128)(2,1)S(1)}, bf16[128,2048]{1,0:T(8,128)(2,1)}, u32[]{:S(2)}) copy-start(bf16[128,2048]{1,0:T(8,128)(2,1)} %out_maj.1) | copy-start | bytes 1572868
  39.4 33.9 %copy-start.4 = (bf16[64,2048]{1,0:T(8,128)(2,1)S(1)}, bf16[64,2048]{1,0:T(8,128)(2,1)}, u32[]{:S(2)}) copy-start(bf16[64,2048]{1,0:T(8,128)(2,1)} %out_min.1) | copy-start | bytes 786436
  39.4 18.8 %collective-permute-start.1 = (bf16[128,640]{1,0:T(8,128)(2,1)S(1)}, bf16[128,640]{1,0:T(8,128)(2,1)S(1)}, u32[]{:S(2)}, u32[]{:S(2)}) collective-permute-start(bf16[128,640]{1,0:T(8,128)(2,1)S(1)} %get-tuple-element.16.refs_2_), channel_id=1, source_target_pairs={{0,64},{16,80},{32,96},{48,112},{64,128},{80,144},{96,160},{112,17... | collective-permute-start | bytes 491528 | tf_op jit(solution)/shard_map/ppermute | solution.py:461
  44.5 13.7 %collective-permute-start.2 = (bf16[128,640]{1,0:T(8,128)(2,1)S(1)}, bf16[128,640]{1,0:T(8,128)(2,1)S(1)}, u32[]{:S(2)}, u32[]{:S(2)}) collective-permute-start(bf16[128,640]{1,0:T(8,128)(2,1)S(1)} %get-tuple-element.16.refs_2_), channel_id=1, source_target_pairs={{0,32},{16,48},{32,64},{48,80},{64,96},{80,112},{96,128},{112,144}... | collective-permute-start | bytes 491528 | tf_op jit(solution)/shard_map/ppermute | solution.py:461
  48.5 9.8 %collective-permute-start.3 = (bf16[128,640]{1,0:T(8,128)(2,1)S(1)}, bf16[128,640]{1,0:T(8,128)(2,1)S(1)}, u32[]{:S(2)}, u32[]{:S(2)}) collective-permute-start(bf16[128,640]{1,0:T(8,128)(2,1)S(1)} %get-tuple-element.16.refs_2_), channel_id=1, source_target_pairs={{0,480},{16,496},{32,0},{48,16},{64,32},{80,48},{96,64},{112,80},{... | collective-permute-start | bytes 491528 | tf_op jit(solution)/shard_map/ppermute | solution.py:461
  51.1 7.1 %collective-permute-start = (bf16[128,320]{1,0:T(8,128)(2,1)S(1)}, bf16[128,320]{1,0:T(8,128)(2,1)S(1)}, u32[]{:S(2)}, u32[]{:S(2)}) collective-permute-start(bf16[128,320]{1,0:T(8,128)(2,1)S(1)} %get-tuple-element.14.q_own_in), channel_id=1, source_target_pairs={{0,16},{16,0},{32,48},{48,32},{64,80},{80,64},{96,112},{112,96},{1... | collective-permute-start | bytes 245768 | tf_op jit(solution)/shard_map/ppermute | solution.py:460
  58.2 0.6 copy-start.16
  58.2 0.7 copy-start.13
  58.2 0.8 copy-start.14
  58.2 0.8 copy-start.15
  64.2 14.0 %copy-start.20 = (s32[128,2]{0,1:T(2,128)S(1)}, s32[128,2]{0,1:T(2,128)}, u32[]{:S(2)}) copy-start(s32[128,2]{0,1:T(2,128)} %param.30) | copy-start | bytes 3076
  64.3 24.9 %copy-start.10 = (bf16[128,128]{1,0:T(8,128)(2,1)S(1)}, bf16[128,128]{1,0:T(8,128)(2,1)}, u32[]{:S(2)}) copy-start(bf16[128,128]{1,0:T(8,128)(2,1)} %residual.1) | copy-start | bytes 98308
  64.3 9.0 %collective-permute-start.4 = (f32[128,256]{1,0:T(8,128)S(1)}, f32[128,256]{1,0:T(8,128)S(1)}, u32[]{:S(2)}, u32[]{:S(2)}) collective-permute-start(f32[128,256]{1,0:T(8,128)S(1)} %get-tuple-element.18), channel_id=1, source_target_pairs={{0,16},{16,0},{32,48},{48,32},{64,80},{80,64},{96,112},{112,96},{1... | collective-permute-start | bytes 393224 | tf_op jit(solution)/shard_map/ppermute | solution.py:479
  74.7 14.5 %all-to-all-start.2 = ((bf16[16,128,128]{2,1,0:T(8,128)(2,1)}), bf16[16,128,128]{2,1,0:T(8,128)(2,1)S(1)}, u32[]{:S(2)}, u32[]{:S(2)}) async-start(bf16[16,128,128]{2,1,0:T(8,128)(2,1)} %shard_map.176), calls=%async_computation.2 | async-start | bytes 1048576 | tf_op jit(solution)/shard_map/all_to_all | solution.py:398
  90.5 25.8 %all-to-all-start.3 = ((bf16[32,16,128]{2,1,0:T(8,128)(2,1)}), bf16[32,16,128]{2,1,0:T(8,128)(2,1)S(1)}, u32[]{:S(2)}, u32[]{:S(2)}) async-start(bf16[32,16,128]{2,1,0:T(8,128)(2,1)} %bitcast.1), calls=%async_computation.3 | async-start | bytes 262144 | tf_op jit(solution)/shard_map/all_to_all | solution.py:398
  103.7 23.9 %collective-permute-start.5 = (bf16[6144,128]{1,0:T(8,128)(2,1)}, bf16[6144,128]{1,0:T(8,128)(2,1)}, u32[]{:S(2)}, u32[]{:S(2)}) collective-permute-start(bf16[6144,128]{1,0:T(8,128)(2,1)} %get-tuple-element.20), channel_id=1, source_target_pairs={{0,1},{1,2},{2,3},{3,0},{4,5},{5,6},{6,7},{7,4},{8,9},{9,10},{10,1... | collective-permute-start | bytes 4718600 | tf_op jit(solution)/shard_map/ppermute | solution.py:462
  105.6 32.5 %collective-permute-start.6 = (bf16[6144,128]{1,0:T(8,128)(2,1)S(1)}, bf16[6144,128]{1,0:T(8,128)(2,1)}, u32[]{:S(2)}, u32[]{:S(2)}) collective-permute-start(bf16[6144,128]{1,0:T(8,128)(2,1)S(1)} %get-tuple-element.21), channel_id=1, source_target_pairs={{0,3},{1,0},{2,1},{3,2},{4,7},{5,4},{6,5},{7,6},{8,11},{9,8},{10,9... | collective-permute-start | bytes 4718600 | tf_op jit(solution)/shard_map/ppermute | solution.py:463
  116.3 22.6 %copy-start.12 = (f32[2048]{0:T(1024)S(1)}, f32[2048]{0:T(1024)}, u32[]{:S(2)}) copy-start(f32[2048]{0:T(1024)} %param.29) | copy-start | bytes 24580
  117.5 21.4 %all-to-all-start.4 = ((bf16[16,256,128]{2,1,0:T(8,128)(2,1)}), bf16[16,256,128]{2,1,0:T(8,128)(2,1)S(1)}, u32[]{:S(2)}, u32[]{:S(2)}) async-start(bf16[16,256,128]{2,1,0:T(8,128)(2,1)} %broadcast_select_fusion), calls=%async_computation.4 | async-start | bytes 2097152 | tf_op jit(solution)/shard_map/all_to_all | solution.py:398
  143.0 35.3 %copy-start.21 = (f32[128,2]{0,1:T(2,128)S(1)}, f32[128,2]{0,1:T(2,128)}, u32[]{:S(2)}) copy-start(f32[128,2]{0,1:T(2,128)} %param.31) | copy-start | bytes 3076
  161.5 32.7 %all-to-all-start.6 = ((bf16[32,16,128]{2,1,0:T(8,128)(2,1)}), bf16[32,16,128]{2,1,0:T(8,128)(2,1)S(1)}, u32[]{:S(2)}, u32[]{:S(2)}) async-start(bf16[32,16,128]{2,1,0:T(8,128)(2,1)} %bitcast.5), calls=%async_computation.6 | async-start | bytes 262144 | tf_op jit(solution)/shard_map/all_to_all | solution.py:398

commit v5 on v4

--- a/solution.py
+++ b/solution.py
@@ -179,7 +179,7 @@
     scale_maj = (NOPE_MAJOR + ROPE) ** -0.5
     scale_min = (NOPE_MINOR + ROPE) ** -0.5
     tops = [jnp.full((2 * TOK, 128), MASKED, F32)] * 2
-    for c in copies:
+    for c in copies[:3]:
         c.wait()
     weights = up_weights[...]
     q_maj, q_min = q_all[:, :192], q_all[:, 192:320]
@@ -202,10 +202,6 @@
             found.append(top)
         return found
 
-    col = lax.broadcasted_iota(jnp.int32, (1, len(NEAR) * TOK), 1)
-    k_pos = (2 * ((z + NEAR[0] + N_Z + col // TOK) % N_Z) + core) * TOK + col % TOK
-    tops = scored(0, len(NEAR) * TOK, near[:, :512], near[:, 512:576], k_pos, tops)
-    first = len(NEAR) * TOK
     col = lax.broadcasted_iota(jnp.int32, (1, CHUNK), 1)
     for n in range(N_CHUNK):
         lat_rows, rope_rows = [], []
@@ -222,7 +218,12 @@
         inner = col % FAR_ROWS
         k_z = (z + NEAR[-1] + 1 + inner // ROWS) % N_Z
         k_pos = (2 * k_z + core) * TOK + ROWS * (n * PER + col // FAR_ROWS) + inner % ROWS
-        tops = scored(first + CHUNK * n, CHUNK, lat, rope, k_pos, tops)
+        tops = scored(CHUNK * n, CHUNK, lat, rope, k_pos, tops)
+    for c in copies[3:]:
+        c.wait()
+    col = lax.broadcasted_iota(jnp.int32, (1, len(NEAR) * TOK), 1)
+    k_pos = (2 * ((z + NEAR[0] + N_Z + col // TOK) % N_Z) + core) * TOK + col % TOK
+    tops = scored(N_CHUNK * CHUNK, len(NEAR) * TOK, near[:, :512], near[:, 512:576], k_pos, tops)
     top_maj, top_min = tops
     m_maj = jnp.max(top_maj, axis=1, keepdims=True)
     m_min = jnp.max(top_min, axis=1, keepdims=True)

time: 196 us -> 196 us (level)
  no operation moved by 1% of the time
where the time goes in v5:
time: 196 us; the launch traced here: 195 us
  starting transfers between devices  73.3 us (37%)
  waiting for transfers between devices  52.3 us (27%)
  blocking collectives  45.4 us (23%)
  Pallas kernels  19.1 us (10%)
  local copies, waits for them, and re-layouts  3.63 us (2%)
    all_to_all x2, blocking collectives, to_each(): lax.all_to_all(array, axis, 0, 0, tiled=True, axis_index_groups=groups)  45.4 us
    all_to_all x5, starting transfers between devices, to_each(): lax.all_to_all(array, axis, 0, 0, tiled=True, axis_index_groups=groups)  40.9 us
    all_to_all x5, waiting for transfers between devices, to_each(): lax.all_to_all(array, axis, 0, 0, tiled=True, axis_index_groups=groups)  33.5 us
    pallas_call x10, Pallas kernels, kernel(): pl.pallas_call(body, out_shape=outs, in_specs=[pl.BlockSpec(memory_space=...  19.1 us
    ppermute x3, starting transfers between devices, per_device(): lax.ppermute(own_block, 'sp', along_z(-step))  11.6 us
    ppermute x1, waiting for transfers between devices, per_device(): from_high = lax.ppermute(high, ('sp', 'tp'), ring(-1))  10.5 us
    ppermute x1, starting transfers between devices, per_device(): from_other = lax.ppermute(other, 'sp', OTHER_CORE)  8.06 us
    ppermute x1, waiting for transfers between devices, per_device(): from_low = lax.ppermute(low, ('sp', 'tp'), ring(1))  6.47 us
  transfers between devices with their start and end apart: 12, of which 8 were waited for; matrix products, arithmetic and copies ran while one was open for 1% of the time, Pallas kernels for 2%

profile of v5, /device:TPU:1, one launch (start us, length us, event | category | flops | bytes accessed | tf_op | source)
XLA Modules:
  0.0 195.3 jit_solution(16325619943894664052)
XLA Ops:
  0.0 1.2 shard_map.172
  1.2 27.7 %all_to_all.35.got = bf16[16,8,640]{2,1,0:T(8,128)(2,1)S(1)} all-to-all(bf16[16,8,640]{2,1,0:T(8,128)(2,1)S(1)} %shard_map.172), channel_id=1, replica_groups={{0,32,64,96,128,160,192,224,256,288,320,352,384,416,448,480},{16,48,80,..., dimensions={0} | all-to-all | bytes 327680 | tf_op jit(solution)/shard_map/all_to_all | solution.py:399
  28.9 0.1 shard_map.173.after
  29.0 1.5 broadcast_in_dim.33
  30.5 0.0 copy-start.3
  30.5 0.0 copy-start.7
  30.5 0.0 copy-start.9
  30.5 6.9 %all-to-all-start.1 = ((bf16[16,432,128]{2,1,0:T(8,128)(2,1)}), bf16[16,432,128]{2,1,0:T(8,128)(2,1)S(1)}, u32[]{:S(2)}, u32[]{:S(2)}) async-start(bf16[16,432,128]{2,1,0:T(8,128)(2,1)} %broadcast_in_dim.33), calls=%async_computation.1 | async-start | bytes 3538944 | tf_op jit(solution)/shard_map/all_to_all | solution.py:399
  37.5 0.1 copy.20.ku_min
  37.6 0.1 copy.21.vu_min
  37.7 0.1 copy.19.maj
  37.9 0.8 shard_map.174
  38.7 0.7 copy-done.2
  39.4 5.1 %collective-permute-start.1 = (bf16[128,640]{1,0:T(8,128)(2,1)S(1)}, bf16[128,640]{1,0:T(8,128)(2,1)S(1)}, u32[]{:S(2)}, u32[]{:S(2)}) collective-permute-start(bf16[128,640]{1,0:T(8,128)(2,1)S(1)} %get-tuple-element.16.refs_2_), channel_id=1, source_target_pairs={{0,64},{16,80},{32,96},{48,112},{64,128},{80,144},{96,160},{112,17... | collective-permute-start | bytes 491528 | tf_op jit(solution)/shard_map/ppermute | solution.py:462
  44.5 3.9 %collective-permute-start.2 = (bf16[128,640]{1,0:T(8,128)(2,1)S(1)}, bf16[128,640]{1,0:T(8,128)(2,1)S(1)}, u32[]{:S(2)}, u32[]{:S(2)}) collective-permute-start(bf16[128,640]{1,0:T(8,128)(2,1)S(1)} %get-tuple-element.16.refs_2_), channel_id=1, source_target_pairs={{0,32},{16,48},{32,64},{48,80},{64,96},{80,112},{96,128},{112,144}... | collective-permute-start | bytes 491528 | tf_op jit(solution)/shard_map/ppermute | solution.py:462
  48.5 2.6 %collective-permute-start.3 = (bf16[128,640]{1,0:T(8,128)(2,1)S(1)}, bf16[128,640]{1,0:T(8,128)(2,1)S(1)}, u32[]{:S(2)}, u32[]{:S(2)}) collective-permute-start(bf16[128,640]{1,0:T(8,128)(2,1)S(1)} %get-tuple-element.16.refs_2_), channel_id=1, source_target_pairs={{0,480},{16,496},{32,0},{48,16},{64,32},{80,48},{96,64},{112,80},{... | collective-permute-start | bytes 491528 | tf_op jit(solution)/shard_map/ppermute | solution.py:462
  51.1 6.2 %collective-permute-start = (bf16[128,320]{1,0:T(8,128)(2,1)S(1)}, bf16[128,320]{1,0:T(8,128)(2,1)S(1)}, u32[]{:S(2)}, u32[]{:S(2)}) collective-permute-start(bf16[128,320]{1,0:T(8,128)(2,1)S(1)} %get-tuple-element.14.q_own_in), channel_id=1, source_target_pairs={{0,16},{16,0},{32,48},{48,32},{64,80},{80,64},{96,112},{112,96},{1... | collective-permute-start | bytes 245768 | tf_op jit(solution)/shard_map/ppermute | solution.py:461
  57.3 0.9 collective-permute-done.q_other_in
  58.2 0.0 all-to-all-done.1.keys
  58.3 0.5 copy-done.16
  58.8 0.1 copy-done.13
  58.9 0.1 copy-done.14
  59.0 0.1 copy-done.15
  59.0 5.0 %shard_map.175 = (f32[128,256]{1,0:T(8,128)S(1)}, f32[128,256]{1,0:T(8,128)S(1)}) custom-call(bf16[16,432,128]{2,1,0:T(8,128)(2,1)S(1)} %all-to-all-done.1.keys, bf16[128,320]{1,0:T(8,128)(2,1)} %copy-done.8, bf16[128,320]{1,0:T(8,128)(2,1)} %copy-done.16, bf16[512,384]{1,0:T(8,128)(2,1)} %copy-done.2, bf16[128,640]{1,0:T(8,128)(2,1)} %copy-done.13, ...), custom_call_target="tpu_custom_call" | custom-call | tf_op jit(solution)/shard_map/pallas_call | solution.py:388
  64.1 8.1 %collective-permute-start.4 = (f32[128,256]{1,0:T(8,128)S(1)}, f32[128,256]{1,0:T(8,128)S(1)}, u32[]{:S(2)}, u32[]{:S(2)}) collective-permute-start(f32[128,256]{1,0:T(8,128)S(1)} %get-tuple-element.18), channel_id=1, source_target_pairs={{0,16},{16,0},{32,48},{48,32},{64,80},{80,64},{96,112},{112,96},{1... | collective-permute-start | bytes 393224 | tf_op jit(solution)/shard_map/ppermute | solution.py:480
  72.1 1.0 collective-permute-done.4.b
  73.1 1.4 shard_map.176
  74.5 3.6 %all-to-all-start.2 = ((bf16[16,128,128]{2,1,0:T(8,128)(2,1)}), bf16[16,128,128]{2,1,0:T(8,128)(2,1)S(1)}, u32[]{:S(2)}, u32[]{:S(2)}) async-start(bf16[16,128,128]{2,1,0:T(8,128)(2,1)} %shard_map.176), calls=%async_computation.2 | async-start | bytes 1048576 | tf_op jit(solution)/shard_map/all_to_all | solution.py:399
  78.0 0.1 copy.22.ids
  78.2 10.8 %all-to-all-done.2.parts = bf16[16,128,128]{2,1,0:T(8,128)(2,1)S(1)} async-done(((bf16[16,128,128]{2,1,0:T(8,128)(2,1)}), bf16[16,128,128]{2,1,0:T(8,128)(2,1)S(1)}, u32[]{:S(2)}, u32[]{:S(2)}) %all-to-all-start.2) | async-done | bytes 524320 | tf_op jit(solution)/shard_map/all_to_all | solution.py:399
  89.0 1.3 shard_map.177
  90.3 10.0 %all-to-all-start.3 = ((bf16[32,16,128]{2,1,0:T(8,128)(2,1)}), bf16[32,16,128]{2,1,0:T(8,128)(2,1)S(1)}, u32[]{:S(2)}, u32[]{:S(2)}) async-start(bf16[32,16,128]{2,1,0:T(8,128)(2,1)} %bitcast.1), calls=%async_computation.3 | async-start | bytes 262144 | tf_op jit(solution)/shard_map/all_to_all | solution.py:399
  100.3 3.2 %shard_map.178 = (bf16[6144,128]{1,0:T(8,128)(2,1)}, bf16[6144,128]{1,0:T(8,128)(2,1)S(1)}) custom-call(bf16[1,2048,256]{2,1,0:T(8,128)(2,1)} %gate_a.1, bf16[1,2048,256]{2,1,0:T(8,128)(2,1)} %up_a.1, bf16[1,256,2048]{2,1,0:T(8,128)(2,1)} %down_a.1), custom_call_target="tpu_custom_call" | custom-call | tf_op jit(solution)/shard_map/pallas_call | solution.py:388
  103.5 1.9 collective-permute-start.5
  105.4 4.6 %collective-permute-start.6 = (bf16[6144,128]{1,0:T(8,128)(2,1)S(1)}, bf16[6144,128]{1,0:T(8,128)(2,1)}, u32[]{:S(2)}, u32[]{:S(2)}) collective-permute-start(bf16[6144,128]{1,0:T(8,128)(2,1)S(1)} %get-tuple-element.21), channel_id=1, source_target_pairs={{0,3},{1,0},{2,1},{3,2},{4,7},{5,4},{6,5},{7,6},{8,11},{9,8},{10,9... | collective-permute-start | bytes 4718600 | tf_op jit(solution)/shard_map/ppermute | solution.py:464
  110.0 6.1 %all-to-all-done.3 = bf16[32,16,128]{2,1,0:T(8,128)(2,1)S(1)} async-done(((bf16[32,16,128]{2,1,0:T(8,128)(2,1)}), bf16[32,16,128]{2,1,0:T(8,128)(2,1)S(1)}, u32[]{:S(2)}, u32[]{:S(2)}) %all-to-all-start.3) | async-done | bytes 131104 | tf_op jit(solution)/shard_map/all_to_all | solution.py:399
  116.1 1.1 broadcast_select_fusion
  117.3 3.7 %all-to-all-start.4 = ((bf16[16,256,128]{2,1,0:T(8,128)(2,1)}), bf16[16,256,128]{2,1,0:T(8,128)(2,1)S(1)}, u32[]{:S(2)}, u32[]{:S(2)}) async-start(bf16[16,256,128]{2,1,0:T(8,128)(2,1)} %broadcast_select_fusion), calls=%async_computation.4 | async-start | bytes 2097152 | tf_op jit(solution)/shard_map/all_to_all | solution.py:399
  120.9 6.5 %collective-permute-done.5.low = bf16[6144,128]{1,0:T(8,128)(2,1)} collective-permute-done((bf16[6144,128]{1,0:T(8,128)(2,1)}, bf16[6144,128]{1,0:T(8,128)(2,1)}, u32[]{:S(2)}, u32[]{:S(2)}) %collective-permute-start.5) | collective-permute-done | bytes 1572896 | tf_op jit(solution)/shard_map/ppermute | solution.py:463
  127.4 10.5 %collective-permute-done.6.high = bf16[6144,128]{1,0:T(8,128)(2,1)} collective-permute-done((bf16[6144,128]{1,0:T(8,128)(2,1)S(1)}, bf16[6144,128]{1,0:T(8,128)(2,1)}, u32[]{:S(2)}, u32[]{:S(2)}) %collective-permute-start.6) | collective-permute-done | bytes 1572896 | tf_op jit(solution)/shard_map/ppermute | solution.py:464
  137.9 0.8 all-to-all-done.4.got
  138.7 4.1 %shard_map.179 = bf16[16,256,128]{2,1,0:T(8,128)(2,1)S(1)} custom-call(bf16[16,256,128]{2,1,0:T(8,128)(2,1)S(1)} %all-to-all-done.4.got, f32[1,2048]{1,0:T(1,128)S(1)} %bitcast.10, bf16[1,2048,256]{2,1,0:T(8,128)(2,1)} %gate_a.1, bf16[1,2048,256]{2,1,0:T(8,128)(2,1)} %up_a.1, bf16[1,256,2048]{2,1,0:T(8,128)(2,1)} %down_a.1, ...), custom_call_target="tpu_custom_call" | custom-call | tf_op jit(solution)/shard_map/pallas_call | solution.py:388
  142.9 17.7 %all_to_all.36.parts = bf16[16,256,128]{2,1,0:T(8,128)(2,1)S(1)} all-to-all(bf16[16,256,128]{2,1,0:T(8,128)(2,1)S(1)} %shard_map.179), channel_id=1, replica_groups=mesh['sp'=32,'tp'=16] {'tp'}, dimensions={0} | all-to-all | bytes 2097152 | tf_op jit(solution)/shard_map/all_to_all | solution.py:399
  160.6 0.8 shard_map.180
  161.3 16.8 %all-to-all-start.6 = ((bf16[32,16,128]{2,1,0:T(8,128)(2,1)}), bf16[32,16,128]{2,1,0:T(8,128)(2,1)S(1)}, u32[]{:S(2)}, u32[]{:S(2)}) async-start(bf16[32,16,128]{2,1,0:T(8,128)(2,1)} %bitcast.5), calls=%async_computation.6 | async-start | bytes 262144 | tf_op jit(solution)/shard_map/all_to_all | solution.py:399
  178.2 0.1 copy.24.weights
  178.3 15.7 %all-to-all-done.6 = bf16[32,16,128]{2,1,0:T(8,128)(2,1)S(1)} async-done(((bf16[32,16,128]{2,1,0:T(8,128)(2,1)}), bf16[32,16,128]{2,1,0:T(8,128)(2,1)S(1)}, u32[]{:S(2)}, u32[]{:S(2)}) %all-to-all-start.6) | async-done | bytes 131104 | tf_op jit(solution)/shard_map/all_to_all | solution.py:399
  194.0 1.2 shard_map.181
  (41 shorter events, 0.1 us)
Async XLA Ops:
  30.5 7.0 %copy-start.17 = (bf16[512,64]{0,1:T(8,128)(2,1)S(1)}, bf16[512,64]{0,1:T(8,128)(2,1)}, u32[]{:S(2)}) copy-start(bf16[512,64]{0,1:T(8,128)(2,1)} %param.24) | copy-start | bytes 196612
  30.5 7.1 %copy-start.18 = (bf16[512,64]{0,1:T(8,128)(2,1)S(1)}, bf16[512,64]{0,1:T(8,128)(2,1)}, u32[]{:S(2)}) copy-start(bf16[512,64]{0,1:T(8,128)(2,1)} %param.25) | copy-start | bytes 196612
  30.5 7.2 %copy-start.19 = (bf16[128,192]{0,1:T(8,128)(2,1)S(1)}, bf16[128,192]{0,1:T(8,128)(2,1)}, u32[]{:S(2)}) copy-start(bf16[128,192]{0,1:T(8,128)(2,1)} %param.18) | copy-start | bytes 147460
  30.5 7.4 %copy-start.1 = (bf16[128,512]{1,0:T(8,128)(2,1)S(1)}, bf16[128,512]{1,0:T(8,128)(2,1)}, u32[]{:S(2)}) copy-start(bf16[128,512]{1,0:T(8,128)(2,1)} %lat.1) | copy-start | bytes 393220
  30.5 7.4 %copy-start.3 = (f32[160,128]{1,0:T(8,128)S(1)}, f32[160,128]{1,0:T(8,128)}, u32[]{:S(2)}) copy-start(f32[160,128]{1,0:T(8,128)} %constant.52.clone.table_in.table) | copy-start | bytes 245764
  30.5 7.4 %copy-start.6 = (bf16[512,128]{1,0:T(8,128)(2,1)S(1)}, bf16[512,128]{1,0:T(8,128)(2,1)}, u32[]{:S(2)}) copy-start(bf16[512,128]{1,0:T(8,128)(2,1)} %ku_maj.1) | copy-start | bytes 393220
  30.5 7.4 %copy-start.7 = (bf16[512,128]{1,0:T(8,128)(2,1)S(1)}, bf16[512,128]{1,0:T(8,128)(2,1)}, u32[]{:S(2)}) copy-start(bf16[512,128]{1,0:T(8,128)(2,1)} %vu_maj.1) | copy-start | bytes 393220
  30.5 7.4 %copy-start.9 = (bf16[128,64]{0,1:T(8,128)(2,1)S(1)}, bf16[128,64]{0,1:T(8,128)(2,1)}, u32[]{:S(2)}) copy-start(bf16[128,64]{0,1:T(8,128)(2,1)} %param.21) | copy-start | bytes 49156
  30.5 7.4 %copy-start.11 = (bf16[128,128]{1,0:T(8,128)(2,1)S(1)}, bf16[128,128]{1,0:T(8,128)(2,1)}, u32[]{:S(2)}) copy-start(bf16[128,128]{1,0:T(8,128)(2,1)} %low.1) | copy-start | bytes 98308
  30.5 27.7 %all-to-all-start.1 = ((bf16[16,432,128]{2,1,0:T(8,128)(2,1)}), bf16[16,432,128]{2,1,0:T(8,128)(2,1)S(1)}, u32[]{:S(2)}, u32[]{:S(2)}) async-start(bf16[16,432,128]{2,1,0:T(8,128)(2,1)} %broadcast_in_dim.33), calls=%async_computation.1 | async-start | bytes 3538944 | tf_op jit(solution)/shard_map/all_to_all | solution.py:399
  38.7 0.7 copy-start.2
  39.4 18.9 %copy-start.5 = (bf16[128,640]{1,0:T(8,128)(2,1)}, bf16[128,640]{1,0:T(8,128)(2,1)S(1)}, u32[]{:S(2)}) copy-start(bf16[128,640]{1,0:T(8,128)(2,1)S(1)} %get-tuple-element.16.refs_2_) | copy-start | bytes 491524
  39.4 18.9 %copy-start.8 = (bf16[128,320]{1,0:T(8,128)(2,1)}, bf16[128,320]{1,0:T(8,128)(2,1)S(1)}, u32[]{:S(2)}) copy-start(bf16[128,320]{1,0:T(8,128)(2,1)S(1)} %get-tuple-element.14.q_own_in) | copy-start | bytes 245764
  39.4 33.7 %copy-start = (bf16[128,2048]{1,0:T(8,128)(2,1)S(1)}, bf16[128,2048]{1,0:T(8,128)(2,1)}, u32[]{:S(2)}) copy-start(bf16[128,2048]{1,0:T(8,128)(2,1)} %out_maj.1) | copy-start | bytes 1572868
  39.4 33.7 %copy-start.4 = (bf16[64,2048]{1,0:T(8,128)(2,1)S(1)}, bf16[64,2048]{1,0:T(8,128)(2,1)}, u32[]{:S(2)}) copy-start(bf16[64,2048]{1,0:T(8,128)(2,1)} %out_min.1) | copy-start | bytes 786436
  39.4 18.8 %collective-permute-start.1 = (bf16[128,640]{1,0:T(8,128)(2,1)S(1)}, bf16[128,640]{1,0:T(8,128)(2,1)S(1)}, u32[]{:S(2)}, u32[]{:S(2)}) collective-permute-start(bf16[128,640]{1,0:T(8,128)(2,1)S(1)} %get-tuple-element.16.refs_2_), channel_id=1, source_target_pairs={{0,64},{16,80},{32,96},{48,112},{64,128},{80,144},{96,160},{112,17... | collective-permute-start | bytes 491528 | tf_op jit(solution)/shard_map/ppermute | solution.py:462
  44.5 13.7 %collective-permute-start.2 = (bf16[128,640]{1,0:T(8,128)(2,1)S(1)}, bf16[128,640]{1,0:T(8,128)(2,1)S(1)}, u32[]{:S(2)}, u32[]{:S(2)}) collective-permute-start(bf16[128,640]{1,0:T(8,128)(2,1)S(1)} %get-tuple-element.16.refs_2_), channel_id=1, source_target_pairs={{0,32},{16,48},{32,64},{48,80},{64,96},{80,112},{96,128},{112,144}... | collective-permute-start | bytes 491528 | tf_op jit(solution)/shard_map/ppermute | solution.py:462
  48.5 9.8 %collective-permute-start.3 = (bf16[128,640]{1,0:T(8,128)(2,1)S(1)}, bf16[128,640]{1,0:T(8,128)(2,1)S(1)}, u32[]{:S(2)}, u32[]{:S(2)}) collective-permute-start(bf16[128,640]{1,0:T(8,128)(2,1)S(1)} %get-tuple-element.16.refs_2_), channel_id=1, source_target_pairs={{0,480},{16,496},{32,0},{48,16},{64,32},{80,48},{96,64},{112,80},{... | collective-permute-start | bytes 491528 | tf_op jit(solution)/shard_map/ppermute | solution.py:462
  51.1 7.1 %collective-permute-start = (bf16[128,320]{1,0:T(8,128)(2,1)S(1)}, bf16[128,320]{1,0:T(8,128)(2,1)S(1)}, u32[]{:S(2)}, u32[]{:S(2)}) collective-permute-start(bf16[128,320]{1,0:T(8,128)(2,1)S(1)} %get-tuple-element.14.q_own_in), channel_id=1, source_target_pairs={{0,16},{16,0},{32,48},{48,32},{64,80},{80,64},{96,112},{112,96},{1... | collective-permute-start | bytes 245768 | tf_op jit(solution)/shard_map/ppermute | solution.py:461
  58.2 0.6 copy-start.16
  58.2 0.7 copy-start.13
  58.2 0.8 copy-start.14
  58.2 0.8 copy-start.15
  64.0 14.0 %copy-start.20 = (s32[128,2]{0,1:T(2,128)S(1)}, s32[128,2]{0,1:T(2,128)}, u32[]{:S(2)}) copy-start(s32[128,2]{0,1:T(2,128)} %param.30) | copy-start | bytes 3076
  64.0 24.9 %copy-start.10 = (bf16[128,128]{1,0:T(8,128)(2,1)S(1)}, bf16[128,128]{1,0:T(8,128)(2,1)}, u32[]{:S(2)}) copy-start(bf16[128,128]{1,0:T(8,128)(2,1)} %residual.1) | copy-start | bytes 98308
  64.1 9.0 %collective-permute-start.4 = (f32[128,256]{1,0:T(8,128)S(1)}, f32[128,256]{1,0:T(8,128)S(1)}, u32[]{:S(2)}, u32[]{:S(2)}) collective-permute-start(f32[128,256]{1,0:T(8,128)S(1)} %get-tuple-element.18), channel_id=1, source_target_pairs={{0,16},{16,0},{32,48},{48,32},{64,80},{80,64},{96,112},{112,96},{1... | collective-permute-start | bytes 393224 | tf_op jit(solution)/shard_map/ppermute | solution.py:480
  74.5 14.5 %all-to-all-start.2 = ((bf16[16,128,128]{2,1,0:T(8,128)(2,1)}), bf16[16,128,128]{2,1,0:T(8,128)(2,1)S(1)}, u32[]{:S(2)}, u32[]{:S(2)}) async-start(bf16[16,128,128]{2,1,0:T(8,128)(2,1)} %shard_map.176), calls=%async_computation.2 | async-start | bytes 1048576 | tf_op jit(solution)/shard_map/all_to_all | solution.py:399
  90.3 25.8 %all-to-all-start.3 = ((bf16[32,16,128]{2,1,0:T(8,128)(2,1)}), bf16[32,16,128]{2,1,0:T(8,128)(2,1)S(1)}, u32[]{:S(2)}, u32[]{:S(2)}) async-start(bf16[32,16,128]{2,1,0:T(8,128)(2,1)} %bitcast.1), calls=%async_computation.3 | async-start | bytes 262144 | tf_op jit(solution)/shard_map/all_to_all | solution.py:399
  103.5 23.9 %collective-permute-start.5 = (bf16[6144,128]{1,0:T(8,128)(2,1)}, bf16[6144,128]{1,0:T(8,128)(2,1)}, u32[]{:S(2)}, u32[]{:S(2)}) collective-permute-start(bf16[6144,128]{1,0:T(8,128)(2,1)} %get-tuple-element.20), channel_id=1, source_target_pairs={{0,1},{1,2},{2,3},{3,0},{4,5},{5,6},{6,7},{7,4},{8,9},{9,10},{10,1... | collective-permute-start | bytes 4718600 | tf_op jit(solution)/shard_map/ppermute | solution.py:463
  105.4 32.5 %collective-permute-start.6 = (bf16[6144,128]{1,0:T(8,128)(2,1)S(1)}, bf16[6144,128]{1,0:T(8,128)(2,1)}, u32[]{:S(2)}, u32[]{:S(2)}) collective-permute-start(bf16[6144,128]{1,0:T(8,128)(2,1)S(1)} %get-tuple-element.21), channel_id=1, source_target_pairs={{0,3},{1,0},{2,1},{3,2},{4,7},{5,4},{6,5},{7,6},{8,11},{9,8},{10,9... | collective-permute-start | bytes 4718600 | tf_op jit(solution)/shard_map/ppermute | solution.py:464
  116.1 22.6 %copy-start.12 = (f32[2048]{0:T(1024)S(1)}, f32[2048]{0:T(1024)}, u32[]{:S(2)}) copy-start(f32[2048]{0:T(1024)} %param.29) | copy-start | bytes 24580
  117.3 21.4 %all-to-all-start.4 = ((bf16[16,256,128]{2,1,0:T(8,128)(2,1)}), bf16[16,256,128]{2,1,0:T(8,128)(2,1)S(1)}, u32[]{:S(2)}, u32[]{:S(2)}) async-start(bf16[16,256,128]{2,1,0:T(8,128)(2,1)} %broadcast_select_fusion), calls=%async_computation.4 | async-start | bytes 2097152 | tf_op jit(solution)/shard_map/all_to_all | solution.py:399
  142.8 35.3 %copy-start.21 = (f32[128,2]{0,1:T(2,128)S(1)}, f32[128,2]{0,1:T(2,128)}, u32[]{:S(2)}) copy-start(f32[128,2]{0,1:T(2,128)} %param.31) | copy-start | bytes 3076
  161.3 32.7 %all-to-all-start.6 = ((bf16[32,16,128]{2,1,0:T(8,128)(2,1)}), bf16[32,16,128]{2,1,0:T(8,128)(2,1)S(1)}, u32[]{:S(2)}, u32[]{:S(2)}) async-start(bf16[32,16,128]{2,1,0:T(8,128)(2,1)} %bitcast.5), calls=%async_computation.6 | async-start | bytes 262144 | tf_op jit(solution)/shard_map/all_to_all | solution.py:399

commit v6 on v5

--- a/solution.py
+++ b/solution.py
@@ -25,10 +25,11 @@
 MASKED = -1e30
 NORM_EPS = 1e-6
 HALF = SLOTS // 2
-NEAR = (-2, -1, 0, 1)
+NEAR = (-2, -1, 0, 1, 2)
 FAR = N_Z - len(NEAR)
 FAR_ROWS = FAR * ROWS
-PACKED = 4 * FAR_ROWS + FAR_ROWS // 2
+FIRST_ROPE = -(-FAR_ROWS // 32) * 16
+PACKED = 4 * FAR_ROWS + FIRST_ROPE
 
 
 def along_z(step):
@@ -59,10 +60,11 @@
 
 
 HALF = SLOTS // 2
-NEAR = (-2, -1, 0, 1)
+NEAR = (-2, -1, 0, 1, 2)
 FAR = N_Z - len(NEAR)
 FAR_ROWS = FAR * ROWS
-PACKED = 4 * FAR_ROWS + FAR_ROWS // 2
+FIRST_ROPE = -(-FAR_ROWS // 32) * 16
+PACKED = 4 * FAR_ROWS + FIRST_ROPE
 
 
 def along_z(step):
@@ -129,11 +131,28 @@
         out[z] = row
 
 
-def queries_body(maj, low, table, after, ku_maj, vu_maj, ku_min, vu_min, lat, rope, out, weights, block):
-    weights[...] = jnp.concatenate([ku_maj[...], vu_maj[...], ku_min[...], vu_min[...]], axis=1)
+def queries_body(
+    maj, low_in, table_in, ku_maj, vu_maj, ku_min, vu_min, lat, rope_in,
+    out, weights, block,
+    low, table, rope, sems,
+):
+    copies = fetch(
+        (
+            (low_in, low),
+            (table_in, table),
+            (rope_in, rope),
+            (ku_maj, weights.at[:, pl.ds(0, 128)]),
+            (vu_maj, weights.at[:, pl.ds(128, 128)]),
+            (lat, block.at[:, pl.ds(0, LATENT)]),
+        ),
+        sems,
+    )
+    weights[:, 256:384] = jnp.concatenate([ku_min[...], vu_min[...]], axis=1)
+    for c in copies[:3]:
+        c.wait()
     c, s = turn_at(table, lax.axis_index("sp"), table[2 * N_Z :, :])
     key = turned(rope[...].astype(F32).T, c, s)
-    block[...] = jnp.concatenate([lat[...], key, jnp.zeros((TOK, 64), BF16)], axis=1)
+    block[:, LATENT:] = jnp.concatenate([key, jnp.zeros((TOK, 64), BF16)], axis=1)
     out[...] = jnp.concatenate(
         [
             maj[:, :NOPE_MAJOR],
@@ -143,6 +162,8 @@
         ],
         axis=1,
     )
+    for c in copies[3:]:
+        c.wait()
 
 
 def choose_body(got, out, flat):
@@ -152,10 +173,11 @@
     for k in range(4):
         out[FAR_ROWS * k : FAR_ROWS * (k + 1), :] = flat[:, 128 * k : 128 * (k + 1)]
     rope = flat[:, 512:576]
-    out[4 * FAR_ROWS :, :] = jnp.concatenate([rope[: FAR_ROWS // 2], rope[FAR_ROWS // 2 :]], axis=1)
-
-
-PER = 4
+    rest = jnp.concatenate([rope[FIRST_ROPE:], jnp.zeros((2 * FIRST_ROPE - FAR_ROWS, 64), BF16)], axis=0)
+    out[4 * FAR_ROWS :, :] = jnp.concatenate([rope[:FIRST_ROPE], rest], axis=1)
+
+
+PER = 16
 CHUNK = PER * FAR_ROWS
 N_CHUNK = N_TP // PER
 
@@ -212,7 +234,7 @@
                 )
             )
             half = keys[t, 4 * FAR_ROWS :, :]
-            rope_rows.append(jnp.concatenate([half[:, :64], half[:, 64:]], axis=0))
+            rope_rows.append(jnp.concatenate([half[:, :64], half[: FAR_ROWS - FIRST_ROPE, 64:]], axis=0))
         lat = jnp.concatenate(lat_rows, axis=0)
         rope = jnp.concatenate(rope_rows, axis=0)
         inner = col % FAR_ROWS
@@ -307,25 +329,24 @@
         c.wait()
 
 
-def expert_body(
-    got, gain, gate_a, up_a, down_a, low, high,
-    parts,
-    gate_w, up_w, down_w, x, sems,
-):
-    pairs = [(gate_a.at[0], gate_w.at[0]), (up_a.at[0], up_w.at[0])]
+def assemble_body(gate_a, low, high, gate_w, sems):
+    pairs = [(gate_a.at[0], gate_w.at[:, pl.ds(0, 256)])]
     for i, packed in enumerate((low, high)):
-        mine = pl.ds(128 * i, 128)
-        pairs.append((packed.at[pl.ds(0, D)], gate_w.at[1, :, mine]))
-        pairs.append((packed.at[pl.ds(D, D)], up_w.at[1, :, mine]))
-    pairs.append((down_a.at[0], down_w.at[0]))
+        pairs.append((packed.at[pl.ds(0, D)], gate_w.at[:, pl.ds(256 + 128 * i, 128)]))
+    for c in fetch(pairs, sems):
+        c.wait()
+
+
+def expert_body(got, gain, gate_w, up_a, down_a, low, high, parts, up_w, down_w, x, sems):
+    own = pl.ds(0, 256)
+    pairs = [(up_a.at[0], up_w.at[:, own])]
+    for i, packed in enumerate((low, high)):
+        pairs.append((packed.at[pl.ds(D, D)], up_w.at[:, pl.ds(256 + 128 * i, 128)]))
+    pairs.append((down_a.at[0], down_w.at[own]))
     for i, packed in enumerate((low, high)):
         for t in range(N_TP):
-            pairs.append(
-                (
-                    packed.at[pl.ds(2 * D + 128 * t, 128)],
-                    down_w.at[1, pl.ds(128 * i, 128), pl.ds(128 * t, 128)],
-                )
-            )
+            mine, cols = pl.ds(256 + 128 * i, 128), pl.ds(128 * t, 128)
+            pairs.append((packed.at[pl.ds(2 * D + 128 * t, 128)], down_w.at[mine, cols]))
     copies = fetch(pairs, sems)
     squares = jnp.zeros((HALF, 128), F32)
     for t in range(N_TP):
@@ -336,18 +357,15 @@
         x[:, 128 * t : 128 * (t + 1)] = (
             got[t].astype(F32) * factor * gain[:, 128 * t : 128 * (t + 1)]
         ).astype(BF16)
-    hidden = []
-    for i in range(2):
-        for c in copies[2 * i : 2 + 4 * i]:
-            c.wait()
-        gate = dot(x[...], gate_w[i])
-        up = dot(x[...], up_w[i])
-        hidden.append((gate / (1.0 + jnp.exp(-gate)) * up).astype(BF16))
-    for c in copies[6:]:
+    gate = dot(x[...], gate_w[...])
+    for c in copies[:3]:
+        c.wait()
+    up = dot(x[...], up_w[...])
+    hidden = (gate / (1.0 + jnp.exp(-gate)) * up).astype(BF16)
+    for c in copies[3:]:
         c.wait()
     for t in range(0, N_TP, 2):
-        cols = slice(128 * t, 128 * (t + 2))
-        value = dot(hidden[0], down_w[0, :, cols]) + dot(hidden[1], down_w[1, :, cols])
+        value = dot(hidden, down_w[:, 128 * t : 128 * (t + 2)])
         parts[t] = value[:, :128].astype(BF16)
         parts[t + 1] = value[:, 128:].astype(BF16)
 
@@ -442,13 +460,12 @@
     q_own, up_weights, own_block = kernel(
         queries_body,
         (shape((TOK, 320)), shape((LATENT, 384)), shape((TOK, 640))),
-        [],
-        0,
+        [room((TOK, 128)), room((160, 128), F32), room((ROPE, TOK))],
+        6,
         (
             query_major,
             query_minor,
             table,
-            packed,
             key_up_major,
             value_up_major,
             key_up_minor,
@@ -456,7 +473,7 @@
             latent_rows,
             rope_keys.T,
         ),
-        range(10),
+        (0, 5, 6),
     )
     q_other = lax.ppermute(q_own, "sp", OTHER_CORE)
     blocks = [lax.ppermute(own_block, "sp", along_z(-step)) if step else own_block for step in NEAR]
@@ -500,18 +517,14 @@
     half_of = jnp.where(lax.axis_index("sp") % 2 == 0, peers % 2, (peers // 4) % 2)
     half_rows = jnp.where(half_of[:, None, None] == 0, arrived[0], arrived[1])
     everyone = to_each(half_rows, "tp")
+    gate_w = kernel(assemble_body, shape((D, 512)), [], 3, (gate_proj, from_low, from_high))
     down_parts = kernel(
         expert_body,
         shape((N_TP, HALF, 128)),
-        [
-            room((2, D, 256)),
-            room((2, D, 256)),
-            room((2, 256, D)),
-            room((HALF, D)),
-        ],
-        7 + 2 * N_TP,
-        (everyone, norm_gain.reshape(1, D), gate_proj, up_proj, down_proj, from_low, from_high),
-        (0, 1),
+        [room((D, 512)), room((512, D)), room((HALF, D))],
+        4 + 2 * N_TP,
+        (everyone, norm_gain.reshape(1, D), gate_w, up_proj, down_proj, from_low, from_high),
+        (0, 1, 2),
     )
     down_parts = to_each(down_parts, "tp")
     expert_out = kernel(gather_sum_body, shape((SLOTS, 128)), [], 0, (down_parts,), (0,))

time: 196 us -> 200 us (1.020)
    ppermute x1, starting transfers between devices: 8.06 us -> 3.78 us  [per_device(): from_other = lax.ppermute(other, 'sp', OTHER_CORE)]
    ppermute x3 -> x4, starting transfers between devices: 11.6 us -> 14.4 us  [per_device(): lax.ppermute(own_block, 'sp', along_z(-step))]
    ppermute x3 -> x4, waiting for transfers between devices: 0.01 us -> 2.69 us  [per_device(): lax.ppermute(own_block, 'sp', along_z(-step))]
    pallas_call x10 -> x11, Pallas kernels: 19.1 us -> 21 us  [kernel(): pl.pallas_call(body, out_shape=outs, in_specs=[pl.BlockSpec(memory_space=...]
  transfers between devices with their start and end apart: 12 -> 13, of which waited for: 8 -> 8; matrix products, arithmetic and copies ran while one was open for 1% -> 1% of each run, Pallas kernels for 2% -> 3%
where the time goes in v6:
time: 200 us; the launch traced here: 199 us
  starting transfers between devices  72.8 us (36%)
  waiting for transfers between devices  53.9 us (27%)
  blocking collectives  46.1 us (23%)
  Pallas kernels  21 us (10%)
  local copies, waits for them, and re-layouts  3.39 us (2%)
    all_to_all x2, blocking collectives, to_each(): lax.all_to_all(array, axis, 0, 0, tiled=True, axis_index_groups=groups)  46.1 us
    all_to_all x5, starting transfers between devices, to_each(): lax.all_to_all(array, axis, 0, 0, tiled=True, axis_index_groups=groups)  42.1 us
    all_to_all x5, waiting for transfers between devices, to_each(): lax.all_to_all(array, axis, 0, 0, tiled=True, axis_index_groups=groups)  32.4 us
    pallas_call x11, Pallas kernels, kernel(): pl.pallas_call(body, out_shape=outs, in_specs=[pl.BlockSpec(memory_space=...  21 us
    ppermute x4, starting transfers between devices, per_device(): lax.ppermute(own_block, 'sp', along_z(-step))  14.4 us
    ppermute x1, waiting for transfers between devices, per_device(): from_high = lax.ppermute(high, ('sp', 'tp'), ring(-1))  10.5 us
    ppermute x1, waiting for transfers between devices, per_device(): from_low = lax.ppermute(low, ('sp', 'tp'), ring(1))  6.45 us
    ppermute x1, starting transfers between devices, per_device(): q_other = lax.ppermute(q_own, 'sp', OTHER_CORE)  6.07 us
  transfers between devices with their start and end apart: 13, of which 8 were waited for; matrix products, arithmetic and copies ran while one was open for 1% of the time, Pallas kernels for 3%

profile of v6, /device:TPU:1, one launch (start us, length us, event | category | flops | bytes accessed | tf_op | source)
XLA Modules:
  0.0 198.8 jit_solution(17451543370539964687)
XLA Ops:
  0.0 1.2 shard_map.172
  1.2 27.7 %all_to_all.35.got = bf16[16,8,640]{2,1,0:T(8,128)(2,1)S(1)} all-to-all(bf16[16,8,640]{2,1,0:T(8,128)(2,1)S(1)} %shard_map.172), channel_id=1, replica_groups={{0,32,64,96,128,160,192,224,256,288,320,352,384,416,448,480},{16,48,80,..., dimensions={0} | all-to-all | bytes 327680 | tf_op jit(solution)/shard_map/all_to_all | solution.py:417
  28.9 0.1 shard_map.173
  29.0 1.4 broadcast_in_dim.33
  30.4 6.9 %all-to-all-start.1 = ((bf16[16,400,128]{2,1,0:T(8,128)(2,1)}), bf16[16,400,128]{2,1,0:T(8,128)(2,1)S(1)}, u32[]{:S(2)}, u32[]{:S(2)}) async-start(bf16[16,400,128]{2,1,0:T(8,128)(2,1)} %broadcast_in_dim.33), calls=%async_computation.1 | async-start | bytes 3276800 | tf_op jit(solution)/shard_map/all_to_all | solution.py:417
  37.3 0.1 copy.20.ku_min
  37.5 0.1 copy.21.vu_min
  37.6 0.1 copy.19.maj
  37.7 1.6 shard_map.174
  39.4 0.7 copy-done.1
  40.1 5.1 %collective-permute-start.1 = (bf16[128,640]{1,0:T(8,128)(2,1)S(1)}, bf16[128,640]{1,0:T(8,128)(2,1)S(1)}, u32[]{:S(2)}, u32[]{:S(2)}) collective-permute-start(bf16[128,640]{1,0:T(8,128)(2,1)S(1)} %get-tuple-element.16.refs_2_), channel_id=1, source_target_pairs={{0,64},{16,80},{32,96},{48,112},{64,128},{80,144},{96,160},{112,17... | collective-permute-start | bytes 491528 | tf_op jit(solution)/shard_map/ppermute | solution.py:479
  45.2 3.9 %collective-permute-start.2 = (bf16[128,640]{1,0:T(8,128)(2,1)S(1)}, bf16[128,640]{1,0:T(8,128)(2,1)S(1)}, u32[]{:S(2)}, u32[]{:S(2)}) collective-permute-start(bf16[128,640]{1,0:T(8,128)(2,1)S(1)} %get-tuple-element.16.refs_2_), channel_id=1, source_target_pairs={{0,32},{16,48},{32,64},{48,80},{64,96},{80,112},{96,128},{112,144}... | collective-permute-start | bytes 491528 | tf_op jit(solution)/shard_map/ppermute | solution.py:479
  49.2 2.6 %collective-permute-start.3 = (bf16[128,640]{1,0:T(8,128)(2,1)S(1)}, bf16[128,640]{1,0:T(8,128)(2,1)S(1)}, u32[]{:S(2)}, u32[]{:S(2)}) collective-permute-start(bf16[128,640]{1,0:T(8,128)(2,1)S(1)} %get-tuple-element.16.refs_2_), channel_id=1, source_target_pairs={{0,480},{16,496},{32,0},{48,16},{64,32},{80,48},{96,64},{112,80},{... | collective-permute-start | bytes 491528 | tf_op jit(solution)/shard_map/ppermute | solution.py:479
  51.8 2.8 %collective-permute-start.4 = (bf16[128,640]{1,0:T(8,128)(2,1)S(1)}, bf16[128,640]{1,0:T(8,128)(2,1)S(1)}, u32[]{:S(2)}, u32[]{:S(2)}) collective-permute-start(bf16[128,640]{1,0:T(8,128)(2,1)S(1)} %get-tuple-element.16.refs_2_), channel_id=1, source_target_pairs={{0,448},{16,464},{32,480},{48,496},{64,0},{80,16},{96,32},{112,48}... | collective-permute-start | bytes 491528 | tf_op jit(solution)/shard_map/ppermute | solution.py:479
  54.5 6.1 %collective-permute-start = (bf16[128,320]{1,0:T(8,128)(2,1)S(1)}, bf16[128,320]{1,0:T(8,128)(2,1)S(1)}, u32[]{:S(2)}, u32[]{:S(2)}) collective-permute-start(bf16[128,320]{1,0:T(8,128)(2,1)S(1)} %get-tuple-element.14.q_own_in), channel_id=1, source_target_pairs={{0,16},{16,0},{32,48},{48,32},{64,80},{80,64},{96,112},{112,96},{1... | collective-permute-start | bytes 245768 | tf_op jit(solution)/shard_map/ppermute | solution.py:478
  60.6 0.9 collective-permute-done.q_other_in
  61.6 0.0 collective-permute-done.1.refs_0_
  61.6 2.7 %collective-permute-done.4.refs_4_ = bf16[128,640]{1,0:T(8,128)(2,1)S(1)} collective-permute-done((bf16[128,640]{1,0:T(8,128)(2,1)S(1)}, bf16[128,640]{1,0:T(8,128)(2,1)S(1)}, u32[]{:S(2)}, u32[]{:S(2)}) %collective-permute-start.4) | collective-permute-done | bytes 163872 | tf_op jit(solution)/shard_map/ppermute | solution.py:479
  64.3 0.6 copy-done.10
  64.9 4.6 %shard_map.175 = (f32[128,256]{1,0:T(8,128)S(1)}, f32[128,256]{1,0:T(8,128)S(1)}) custom-call(bf16[16,400,128]{2,1,0:T(8,128)(2,1)S(1)} %all-to-all-done.1.keys, bf16[128,320]{1,0:T(8,128)(2,1)} %copy-done.4, bf16[128,320]{1,0:T(8,128)(2,1)} %copy-done.11, bf16[512,384]{1,0:T(8,128)(2,1)} %copy-done.1, bf16[128,640]{1,0:T(8,128)(2,1)} %copy-done.7, ...), custom_call_target="tpu_custom_call" | custom-call | tf_op jit(solution)/shard_map/pallas_call | solution.py:406
  69.5 0.0 copy-start.15
  69.6 0.0 copy-start.5
  69.6 3.8 %collective-permute-start.5 = (f32[128,256]{1,0:T(8,128)S(1)}, f32[128,256]{1,0:T(8,128)S(1)}, u32[]{:S(2)}, u32[]{:S(2)}) collective-permute-start(f32[128,256]{1,0:T(8,128)S(1)} %get-tuple-element.18), channel_id=1, source_target_pairs={{0,16},{16,0},{32,48},{48,32},{64,80},{80,64},{96,112},{112,96},{1... | collective-permute-start | bytes 393224 | tf_op jit(solution)/shard_map/ppermute | solution.py:497
  73.4 1.0 collective-permute-done.5.b
  74.3 1.4 shard_map.176
  75.7 6.9 %all-to-all-start.2 = ((bf16[16,128,128]{2,1,0:T(8,128)(2,1)}), bf16[16,128,128]{2,1,0:T(8,128)(2,1)S(1)}, u32[]{:S(2)}, u32[]{:S(2)}) async-start(bf16[16,128,128]{2,1,0:T(8,128)(2,1)} %shard_map.176), calls=%async_computation.2 | async-start | bytes 1048576 | tf_op jit(solution)/shard_map/all_to_all | solution.py:417
  82.6 0.1 copy.22.ids
  82.7 10.6 %all-to-all-done.2.parts = bf16[16,128,128]{2,1,0:T(8,128)(2,1)S(1)} async-done(((bf16[16,128,128]{2,1,0:T(8,128)(2,1)}), bf16[16,128,128]{2,1,0:T(8,128)(2,1)S(1)}, u32[]{:S(2)}, u32[]{:S(2)}) %all-to-all-start.2) | async-done | bytes 524320 | tf_op jit(solution)/shard_map/all_to_all | solution.py:417
  93.4 1.3 shard_map.177
  94.7 8.7 %all-to-all-start.3 = ((bf16[32,16,128]{2,1,0:T(8,128)(2,1)}), bf16[32,16,128]{2,1,0:T(8,128)(2,1)S(1)}, u32[]{:S(2)}, u32[]{:S(2)}) async-start(bf16[32,16,128]{2,1,0:T(8,128)(2,1)} %bitcast.1), calls=%async_computation.3 | async-start | bytes 262144 | tf_op jit(solution)/shard_map/all_to_all | solution.py:417
  103.4 3.2 %shard_map.178 = (bf16[6144,128]{1,0:T(8,128)(2,1)}, bf16[6144,128]{1,0:T(8,128)(2,1)S(1)}) custom-call(bf16[1,2048,256]{2,1,0:T(8,128)(2,1)} %gate_a.1, bf16[1,2048,256]{2,1,0:T(8,128)(2,1)} %up_a.1, bf16[1,256,2048]{2,1,0:T(8,128)(2,1)} %down_a.1), custom_call_target="tpu_custom_call" | custom-call | tf_op jit(solution)/shard_map/pallas_call | solution.py:406
  106.6 1.9 collective-permute-start.6
  108.5 4.6 %collective-permute-start.7 = (bf16[6144,128]{1,0:T(8,128)(2,1)S(1)}, bf16[6144,128]{1,0:T(8,128)(2,1)}, u32[]{:S(2)}, u32[]{:S(2)}) collective-permute-start(bf16[6144,128]{1,0:T(8,128)(2,1)S(1)} %get-tuple-element.21), channel_id=1, source_target_pairs={{0,3},{1,0},{2,1},{3,2},{4,7},{5,4},{6,5},{7,6},{8,11},{9,8},{10,9... | collective-permute-start | bytes 4718600 | tf_op jit(solution)/shard_map/ppermute | solution.py:481
  113.1 6.1 %all-to-all-done.3 = bf16[32,16,128]{2,1,0:T(8,128)(2,1)S(1)} async-done(((bf16[32,16,128]{2,1,0:T(8,128)(2,1)}), bf16[32,16,128]{2,1,0:T(8,128)(2,1)S(1)}, u32[]{:S(2)}, u32[]{:S(2)}) %all-to-all-start.3) | async-done | bytes 131104 | tf_op jit(solution)/shard_map/all_to_all | solution.py:417
  119.2 1.2 broadcast_select_fusion
  120.4 3.7 %all-to-all-start.4 = ((bf16[16,256,128]{2,1,0:T(8,128)(2,1)}), bf16[16,256,128]{2,1,0:T(8,128)(2,1)S(1)}, u32[]{:S(2)}, u32[]{:S(2)}) async-start(bf16[16,256,128]{2,1,0:T(8,128)(2,1)} %broadcast_select_fusion), calls=%async_computation.4 | async-start | bytes 2097152 | tf_op jit(solution)/shard_map/all_to_all | solution.py:417
  124.0 0.0 copy-start.6
  124.1 6.4 %collective-permute-done.6.low = bf16[6144,128]{1,0:T(8,128)(2,1)} collective-permute-done((bf16[6144,128]{1,0:T(8,128)(2,1)}, bf16[6144,128]{1,0:T(8,128)(2,1)}, u32[]{:S(2)}, u32[]{:S(2)}) %collective-permute-start.6) | collective-permute-done | bytes 1572896 | tf_op jit(solution)/shard_map/ppermute | solution.py:480
  130.5 10.5 %collective-permute-done.7.high = bf16[6144,128]{1,0:T(8,128)(2,1)} collective-permute-done((bf16[6144,128]{1,0:T(8,128)(2,1)S(1)}, bf16[6144,128]{1,0:T(8,128)(2,1)}, u32[]{:S(2)}, u32[]{:S(2)}) %collective-permute-start.7) | collective-permute-done | bytes 1572896 | tf_op jit(solution)/shard_map/ppermute | solution.py:481
  141.0 1.5 shard_map.179.gate_w
  142.5 4.0 %shard_map.180 = bf16[16,256,128]{2,1,0:T(8,128)(2,1)S(1)} custom-call(bf16[16,256,128]{2,1,0:T(8,128)(2,1)S(1)} %all-to-all-done.4.got, f32[1,2048]{1,0:T(1,128)S(1)} %bitcast.8, bf16[2048,512]{1,0:T(8,128)(2,1)S(1)} %shard_map.179.gate_w, bf16[1,2048,256]{2,1,0:T(8,128)(2,1)} %up_a.1, bf16[1,256,2048]{2,1,0:T(8,128)(2,1)} %down_a.1, ...), custom_call_target="tpu_custom_call" | custom-call | tf_op jit(solution)/shard_map/pallas_call | solution.py:406
  146.6 0.0 copy-start.16
  146.6 18.4 %all_to_all.36.parts = bf16[16,256,128]{2,1,0:T(8,128)(2,1)S(1)} all-to-all(bf16[16,256,128]{2,1,0:T(8,128)(2,1)S(1)} %shard_map.180), channel_id=1, replica_groups=mesh['sp'=32,'tp'=16] {'tp'}, dimensions={0} | all-to-all | bytes 2097152 | tf_op jit(solution)/shard_map/all_to_all | solution.py:417
  165.0 0.8 shard_map.181
  165.8 16.0 %all-to-all-start.6 = ((bf16[32,16,128]{2,1,0:T(8,128)(2,1)}), bf16[32,16,128]{2,1,0:T(8,128)(2,1)S(1)}, u32[]{:S(2)}, u32[]{:S(2)}) async-start(bf16[32,16,128]{2,1,0:T(8,128)(2,1)} %bitcast.5), calls=%async_computation.6 | async-start | bytes 262144 | tf_op jit(solution)/shard_map/all_to_all | solution.py:417
  181.7 0.1 copy.24.weights
  181.9 15.7 %all-to-all-done.6 = bf16[32,16,128]{2,1,0:T(8,128)(2,1)S(1)} async-done(((bf16[32,16,128]{2,1,0:T(8,128)(2,1)}), bf16[32,16,128]{2,1,0:T(8,128)(2,1)S(1)}, u32[]{:S(2)}, u32[]{:S(2)}) %all-to-all-start.6) | async-done | bytes 131104 | tf_op jit(solution)/shard_map/all_to_all | solution.py:417
  197.6 1.2 shard_map.182
  (34 shorter events, 0.1 us)
Async XLA Ops:
  30.4 6.9 %copy-start.12 = (bf16[512,64]{0,1:T(8,128)(2,1)S(1)}, bf16[512,64]{0,1:T(8,128)(2,1)}, u32[]{:S(2)}) copy-start(bf16[512,64]{0,1:T(8,128)(2,1)} %param.24) | copy-start | bytes 196612
  30.4 7.0 %copy-start.13 = (bf16[512,64]{0,1:T(8,128)(2,1)S(1)}, bf16[512,64]{0,1:T(8,128)(2,1)}, u32[]{:S(2)}) copy-start(bf16[512,64]{0,1:T(8,128)(2,1)} %param.25) | copy-start | bytes 196612
  30.4 7.2 %copy-start.14 = (bf16[128,192]{0,1:T(8,128)(2,1)S(1)}, bf16[128,192]{0,1:T(8,128)(2,1)}, u32[]{:S(2)}) copy-start(bf16[128,192]{0,1:T(8,128)(2,1)} %param.18) | copy-start | bytes 147460
  30.4 33.9 %all-to-all-start.1 = ((bf16[16,400,128]{2,1,0:T(8,128)(2,1)}), bf16[16,400,128]{2,1,0:T(8,128)(2,1)S(1)}, u32[]{:S(2)}, u32[]{:S(2)}) async-start(bf16[16,400,128]{2,1,0:T(8,128)(2,1)} %broadcast_in_dim.33), calls=%async_computation.1 | async-start | bytes 3276800 | tf_op jit(solution)/shard_map/all_to_all | solution.py:417
  39.4 0.8 copy-start.1
  40.1 24.2 %copy-start.3 = (bf16[128,640]{1,0:T(8,128)(2,1)}, bf16[128,640]{1,0:T(8,128)(2,1)S(1)}, u32[]{:S(2)}) copy-start(bf16[128,640]{1,0:T(8,128)(2,1)S(1)} %get-tuple-element.16.refs_2_) | copy-start | bytes 491524
  40.1 24.2 %copy-start.4 = (bf16[128,320]{1,0:T(8,128)(2,1)}, bf16[128,320]{1,0:T(8,128)(2,1)S(1)}, u32[]{:S(2)}) copy-start(bf16[128,320]{1,0:T(8,128)(2,1)S(1)} %get-tuple-element.14.q_own_in) | copy-start | bytes 245764
  40.1 34.2 %copy-start = (bf16[128,2048]{1,0:T(8,128)(2,1)S(1)}, bf16[128,2048]{1,0:T(8,128)(2,1)}, u32[]{:S(2)}) copy-start(bf16[128,2048]{1,0:T(8,128)(2,1)} %out_maj.1) | copy-start | bytes 1572868
  40.1 34.2 %copy-start.2 = (bf16[64,2048]{1,0:T(8,128)(2,1)S(1)}, bf16[64,2048]{1,0:T(8,128)(2,1)}, u32[]{:S(2)}) copy-start(bf16[64,2048]{1,0:T(8,128)(2,1)} %out_min.1) | copy-start | bytes 786436
  40.1 21.4 %collective-permute-start.1 = (bf16[128,640]{1,0:T(8,128)(2,1)S(1)}, bf16[128,640]{1,0:T(8,128)(2,1)S(1)}, u32[]{:S(2)}, u32[]{:S(2)}) collective-permute-start(bf16[128,640]{1,0:T(8,128)(2,1)S(1)} %get-tuple-element.16.refs_2_), channel_id=1, source_target_pairs={{0,64},{16,80},{32,96},{48,112},{64,128},{80,144},{96,160},{112,17... | collective-permute-start | bytes 491528 | tf_op jit(solution)/shard_map/ppermute | solution.py:479
  45.2 16.3 %collective-permute-start.2 = (bf16[128,640]{1,0:T(8,128)(2,1)S(1)}, bf16[128,640]{1,0:T(8,128)(2,1)S(1)}, u32[]{:S(2)}, u32[]{:S(2)}) collective-permute-start(bf16[128,640]{1,0:T(8,128)(2,1)S(1)} %get-tuple-element.16.refs_2_), channel_id=1, source_target_pairs={{0,32},{16,48},{32,64},{48,80},{64,96},{80,112},{96,128},{112,144}... | collective-permute-start | bytes 491528 | tf_op jit(solution)/shard_map/ppermute | solution.py:479
  49.2 12.4 %collective-permute-start.3 = (bf16[128,640]{1,0:T(8,128)(2,1)S(1)}, bf16[128,640]{1,0:T(8,128)(2,1)S(1)}, u32[]{:S(2)}, u32[]{:S(2)}) collective-permute-start(bf16[128,640]{1,0:T(8,128)(2,1)S(1)} %get-tuple-element.16.refs_2_), channel_id=1, source_target_pairs={{0,480},{16,496},{32,0},{48,16},{64,32},{80,48},{96,64},{112,80},{... | collective-permute-start | bytes 491528 | tf_op jit(solution)/shard_map/ppermute | solution.py:479
  51.8 12.5 %collective-permute-start.4 = (bf16[128,640]{1,0:T(8,128)(2,1)S(1)}, bf16[128,640]{1,0:T(8,128)(2,1)S(1)}, u32[]{:S(2)}, u32[]{:S(2)}) collective-permute-start(bf16[128,640]{1,0:T(8,128)(2,1)S(1)} %get-tuple-element.16.refs_2_), channel_id=1, source_target_pairs={{0,448},{16,464},{32,480},{48,496},{64,0},{80,16},{96,32},{112,48}... | collective-permute-start | bytes 491528 | tf_op jit(solution)/shard_map/ppermute | solution.py:479
  54.5 7.0 %collective-permute-start = (bf16[128,320]{1,0:T(8,128)(2,1)S(1)}, bf16[128,320]{1,0:T(8,128)(2,1)S(1)}, u32[]{:S(2)}, u32[]{:S(2)}) collective-permute-start(bf16[128,320]{1,0:T(8,128)(2,1)S(1)} %get-tuple-element.14.q_own_in), channel_id=1, source_target_pairs={{0,16},{16,0},{32,48},{48,32},{64,80},{80,64},{96,112},{112,96},{1... | collective-permute-start | bytes 245768 | tf_op jit(solution)/shard_map/ppermute | solution.py:478
  61.5 2.7 %copy-start.11 = (bf16[128,320]{1,0:T(8,128)(2,1)}, bf16[128,320]{1,0:T(8,128)(2,1)S(1)}, u32[]{:S(2)}) copy-start(bf16[128,320]{1,0:T(8,128)(2,1)S(1)} %collective-permute-done.q_other_in) | copy-start | bytes 245764
  61.6 2.8 %copy-start.7 = (bf16[128,640]{1,0:T(8,128)(2,1)}, bf16[128,640]{1,0:T(8,128)(2,1)S(1)}, u32[]{:S(2)}) copy-start(bf16[128,640]{1,0:T(8,128)(2,1)S(1)} %collective-permute-done.1.refs_0_) | copy-start | bytes 491524
  61.6 2.8 %copy-start.8 = (bf16[128,640]{1,0:T(8,128)(2,1)}, bf16[128,640]{1,0:T(8,128)(2,1)S(1)}, u32[]{:S(2)}) copy-start(bf16[128,640]{1,0:T(8,128)(2,1)S(1)} %collective-permute-done.2.refs_1_) | copy-start | bytes 491524
  61.6 2.7 %copy-start.9 = (bf16[128,640]{1,0:T(8,128)(2,1)}, bf16[128,640]{1,0:T(8,128)(2,1)S(1)}, u32[]{:S(2)}) copy-start(bf16[128,640]{1,0:T(8,128)(2,1)S(1)} %collective-permute-done.3.refs_3_) | copy-start | bytes 491524
  64.3 0.7 copy-start.10
  69.5 13.1 %copy-start.15 = (s32[128,2]{0,1:T(2,128)S(1)}, s32[128,2]{0,1:T(2,128)}, u32[]{:S(2)}) copy-start(s32[128,2]{0,1:T(2,128)} %param.30) | copy-start | bytes 3076
  69.6 23.8 %copy-start.5 = (bf16[128,128]{1,0:T(8,128)(2,1)S(1)}, bf16[128,128]{1,0:T(8,128)(2,1)}, u32[]{:S(2)}) copy-start(bf16[128,128]{1,0:T(8,128)(2,1)} %residual.1) | copy-start | bytes 98308
  69.6 4.8 %collective-permute-start.5 = (f32[128,256]{1,0:T(8,128)S(1)}, f32[128,256]{1,0:T(8,128)S(1)}, u32[]{:S(2)}, u32[]{:S(2)}) collective-permute-start(f32[128,256]{1,0:T(8,128)S(1)} %get-tuple-element.18), channel_id=1, source_target_pairs={{0,16},{16,0},{32,48},{48,32},{64,80},{80,64},{96,112},{112,96},{1... | collective-permute-start | bytes 393224 | tf_op jit(solution)/shard_map/ppermute | solution.py:497
  75.7 17.7 %all-to-all-start.2 = ((bf16[16,128,128]{2,1,0:T(8,128)(2,1)}), bf16[16,128,128]{2,1,0:T(8,128)(2,1)S(1)}, u32[]{:S(2)}, u32[]{:S(2)}) async-start(bf16[16,128,128]{2,1,0:T(8,128)(2,1)} %shard_map.176), calls=%async_computation.2 | async-start | bytes 1048576 | tf_op jit(solution)/shard_map/all_to_all | solution.py:417
  94.7 24.5 %all-to-all-start.3 = ((bf16[32,16,128]{2,1,0:T(8,128)(2,1)}), bf16[32,16,128]{2,1,0:T(8,128)(2,1)S(1)}, u32[]{:S(2)}, u32[]{:S(2)}) async-start(bf16[32,16,128]{2,1,0:T(8,128)(2,1)} %bitcast.1), calls=%async_computation.3 | async-start | bytes 262144 | tf_op jit(solution)/shard_map/all_to_all | solution.py:417
  106.6 23.9 %collective-permute-start.6 = (bf16[6144,128]{1,0:T(8,128)(2,1)}, bf16[6144,128]{1,0:T(8,128)(2,1)}, u32[]{:S(2)}, u32[]{:S(2)}) collective-permute-start(bf16[6144,128]{1,0:T(8,128)(2,1)} %get-tuple-element.20), channel_id=1, source_target_pairs={{0,1},{1,2},{2,3},{3,0},{4,5},{5,6},{6,7},{7,4},{8,9},{9,10},{10,1... | collective-permute-start | bytes 4718600 | tf_op jit(solution)/shard_map/ppermute | solution.py:480
  108.5 32.5 %collective-permute-start.7 = (bf16[6144,128]{1,0:T(8,128)(2,1)S(1)}, bf16[6144,128]{1,0:T(8,128)(2,1)}, u32[]{:S(2)}, u32[]{:S(2)}) collective-permute-start(bf16[6144,128]{1,0:T(8,128)(2,1)S(1)} %get-tuple-element.21), channel_id=1, source_target_pairs={{0,3},{1,0},{2,1},{3,2},{4,7},{5,4},{6,5},{7,6},{8,11},{9,8},{10,9... | collective-permute-start | bytes 4718600 | tf_op jit(solution)/shard_map/ppermute | solution.py:481
  120.4 22.1 %all-to-all-start.4 = ((bf16[16,256,128]{2,1,0:T(8,128)(2,1)}), bf16[16,256,128]{2,1,0:T(8,128)(2,1)S(1)}, u32[]{:S(2)}, u32[]{:S(2)}) async-start(bf16[16,256,128]{2,1,0:T(8,128)(2,1)} %broadcast_select_fusion), calls=%async_computation.4 | async-start | bytes 2097152 | tf_op jit(solution)/shard_map/all_to_all | solution.py:417
  124.0 18.5 %copy-start.6 = (f32[2048]{0:T(1024)S(1)}, f32[2048]{0:T(1024)}, u32[]{:S(2)}) copy-start(f32[2048]{0:T(1024)} %param.29) | copy-start | bytes 24580
  146.6 35.2 %copy-start.16 = (f32[128,2]{0,1:T(2,128)S(1)}, f32[128,2]{0,1:T(2,128)}, u32[]{:S(2)}) copy-start(f32[128,2]{0,1:T(2,128)} %param.31) | copy-start | bytes 3076
  165.8 31.8 %all-to-all-start.6 = ((bf16[32,16,128]{2,1,0:T(8,128)(2,1)}), bf16[32,16,128]{2,1,0:T(8,128)(2,1)S(1)}, u32[]{:S(2)}, u32[]{:S(2)}) async-start(bf16[32,16,128]{2,1,0:T(8,128)(2,1)} %bitcast.5), calls=%async_computation.6 | async-start | bytes 262144 | tf_op jit(solution)/shard_map/all_to_all | solution.py:417

commit v7 on v6

--- a/solution.py
+++ b/solution.py
@@ -25,15 +25,15 @@
 MASKED = -1e30
 NORM_EPS = 1e-6
 HALF = SLOTS // 2
-NEAR = (-2, -1, 0, 1, 2)
+NEAR = (-2, -1, 0, 1)
 FAR = N_Z - len(NEAR)
 FAR_ROWS = FAR * ROWS
-FIRST_ROPE = -(-FAR_ROWS // 32) * 16
-PACKED = 4 * FAR_ROWS + FIRST_ROPE
+PACKED = 4 * FAR_ROWS + FAR_ROWS // 2
 
 
 def along_z(step):
-    return [(z * 2 + c, (z + step) % N_Z * 2 + c) for z in range(N_Z) for c in range(2)]
+    moves = [(z, (z + step) % N_Z) for z in range(N_Z)]
+    return [(a * 2 + c, b * 2 + c) for a, b in moves if a <= b for c in range(2)]
 
 
 def turns(positions):
@@ -60,15 +60,15 @@
 
 
 HALF = SLOTS // 2
-NEAR = (-2, -1, 0, 1, 2)
+NEAR = (-2, -1, 0, 1)
 FAR = N_Z - len(NEAR)
 FAR_ROWS = FAR * ROWS
-FIRST_ROPE = -(-FAR_ROWS // 32) * 16
-PACKED = 4 * FAR_ROWS + FIRST_ROPE
+PACKED = 4 * FAR_ROWS + FAR_ROWS // 2
 
 
 def along_z(step):
-    return [(z * 2 + c, (z + step) % N_Z * 2 + c) for z in range(N_Z) for c in range(2)]
+    moves = [(z, (z + step) % N_Z) for z in range(N_Z)]
+    return [(a * 2 + c, b * 2 + c) for a, b in moves if a <= b for c in range(2)]
 
 
 def turns(positions):
@@ -173,11 +173,10 @@
     for k in range(4):
         out[FAR_ROWS * k : FAR_ROWS * (k + 1), :] = flat[:, 128 * k : 128 * (k + 1)]
     rope = flat[:, 512:576]
-    rest = jnp.concatenate([rope[FIRST_ROPE:], jnp.zeros((2 * FIRST_ROPE - FAR_ROWS, 64), BF16)], axis=0)
-    out[4 * FAR_ROWS :, :] = jnp.concatenate([rope[:FIRST_ROPE], rest], axis=1)
-
-
-PER = 16
+    out[4 * FAR_ROWS :, :] = jnp.concatenate([rope[: FAR_ROWS // 2], rope[FAR_ROWS // 2 :]], axis=1)
+
+
+PER = 4
 CHUNK = PER * FAR_ROWS
 N_CHUNK = N_TP // PER
 
@@ -234,7 +233,7 @@
                 )
             )
             half = keys[t, 4 * FAR_ROWS :, :]
-            rope_rows.append(jnp.concatenate([half[:, :64], half[: FAR_ROWS - FIRST_ROPE, 64:]], axis=0))
+            rope_rows.append(jnp.concatenate([half[:, :64], half[:, 64:]], axis=0))
         lat = jnp.concatenate(lat_rows, axis=0)
         rope = jnp.concatenate(rope_rows, axis=0)
         inner = col % FAR_ROWS
@@ -349,18 +348,21 @@
             pairs.append((packed.at[pl.ds(2 * D + 128 * t, 128)], down_w.at[mine, cols]))
     copies = fetch(pairs, sems)
     squares = jnp.zeros((HALF, 128), F32)
-    for t in range(N_TP):
-        v = got[t].astype(F32)
-        squares = squares + v * v
+    gate = jnp.zeros((HALF, 512), F32)
+    wide = 4
+    for n in range(0, N_TP, wide):
+        for t in range(n, n + wide):
+            cols = slice(128 * t, 128 * (t + 1))
+            v = got[t].astype(F32)
+            squares = squares + v * v
+            x[:, cols] = (v * gain[:, cols]).astype(BF16)
+        cols = slice(128 * n, 128 * (n + wide))
+        gate = gate + dot(x[:, cols], gate_w[cols, :])
     factor = lax.rsqrt(jnp.sum(squares, axis=1, keepdims=True) / D + NORM_EPS)
-    for t in range(N_TP):
-        x[:, 128 * t : 128 * (t + 1)] = (
-            got[t].astype(F32) * factor * gain[:, 128 * t : 128 * (t + 1)]
-        ).astype(BF16)
-    gate = dot(x[...], gate_w[...])
     for c in copies[:3]:
         c.wait()
-    up = dot(x[...], up_w[...])
+    gate = gate * factor
+    up = dot(x[...], up_w[...]) * factor
     hidden = (gate / (1.0 + jnp.exp(-gate)) * up).astype(BF16)
     for c in copies[3:]:
         c.wait()

time: 200 us -> 197 us (0.985)
  starting transfers between devices: 72.8 us -> 70.1 us
    ppermute x1, starting transfers between devices: 3.78 us -> 8.79 us  [per_device(): from_other = lax.ppermute(other, 'sp', OTHER_CORE)]
    ppermute x4 -> x3, starting transfers between devices: 14.4 us -> 10.3 us  [per_device(): lax.ppermute(own_block, 'sp', along_z(-step))]
    ppermute x4 -> x3, waiting for transfers between devices: 2.69 us -> 0.01 us  [per_device(): lax.ppermute(own_block, 'sp', along_z(-step))]
    all_to_all x5, waiting for transfers between devices: 32.4 us -> 34.8 us  [to_each(): lax.all_to_all(array, axis, 0, 0, tiled=True, axis_index_groups=groups)]
    all_to_all x5, starting transfers between devices: 42.1 us -> 40 us  [to_each(): lax.all_to_all(array, axis, 0, 0, tiled=True, axis_index_groups=groups)]
  transfers between devices with their start and end apart: 13 -> 12, of which waited for: 8 -> 8; matrix products, arithmetic and copies ran while one was open for 1% -> 1% of each run, Pallas kernels for 3% -> 3%
where the time goes in v7:
time: 197 us; the launch traced here: 196 us
  starting transfers between devices  70.1 us (36%)
  waiting for transfers between devices  53.7 us (27%)
  blocking collectives  46.1 us (23%)
  Pallas kernels  21.4 us (11%)
  local copies, waits for them, and re-layouts  2.85 us (1%)
    all_to_all x2, blocking collectives, to_each(): lax.all_to_all(array, axis, 0, 0, tiled=True, axis_index_groups=groups)  46.1 us
    all_to_all x5, starting transfers between devices, to_each(): lax.all_to_all(array, axis, 0, 0, tiled=True, axis_index_groups=groups)  40 us
    all_to_all x5, waiting for transfers between devices, to_each(): lax.all_to_all(array, axis, 0, 0, tiled=True, axis_index_groups=groups)  34.8 us
    pallas_call x11, Pallas kernels, kernel(): pl.pallas_call(body, out_shape=outs, in_specs=[pl.BlockSpec(memory_space=...  21.4 us
    ppermute x1, waiting for transfers between devices, per_device(): from_high = lax.ppermute(high, ('sp', 'tp'), ring(-1))  10.4 us
    ppermute x3, starting transfers between devices, per_device(): lax.ppermute(own_block, 'sp', along_z(-step))  10.3 us
    ppermute x1, starting transfers between devices, per_device(): from_other = lax.ppermute(other, 'sp', OTHER_CORE)  8.79 us
    ppermute x1, waiting for transfers between devices, per_device(): from_low = lax.ppermute(low, ('sp', 'tp'), ring(1))  6.49 us
  transfers between devices with their start and end apart: 12, of which 8 were waited for; matrix products, arithmetic and copies ran while one was open for 1% of the time, Pallas kernels for 3%

profile of v7, /device:TPU:1, one launch (start us, length us, event | category | flops | bytes accessed | tf_op | source)
XLA Modules:
  0.0 195.7 jit_solution(2284827826505149184)
XLA Ops:
  0.0 1.2 shard_map.172
  1.2 27.7 %all_to_all.35.got = bf16[16,8,640]{2,1,0:T(8,128)(2,1)S(1)} all-to-all(bf16[16,8,640]{2,1,0:T(8,128)(2,1)S(1)} %shard_map.172), channel_id=1, replica_groups={{0,32,64,96,128,160,192,224,256,288,320,352,384,416,448,480},{16,48,80,..., dimensions={0} | all-to-all | bytes 327680 | tf_op jit(solution)/shard_map/all_to_all | solution.py:419
  28.9 0.1 shard_map.173
  29.0 1.5 broadcast_in_dim.33
  30.5 6.9 %all-to-all-start.1 = ((bf16[16,432,128]{2,1,0:T(8,128)(2,1)}), bf16[16,432,128]{2,1,0:T(8,128)(2,1)S(1)}, u32[]{:S(2)}, u32[]{:S(2)}) async-start(bf16[16,432,128]{2,1,0:T(8,128)(2,1)} %broadcast_in_dim.33), calls=%async_computation.1 | async-start | bytes 3538944 | tf_op jit(solution)/shard_map/all_to_all | solution.py:419
  37.4 0.1 copy.20.ku_min
  37.5 0.1 copy.21.vu_min
  37.7 0.1 copy.19.maj
  37.8 1.6 shard_map.174
  39.4 0.7 copy-done.1
  40.2 5.1 %collective-permute-start.1 = (bf16[128,640]{1,0:T(8,128)(2,1)S(1)}, bf16[128,640]{1,0:T(8,128)(2,1)S(1)}, u32[]{:S(2)}, u32[]{:S(2)}) collective-permute-start(bf16[128,640]{1,0:T(8,128)(2,1)S(1)} %get-tuple-element.16.refs_2_), channel_id=1, source_target_pairs={{0,64},{16,80},{32,96},{48,112},{64,128},{80,144},{96,160},{112,17... | collective-permute-start | bytes 491528 | tf_op jit(solution)/shard_map/ppermute | solution.py:481
  45.3 3.9 %collective-permute-start.2 = (bf16[128,640]{1,0:T(8,128)(2,1)S(1)}, bf16[128,640]{1,0:T(8,128)(2,1)S(1)}, u32[]{:S(2)}, u32[]{:S(2)}) collective-permute-start(bf16[128,640]{1,0:T(8,128)(2,1)S(1)} %get-tuple-element.16.refs_2_), channel_id=1, source_target_pairs={{0,32},{16,48},{32,64},{48,80},{64,96},{80,112},{96,128},{112,144}... | collective-permute-start | bytes 491528 | tf_op jit(solution)/shard_map/ppermute | solution.py:481
  49.2 1.3 collective-permute-start.3
  50.5 4.5 %collective-permute-start = (bf16[128,320]{1,0:T(8,128)(2,1)S(1)}, bf16[128,320]{1,0:T(8,128)(2,1)S(1)}, u32[]{:S(2)}, u32[]{:S(2)}) collective-permute-start(bf16[128,320]{1,0:T(8,128)(2,1)S(1)} %get-tuple-element.14.q_own_in), channel_id=1, source_target_pairs={{0,16},{16,0},{32,48},{48,32},{64,80},{80,64},{96,112},{112,96},{1... | collective-permute-start | bytes 245768 | tf_op jit(solution)/shard_map/ppermute | solution.py:480
  55.0 0.9 collective-permute-done.q_other_in
  56.0 0.0 collective-permute-done.1.refs_0_
  56.0 0.0 collective-permute-done.2.refs_1_
  56.0 0.0 collective-permute-done.3.refs_3_
  56.0 2.2 %all-to-all-done.1.keys = bf16[16,432,128]{2,1,0:T(8,128)(2,1)S(1)} async-done(((bf16[16,432,128]{2,1,0:T(8,128)(2,1)}), bf16[16,432,128]{2,1,0:T(8,128)(2,1)S(1)}, u32[]{:S(2)}, u32[]{:S(2)}) %all-to-all-start.1) | async-done | bytes 1769504 | tf_op jit(solution)/shard_map/all_to_all | solution.py:419
  58.2 5.0 %shard_map.175 = (f32[128,256]{1,0:T(8,128)S(1)}, f32[128,256]{1,0:T(8,128)S(1)}) custom-call(bf16[16,432,128]{2,1,0:T(8,128)(2,1)S(1)} %all-to-all-done.1.keys, bf16[128,320]{1,0:T(8,128)(2,1)} %copy-done.4, bf16[128,320]{1,0:T(8,128)(2,1)} %copy-done.10, bf16[512,384]{1,0:T(8,128)(2,1)} %copy-done.1, bf16[128,640]{1,0:T(8,128)(2,1)} %copy-done.7, ...), custom_call_target="tpu_custom_call" | custom-call | tf_op jit(solution)/shard_map/pallas_call | solution.py:408
  63.2 0.0 copy-start.14
  63.3 0.0 copy-start.5
  63.3 8.8 %collective-permute-start.4 = (f32[128,256]{1,0:T(8,128)S(1)}, f32[128,256]{1,0:T(8,128)S(1)}, u32[]{:S(2)}, u32[]{:S(2)}) collective-permute-start(f32[128,256]{1,0:T(8,128)S(1)} %get-tuple-element.18), channel_id=1, source_target_pairs={{0,16},{16,0},{32,48},{48,32},{64,80},{80,64},{96,112},{112,96},{1... | collective-permute-start | bytes 393224 | tf_op jit(solution)/shard_map/ppermute | solution.py:499
  72.1 1.0 collective-permute-done.4.b
  73.0 1.4 shard_map.176
  74.4 3.6 %all-to-all-start.2 = ((bf16[16,128,128]{2,1,0:T(8,128)(2,1)}), bf16[16,128,128]{2,1,0:T(8,128)(2,1)S(1)}, u32[]{:S(2)}, u32[]{:S(2)}) async-start(bf16[16,128,128]{2,1,0:T(8,128)(2,1)} %shard_map.176), calls=%async_computation.2 | async-start | bytes 1048576 | tf_op jit(solution)/shard_map/all_to_all | solution.py:419
  78.0 0.1 copy.22.ids
  78.1 10.8 %all-to-all-done.2.parts = bf16[16,128,128]{2,1,0:T(8,128)(2,1)S(1)} async-done(((bf16[16,128,128]{2,1,0:T(8,128)(2,1)}), bf16[16,128,128]{2,1,0:T(8,128)(2,1)S(1)}, u32[]{:S(2)}, u32[]{:S(2)}) %all-to-all-start.2) | async-done | bytes 524320 | tf_op jit(solution)/shard_map/all_to_all | solution.py:419
  88.9 1.3 shard_map.177
  90.2 10.0 %all-to-all-start.3 = ((bf16[32,16,128]{2,1,0:T(8,128)(2,1)}), bf16[32,16,128]{2,1,0:T(8,128)(2,1)S(1)}, u32[]{:S(2)}, u32[]{:S(2)}) async-start(bf16[32,16,128]{2,1,0:T(8,128)(2,1)} %bitcast.1), calls=%async_computation.3 | async-start | bytes 262144 | tf_op jit(solution)/shard_map/all_to_all | solution.py:419
  100.2 3.2 %shard_map.178 = (bf16[6144,128]{1,0:T(8,128)(2,1)}, bf16[6144,128]{1,0:T(8,128)(2,1)S(1)}) custom-call(bf16[1,2048,256]{2,1,0:T(8,128)(2,1)} %gate_a.1, bf16[1,2048,256]{2,1,0:T(8,128)(2,1)} %up_a.1, bf16[1,256,2048]{2,1,0:T(8,128)(2,1)} %down_a.1), custom_call_target="tpu_custom_call" | custom-call | tf_op jit(solution)/shard_map/pallas_call | solution.py:408
  103.4 1.9 collective-permute-start.5
  105.4 4.6 %collective-permute-start.6 = (bf16[6144,128]{1,0:T(8,128)(2,1)S(1)}, bf16[6144,128]{1,0:T(8,128)(2,1)}, u32[]{:S(2)}, u32[]{:S(2)}) collective-permute-start(bf16[6144,128]{1,0:T(8,128)(2,1)S(1)} %get-tuple-element.21), channel_id=1, source_target_pairs={{0,3},{1,0},{2,1},{3,2},{4,7},{5,4},{6,5},{7,6},{8,11},{9,8},{10,9... | collective-permute-start | bytes 4718600 | tf_op jit(solution)/shard_map/ppermute | solution.py:483
  110.0 6.1 %all-to-all-done.3 = bf16[32,16,128]{2,1,0:T(8,128)(2,1)S(1)} async-done(((bf16[32,16,128]{2,1,0:T(8,128)(2,1)}), bf16[32,16,128]{2,1,0:T(8,128)(2,1)S(1)}, u32[]{:S(2)}, u32[]{:S(2)}) %all-to-all-start.3) | async-done | bytes 131104 | tf_op jit(solution)/shard_map/all_to_all | solution.py:419
  116.1 1.1 broadcast_select_fusion
  117.2 3.7 %all-to-all-start.4 = ((bf16[16,256,128]{2,1,0:T(8,128)(2,1)}), bf16[16,256,128]{2,1,0:T(8,128)(2,1)S(1)}, u32[]{:S(2)}, u32[]{:S(2)}) async-start(bf16[16,256,128]{2,1,0:T(8,128)(2,1)} %broadcast_select_fusion), calls=%async_computation.4 | async-start | bytes 2097152 | tf_op jit(solution)/shard_map/all_to_all | solution.py:419
  120.9 0.0 copy-start.6
  120.9 6.5 %collective-permute-done.5.low = bf16[6144,128]{1,0:T(8,128)(2,1)} collective-permute-done((bf16[6144,128]{1,0:T(8,128)(2,1)}, bf16[6144,128]{1,0:T(8,128)(2,1)}, u32[]{:S(2)}, u32[]{:S(2)}) %collective-permute-start.5) | collective-permute-done | bytes 1572896 | tf_op jit(solution)/shard_map/ppermute | solution.py:482
  127.4 10.4 %collective-permute-done.6.high = bf16[6144,128]{1,0:T(8,128)(2,1)} collective-permute-done((bf16[6144,128]{1,0:T(8,128)(2,1)S(1)}, bf16[6144,128]{1,0:T(8,128)(2,1)}, u32[]{:S(2)}, u32[]{:S(2)}) %collective-permute-start.6) | collective-permute-done | bytes 1572896 | tf_op jit(solution)/shard_map/ppermute | solution.py:483
  137.8 1.5 shard_map.179.gate_w
  139.4 4.0 %shard_map.180 = bf16[16,256,128]{2,1,0:T(8,128)(2,1)S(1)} custom-call(bf16[16,256,128]{2,1,0:T(8,128)(2,1)S(1)} %all-to-all-done.4.got, f32[1,2048]{1,0:T(1,128)S(1)} %bitcast.8, bf16[2048,512]{1,0:T(8,128)(2,1)S(1)} %shard_map.179.gate_w, bf16[1,2048,256]{2,1,0:T(8,128)(2,1)} %up_a.1, bf16[1,256,2048]{2,1,0:T(8,128)(2,1)} %down_a.1, ...), custom_call_target="tpu_custom_call" | custom-call | tf_op jit(solution)/shard_map/pallas_call | solution.py:408
  143.4 0.0 copy-start.15
  143.4 18.4 %all_to_all.36.parts = bf16[16,256,128]{2,1,0:T(8,128)(2,1)S(1)} all-to-all(bf16[16,256,128]{2,1,0:T(8,128)(2,1)S(1)} %shard_map.180), channel_id=1, replica_groups=mesh['sp'=32,'tp'=16] {'tp'}, dimensions={0} | all-to-all | bytes 2097152 | tf_op jit(solution)/shard_map/all_to_all | solution.py:419
  161.8 0.8 shard_map.181
  162.6 16.0 %all-to-all-start.6 = ((bf16[32,16,128]{2,1,0:T(8,128)(2,1)}), bf16[32,16,128]{2,1,0:T(8,128)(2,1)S(1)}, u32[]{:S(2)}, u32[]{:S(2)}) async-start(bf16[32,16,128]{2,1,0:T(8,128)(2,1)} %bitcast.5), calls=%async_computation.6 | async-start | bytes 262144 | tf_op jit(solution)/shard_map/all_to_all | solution.py:419
  178.6 0.1 copy.24.weights
  178.7 15.7 %all-to-all-done.6 = bf16[32,16,128]{2,1,0:T(8,128)(2,1)S(1)} async-done(((bf16[32,16,128]{2,1,0:T(8,128)(2,1)}), bf16[32,16,128]{2,1,0:T(8,128)(2,1)S(1)}, u32[]{:S(2)}, u32[]{:S(2)}) %all-to-all-start.6) | async-done | bytes 131104 | tf_op jit(solution)/shard_map/all_to_all | solution.py:419
  194.4 1.2 shard_map.182
  (30 shorter events, 0.1 us)
Async XLA Ops:
  30.5 6.9 %copy-start.11 = (bf16[512,64]{0,1:T(8,128)(2,1)S(1)}, bf16[512,64]{0,1:T(8,128)(2,1)}, u32[]{:S(2)}) copy-start(bf16[512,64]{0,1:T(8,128)(2,1)} %param.24) | copy-start | bytes 196612
  30.5 7.0 %copy-start.12 = (bf16[512,64]{0,1:T(8,128)(2,1)S(1)}, bf16[512,64]{0,1:T(8,128)(2,1)}, u32[]{:S(2)}) copy-start(bf16[512,64]{0,1:T(8,128)(2,1)} %param.25) | copy-start | bytes 196612
  30.5 7.2 %copy-start.13 = (bf16[128,192]{0,1:T(8,128)(2,1)S(1)}, bf16[128,192]{0,1:T(8,128)(2,1)}, u32[]{:S(2)}) copy-start(bf16[128,192]{0,1:T(8,128)(2,1)} %param.18) | copy-start | bytes 147460
  30.5 27.7 %all-to-all-start.1 = ((bf16[16,432,128]{2,1,0:T(8,128)(2,1)}), bf16[16,432,128]{2,1,0:T(8,128)(2,1)S(1)}, u32[]{:S(2)}, u32[]{:S(2)}) async-start(bf16[16,432,128]{2,1,0:T(8,128)(2,1)} %broadcast_in_dim.33), calls=%async_computation.1 | async-start | bytes 3538944 | tf_op jit(solution)/shard_map/all_to_all | solution.py:419
  39.4 0.7 copy-start.1
  40.2 18.0 %copy-start.3 = (bf16[128,640]{1,0:T(8,128)(2,1)}, bf16[128,640]{1,0:T(8,128)(2,1)S(1)}, u32[]{:S(2)}) copy-start(bf16[128,640]{1,0:T(8,128)(2,1)S(1)} %get-tuple-element.16.refs_2_) | copy-start | bytes 491524
  40.2 18.0 %copy-start.4 = (bf16[128,320]{1,0:T(8,128)(2,1)}, bf16[128,320]{1,0:T(8,128)(2,1)S(1)}, u32[]{:S(2)}) copy-start(bf16[128,320]{1,0:T(8,128)(2,1)S(1)} %get-tuple-element.14.q_own_in) | copy-start | bytes 245764
  40.2 32.9 %copy-start = (bf16[128,2048]{1,0:T(8,128)(2,1)S(1)}, bf16[128,2048]{1,0:T(8,128)(2,1)}, u32[]{:S(2)}) copy-start(bf16[128,2048]{1,0:T(8,128)(2,1)} %out_maj.1) | copy-start | bytes 1572868
  40.2 32.9 %copy-start.2 = (bf16[64,2048]{1,0:T(8,128)(2,1)S(1)}, bf16[64,2048]{1,0:T(8,128)(2,1)}, u32[]{:S(2)}) copy-start(bf16[64,2048]{1,0:T(8,128)(2,1)} %out_min.1) | copy-start | bytes 786436
  40.2 15.8 %collective-permute-start.1 = (bf16[128,640]{1,0:T(8,128)(2,1)S(1)}, bf16[128,640]{1,0:T(8,128)(2,1)S(1)}, u32[]{:S(2)}, u32[]{:S(2)}) collective-permute-start(bf16[128,640]{1,0:T(8,128)(2,1)S(1)} %get-tuple-element.16.refs_2_), channel_id=1, source_target_pairs={{0,64},{16,80},{32,96},{48,112},{64,128},{80,144},{96,160},{112,17... | collective-permute-start | bytes 491528 | tf_op jit(solution)/shard_map/ppermute | solution.py:481
  45.3 10.7 %collective-permute-start.2 = (bf16[128,640]{1,0:T(8,128)(2,1)S(1)}, bf16[128,640]{1,0:T(8,128)(2,1)S(1)}, u32[]{:S(2)}, u32[]{:S(2)}) collective-permute-start(bf16[128,640]{1,0:T(8,128)(2,1)S(1)} %get-tuple-element.16.refs_2_), channel_id=1, source_target_pairs={{0,32},{16,48},{32,64},{48,80},{64,96},{80,112},{96,128},{112,144}... | collective-permute-start | bytes 491528 | tf_op jit(solution)/shard_map/ppermute | solution.py:481
  49.2 6.7 %collective-permute-start.3 = (bf16[128,640]{1,0:T(8,128)(2,1)S(1)}, bf16[128,640]{1,0:T(8,128)(2,1)S(1)}, u32[]{:S(2)}, u32[]{:S(2)}) collective-permute-start(bf16[128,640]{1,0:T(8,128)(2,1)S(1)} %get-tuple-element.16.refs_2_), channel_id=1, source_target_pairs={{0,480},{16,496},{1,481},{17,497},{2,482},{18,498},{3,483},{19,499... | collective-permute-start | bytes 491528 | tf_op jit(solution)/shard_map/ppermute | solution.py:481
  50.5 5.4 %collective-permute-start = (bf16[128,320]{1,0:T(8,128)(2,1)S(1)}, bf16[128,320]{1,0:T(8,128)(2,1)S(1)}, u32[]{:S(2)}, u32[]{:S(2)}) collective-permute-start(bf16[128,320]{1,0:T(8,128)(2,1)S(1)} %get-tuple-element.14.q_own_in), channel_id=1, source_target_pairs={{0,16},{16,0},{32,48},{48,32},{64,80},{80,64},{96,112},{112,96},{1... | collective-permute-start | bytes 245768 | tf_op jit(solution)/shard_map/ppermute | solution.py:480
  56.0 2.3 %copy-start.10 = (bf16[128,320]{1,0:T(8,128)(2,1)}, bf16[128,320]{1,0:T(8,128)(2,1)S(1)}, u32[]{:S(2)}) copy-start(bf16[128,320]{1,0:T(8,128)(2,1)S(1)} %collective-permute-done.q_other_in) | copy-start | bytes 245764
  56.0 2.3 %copy-start.7 = (bf16[128,640]{1,0:T(8,128)(2,1)}, bf16[128,640]{1,0:T(8,128)(2,1)S(1)}, u32[]{:S(2)}) copy-start(bf16[128,640]{1,0:T(8,128)(2,1)S(1)} %collective-permute-done.1.refs_0_) | copy-start | bytes 491524
  56.0 2.3 %copy-start.8 = (bf16[128,640]{1,0:T(8,128)(2,1)}, bf16[128,640]{1,0:T(8,128)(2,1)S(1)}, u32[]{:S(2)}) copy-start(bf16[128,640]{1,0:T(8,128)(2,1)S(1)} %collective-permute-done.2.refs_1_) | copy-start | bytes 491524
  56.0 2.3 %copy-start.9 = (bf16[128,640]{1,0:T(8,128)(2,1)}, bf16[128,640]{1,0:T(8,128)(2,1)S(1)}, u32[]{:S(2)}) copy-start(bf16[128,640]{1,0:T(8,128)(2,1)S(1)} %collective-permute-done.3.refs_3_) | copy-start | bytes 491524
  63.2 14.7 %copy-start.14 = (s32[128,2]{0,1:T(2,128)S(1)}, s32[128,2]{0,1:T(2,128)}, u32[]{:S(2)}) copy-start(s32[128,2]{0,1:T(2,128)} %param.30) | copy-start | bytes 3076
  63.3 25.7 %copy-start.5 = (bf16[128,128]{1,0:T(8,128)(2,1)S(1)}, bf16[128,128]{1,0:T(8,128)(2,1)}, u32[]{:S(2)}) copy-start(bf16[128,128]{1,0:T(8,128)(2,1)} %residual.1) | copy-start | bytes 98308
  63.3 9.8 %collective-permute-start.4 = (f32[128,256]{1,0:T(8,128)S(1)}, f32[128,256]{1,0:T(8,128)S(1)}, u32[]{:S(2)}, u32[]{:S(2)}) collective-permute-start(f32[128,256]{1,0:T(8,128)S(1)} %get-tuple-element.18), channel_id=1, source_target_pairs={{0,16},{16,0},{32,48},{48,32},{64,80},{80,64},{96,112},{112,96},{1... | collective-permute-start | bytes 393224 | tf_op jit(solution)/shard_map/ppermute | solution.py:499
  74.4 14.5 %all-to-all-start.2 = ((bf16[16,128,128]{2,1,0:T(8,128)(2,1)}), bf16[16,128,128]{2,1,0:T(8,128)(2,1)S(1)}, u32[]{:S(2)}, u32[]{:S(2)}) async-start(bf16[16,128,128]{2,1,0:T(8,128)(2,1)} %shard_map.176), calls=%async_computation.2 | async-start | bytes 1048576 | tf_op jit(solution)/shard_map/all_to_all | solution.py:419
  90.2 25.8 %all-to-all-start.3 = ((bf16[32,16,128]{2,1,0:T(8,128)(2,1)}), bf16[32,16,128]{2,1,0:T(8,128)(2,1)S(1)}, u32[]{:S(2)}, u32[]{:S(2)}) async-start(bf16[32,16,128]{2,1,0:T(8,128)(2,1)} %bitcast.1), calls=%async_computation.3 | async-start | bytes 262144 | tf_op jit(solution)/shard_map/all_to_all | solution.py:419
  103.4 23.9 %collective-permute-start.5 = (bf16[6144,128]{1,0:T(8,128)(2,1)}, bf16[6144,128]{1,0:T(8,128)(2,1)}, u32[]{:S(2)}, u32[]{:S(2)}) collective-permute-start(bf16[6144,128]{1,0:T(8,128)(2,1)} %get-tuple-element.20), channel_id=1, source_target_pairs={{0,1},{1,2},{2,3},{3,0},{4,5},{5,6},{6,7},{7,4},{8,9},{9,10},{10,1... | collective-permute-start | bytes 4718600 | tf_op jit(solution)/shard_map/ppermute | solution.py:482
  105.4 32.5 %collective-permute-start.6 = (bf16[6144,128]{1,0:T(8,128)(2,1)S(1)}, bf16[6144,128]{1,0:T(8,128)(2,1)}, u32[]{:S(2)}, u32[]{:S(2)}) collective-permute-start(bf16[6144,128]{1,0:T(8,128)(2,1)S(1)} %get-tuple-element.21), channel_id=1, source_target_pairs={{0,3},{1,0},{2,1},{3,2},{4,7},{5,4},{6,5},{7,6},{8,11},{9,8},{10,9... | collective-permute-start | bytes 4718600 | tf_op jit(solution)/shard_map/ppermute | solution.py:483
  117.2 22.1 %all-to-all-start.4 = ((bf16[16,256,128]{2,1,0:T(8,128)(2,1)}), bf16[16,256,128]{2,1,0:T(8,128)(2,1)S(1)}, u32[]{:S(2)}, u32[]{:S(2)}) async-start(bf16[16,256,128]{2,1,0:T(8,128)(2,1)} %broadcast_select_fusion), calls=%async_computation.4 | async-start | bytes 2097152 | tf_op jit(solution)/shard_map/all_to_all | solution.py:419
  120.9 18.5 %copy-start.6 = (f32[2048]{0:T(1024)S(1)}, f32[2048]{0:T(1024)}, u32[]{:S(2)}) copy-start(f32[2048]{0:T(1024)} %param.29) | copy-start | bytes 24580
  143.4 35.2 %copy-start.15 = (f32[128,2]{0,1:T(2,128)S(1)}, f32[128,2]{0,1:T(2,128)}, u32[]{:S(2)}) copy-start(f32[128,2]{0,1:T(2,128)} %param.31) | copy-start | bytes 3076
  162.6 31.8 %all-to-all-start.6 = ((bf16[32,16,128]{2,1,0:T(8,128)(2,1)}), bf16[32,16,128]{2,1,0:T(8,128)(2,1)S(1)}, u32[]{:S(2)}, u32[]{:S(2)}) async-start(bf16[32,16,128]{2,1,0:T(8,128)(2,1)} %bitcast.5), calls=%async_computation.6 | async-start | bytes 262144 | tf_op jit(solution)/shard_map/all_to_all | solution.py:419

commit v8 on v7

--- a/solution.py
+++ b/solution.py
@@ -25,7 +25,7 @@
 MASKED = -1e30
 NORM_EPS = 1e-6
 HALF = SLOTS // 2
-NEAR = (-2, -1, 0, 1)
+NEAR = (-2, -1, 0, 1, 2, 3)
 FAR = N_Z - len(NEAR)
 FAR_ROWS = FAR * ROWS
 PACKED = 4 * FAR_ROWS + FAR_ROWS // 2
@@ -60,7 +60,7 @@
 
 
 HALF = SLOTS // 2
-NEAR = (-2, -1, 0, 1)
+NEAR = (-2, -1, 0, 1, 2, 3)
 FAR = N_Z - len(NEAR)
 FAR_ROWS = FAR * ROWS
 PACKED = 4 * FAR_ROWS + FAR_ROWS // 2
@@ -176,7 +176,7 @@
     out[4 * FAR_ROWS :, :] = jnp.concatenate([rope[: FAR_ROWS // 2], rope[FAR_ROWS // 2 :]], axis=1)
 
 
-PER = 4
+PER = 8
 CHUNK = PER * FAR_ROWS
 N_CHUNK = N_TP // PER
 
@@ -336,7 +336,7 @@
         c.wait()
 
 
-def expert_body(got, gain, gate_w, up_a, down_a, low, high, parts, up_w, down_w, x, sems):
+def expert_body(got, gain, gate_w, up_a, down_a, low, high, out, up_w, down_w, x, parts, sems, out_sems):
     own = pl.ds(0, 256)
     pairs = [(up_a.at[0], up_w.at[:, own])]
     for i, packed in enumerate((low, high)):
@@ -366,10 +366,16 @@
     hidden = (gate / (1.0 + jnp.exp(-gate)) * up).astype(BF16)
     for c in copies[3:]:
         c.wait()
-    for t in range(0, N_TP, 2):
-        value = dot(hidden, down_w[:, 128 * t : 128 * (t + 2)])
-        parts[t] = value[:, :128].astype(BF16)
-        parts[t + 1] = value[:, 128:].astype(BF16)
+    leaving = []
+    for t in range(0, N_TP, 4):
+        value = dot(hidden, down_w[:, 128 * t : 128 * (t + 4)])
+        for k in range(4):
+            parts[t + k] = value[:, 128 * k : 128 * (k + 1)].astype(BF16)
+        group = pl.ds(t, 4)
+        leaving.append(pltpu.make_async_copy(parts.at[group], out.at[group], out_sems.at[t // 4]))
+        leaving[-1].start()
+    for c in leaving:
+        c.wait()
 
 
 def gather_sum_body(parts, out):
@@ -401,7 +407,7 @@
     return pltpu.VMEM(dims, kind)
 
 
-def kernel(body, outs, rooms, sems, operands, near=()):
+def kernel(body, outs, rooms, sems, operands, near=(), out_spec=None):
     single = not isinstance(outs, tuple)
     places = [pltpu.VMEM if i in near else pltpu.HBM for i in range(len(operands))]
     operands = [pltpu.with_memory_space_constraint(x, m) for x, m in zip(operands, places)]
@@ -409,8 +415,8 @@
         body,
         out_shape=outs,
         in_specs=[pl.BlockSpec(memory_space=m) for m in places],
-        out_specs=vmem(1)[0] if single else tuple(vmem(len(outs))),
-        scratch_shapes=rooms + ([pltpu.SemaphoreType.DMA((sems,))] if sems else []),
+        out_specs=(out_spec or vmem(1)[0]) if single else tuple(vmem(len(outs))),
+        scratch_shapes=rooms + [pltpu.SemaphoreType.DMA((n,)) for n in np.atleast_1d(sems).tolist() if n],
         compiler_params=pltpu.CompilerParams(vmem_limit_bytes=24 * 2**20),
     )(*operands)
 
@@ -522,11 +528,12 @@
     gate_w = kernel(assemble_body, shape((D, 512)), [], 3, (gate_proj, from_low, from_high))
     down_parts = kernel(
         expert_body,
-        shape((N_TP, HALF, 128)),
-        [room((D, 512)), room((512, D)), room((HALF, D))],
-        4 + 2 * N_TP,
+        jax.ShapeDtypeStruct((N_TP, HALF, 128), BF16),
+        [room((D, 512)), room((512, D)), room((HALF, D)), room((N_TP, HALF, 128))],
+        (4 + 2 * N_TP, N_TP // 4),
         (everyone, norm_gain.reshape(1, D), gate_w, up_proj, down_proj, from_low, from_high),
         (0, 1, 2),
+        ANY,
     )
     down_parts = to_each(down_parts, "tp")
     expert_out = kernel(gather_sum_body, shape((SLOTS, 128)), [], 0, (down_parts,), (0,))

time: 197 us -> 211 us (1.071)
  waiting for transfers between devices: 53.7 us -> 66.8 us
    ppermute x3 -> x5, waiting for transfers between devices: 0.01 us -> 16.5 us  [per_device(): lax.ppermute(own_block, 'sp', along_z(-step))]
    ppermute x1, starting transfers between devices: 8.79 us -> 3.06 us  [per_device(): from_other = lax.ppermute(other, 'sp', OTHER_CORE)]
    all_to_all x5, waiting for transfers between devices: 34.8 us -> 32.5 us  [to_each(): lax.all_to_all(array, axis, 0, 0, tiled=True, axis_index_groups=groups)]
    ppermute x1, starting transfers between devices: 4.48 us -> 6.67 us  [per_device(): q_other = lax.ppermute(q_own, 'sp', OTHER_CORE)]
    ppermute x3 -> x5, starting transfers between devices: 10.3 us -> 11.8 us  [per_device(): lax.ppermute(own_block, 'sp', along_z(-step))]
  transfers between devices with their start and end apart: 12 -> 14, of which waited for: 8 -> 9; matrix products, arithmetic and copies ran while one was open for 1% -> 1% of each run, Pallas kernels for 3% -> 3%
where the time goes in v8:
time: 211 us; the launch traced here: 210 us
  starting transfers between devices  70.1 us (33%)
  waiting for transfers between devices  66.8 us (32%)
  blocking collectives  46.1 us (22%)
  Pallas kernels  21.6 us (10%)
  local copies, waits for them, and re-layouts  3.32 us (2%)
    all_to_all x2, blocking collectives, to_each(): lax.all_to_all(array, axis, 0, 0, tiled=True, axis_index_groups=groups)  46.1 us
    all_to_all x5, starting transfers between devices, to_each(): lax.all_to_all(array, axis, 0, 0, tiled=True, axis_index_groups=groups)  42.1 us
    all_to_all x5, waiting for transfers between devices, to_each(): lax.all_to_all(array, axis, 0, 0, tiled=True, axis_index_groups=groups)  32.5 us
    pallas_call x11, Pallas kernels, kernel(): pl.pallas_call(body, out_shape=outs, in_specs=[pl.BlockSpec(memory_space=...  21.6 us
    ppermute x5, waiting for transfers between devices, per_device(): lax.ppermute(own_block, 'sp', along_z(-step))  16.5 us
    ppermute x5, starting transfers between devices, per_device(): lax.ppermute(own_block, 'sp', along_z(-step))  11.8 us
    ppermute x1, waiting for transfers between devices, per_device(): from_high = lax.ppermute(high, ('sp', 'tp'), ring(-1))  10.5 us
    ppermute x1, starting transfers between devices, per_device(): q_other = lax.ppermute(q_own, 'sp', OTHER_CORE)  6.67 us
  transfers between devices with their start and end apart: 14, of which 9 were waited for; matrix products, arithmetic and copies ran while one was open for 1% of the time, Pallas kernels for 3%

profile of v8, /device:TPU:1, one launch (start us, length us, event | category | flops | bytes accessed | tf_op | source)
XLA Modules:
  0.0 209.6 jit_solution(13686209999428315571)
XLA Ops:
  0.0 1.2 shard_map.172
  1.2 27.7 %all_to_all.35.got = bf16[16,8,640]{2,1,0:T(8,128)(2,1)S(1)} all-to-all(bf16[16,8,640]{2,1,0:T(8,128)(2,1)S(1)} %shard_map.172), channel_id=1, replica_groups={{0,32,64,96,128,160,192,224,256,288,320,352,384,416,448,480},{16,48,80,..., dimensions={0} | all-to-all | bytes 327680 | tf_op jit(solution)/shard_map/all_to_all | solution.py:425
  28.9 0.1 shard_map.173
  29.0 1.3 broadcast_in_dim.33
  30.4 6.9 %all-to-all-start.1 = ((bf16[16,360,128]{2,1,0:T(8,128)(2,1)}), bf16[16,360,128]{2,1,0:T(8,128)(2,1)S(1)}, u32[]{:S(2)}, u32[]{:S(2)}) async-start(bf16[16,360,128]{2,1,0:T(8,128)(2,1)} %broadcast_in_dim.33), calls=%async_computation.1 | async-start | bytes 2949120 | tf_op jit(solution)/shard_map/all_to_all | solution.py:425
  37.3 0.1 copy.20.ku_min
  37.4 0.1 copy.21.vu_min
  37.5 0.1 copy.19.maj
  37.6 1.6 shard_map.174
  39.3 0.7 copy-done.1
  40.0 6.7 %collective-permute-start = (bf16[128,320]{1,0:T(8,128)(2,1)S(1)}, bf16[128,320]{1,0:T(8,128)(2,1)S(1)}, u32[]{:S(2)}, u32[]{:S(2)}) collective-permute-start(bf16[128,320]{1,0:T(8,128)(2,1)S(1)} %get-tuple-element.14.q_own_in), channel_id=1, source_target_pairs={{0,16},{16,0},{32,48},{48,32},{64,80},{80,64},{96,112},{112,96},{1... | collective-permute-start | bytes 245768 | tf_op jit(solution)/shard_map/ppermute | solution.py:486
  46.7 3.8 %collective-permute-start.1 = (bf16[128,640]{1,0:T(8,128)(2,1)S(1)}, bf16[128,640]{1,0:T(8,128)(2,1)S(1)}, u32[]{:S(2)}, u32[]{:S(2)}) collective-permute-start(bf16[128,640]{1,0:T(8,128)(2,1)S(1)} %get-tuple-element.16.refs_2_), channel_id=1, source_target_pairs={{0,64},{16,80},{32,96},{48,112},{64,128},{80,144},{96,160},{112,17... | collective-permute-start | bytes 491528 | tf_op jit(solution)/shard_map/ppermute | solution.py:487
  50.5 2.5 %collective-permute-start.2 = (bf16[128,640]{1,0:T(8,128)(2,1)S(1)}, bf16[128,640]{1,0:T(8,128)(2,1)S(1)}, u32[]{:S(2)}, u32[]{:S(2)}) collective-permute-start(bf16[128,640]{1,0:T(8,128)(2,1)S(1)} %get-tuple-element.16.refs_2_), channel_id=1, source_target_pairs={{0,32},{16,48},{32,64},{48,80},{64,96},{80,112},{96,128},{112,144}... | collective-permute-start | bytes 491528 | tf_op jit(solution)/shard_map/ppermute | solution.py:487
  53.0 1.3 collective-permute-start.3
  54.3 2.0 collective-permute-start.4
  56.4 2.2 %collective-permute-start.5 = (bf16[128,640]{1,0:T(8,128)(2,1)S(1)}, bf16[128,640]{1,0:T(8,128)(2,1)S(1)}, u32[]{:S(2)}, u32[]{:S(2)}) collective-permute-start(bf16[128,640]{1,0:T(8,128)(2,1)S(1)} %get-tuple-element.16.refs_2_), channel_id=1, source_target_pairs={{0,416},{16,432},{32,448},{48,464},{64,480},{80,496},{1,417},{17,4... | collective-permute-start | bytes 491528 | tf_op jit(solution)/shard_map/ppermute | solution.py:487
  58.6 9.3 %collective-permute-done.3.refs_3_ = bf16[128,640]{1,0:T(8,128)(2,1)S(1)} collective-permute-done((bf16[128,640]{1,0:T(8,128)(2,1)S(1)}, bf16[128,640]{1,0:T(8,128)(2,1)S(1)}, u32[]{:S(2)}, u32[]{:S(2)}) %collective-permute-start.3) | collective-permute-done | bytes 163872 | tf_op jit(solution)/shard_map/ppermute | solution.py:487
  68.0 3.7 %collective-permute-done.4.refs_4_ = bf16[128,640]{1,0:T(8,128)(2,1)S(1)} collective-permute-done((bf16[128,640]{1,0:T(8,128)(2,1)S(1)}, bf16[128,640]{1,0:T(8,128)(2,1)S(1)}, u32[]{:S(2)}, u32[]{:S(2)}) %collective-permute-start.4) | collective-permute-done | bytes 163872 | tf_op jit(solution)/shard_map/ppermute | solution.py:487
  71.6 3.5 %collective-permute-done.5.refs_5_ = bf16[128,640]{1,0:T(8,128)(2,1)S(1)} collective-permute-done((bf16[128,640]{1,0:T(8,128)(2,1)S(1)}, bf16[128,640]{1,0:T(8,128)(2,1)S(1)}, u32[]{:S(2)}, u32[]{:S(2)}) %collective-permute-start.5) | collective-permute-done | bytes 163872 | tf_op jit(solution)/shard_map/ppermute | solution.py:487
  75.2 0.6 copy-done.11
  75.8 4.6 %shard_map.175 = (f32[128,256]{1,0:T(8,128)S(1)}, f32[128,256]{1,0:T(8,128)S(1)}) custom-call(bf16[16,360,128]{2,1,0:T(8,128)(2,1)S(1)} %all-to-all-done.1.keys, bf16[128,320]{1,0:T(8,128)(2,1)} %copy-done.4, bf16[128,320]{1,0:T(8,128)(2,1)} %copy-done.12, bf16[512,384]{1,0:T(8,128)(2,1)} %copy-done.1, bf16[128,640]{1,0:T(8,128)(2,1)} %copy-done.7, ...), custom_call_target="tpu_custom_call" | custom-call | tf_op jit(solution)/shard_map/pallas_call | solution.py:414
  80.4 0.0 copy-start.16
  80.4 0.0 copy-start.5
  80.4 3.1 %collective-permute-start.6 = (f32[128,256]{1,0:T(8,128)S(1)}, f32[128,256]{1,0:T(8,128)S(1)}, u32[]{:S(2)}, u32[]{:S(2)}) collective-permute-start(f32[128,256]{1,0:T(8,128)S(1)} %get-tuple-element.18), channel_id=1, source_target_pairs={{0,16},{16,0},{32,48},{48,32},{64,80},{80,64},{96,112},{112,96},{1... | collective-permute-start | bytes 393224 | tf_op jit(solution)/shard_map/ppermute | solution.py:505
  83.5 1.0 collective-permute-done.6.b
  84.5 1.4 shard_map.176
  85.8 6.9 %all-to-all-start.2 = ((bf16[16,128,128]{2,1,0:T(8,128)(2,1)}), bf16[16,128,128]{2,1,0:T(8,128)(2,1)S(1)}, u32[]{:S(2)}, u32[]{:S(2)}) async-start(bf16[16,128,128]{2,1,0:T(8,128)(2,1)} %shard_map.176), calls=%async_computation.2 | async-start | bytes 1048576 | tf_op jit(solution)/shard_map/all_to_all | solution.py:425
  92.8 0.1 copy.22.ids
  92.9 10.6 %all-to-all-done.2.parts = bf16[16,128,128]{2,1,0:T(8,128)(2,1)S(1)} async-done(((bf16[16,128,128]{2,1,0:T(8,128)(2,1)}), bf16[16,128,128]{2,1,0:T(8,128)(2,1)S(1)}, u32[]{:S(2)}, u32[]{:S(2)}) %all-to-all-start.2) | async-done | bytes 524320 | tf_op jit(solution)/shard_map/all_to_all | solution.py:425
  103.5 1.3 shard_map.177
  104.8 8.7 %all-to-all-start.3 = ((bf16[32,16,128]{2,1,0:T(8,128)(2,1)}), bf16[32,16,128]{2,1,0:T(8,128)(2,1)S(1)}, u32[]{:S(2)}, u32[]{:S(2)}) async-start(bf16[32,16,128]{2,1,0:T(8,128)(2,1)} %bitcast.1), calls=%async_computation.3 | async-start | bytes 262144 | tf_op jit(solution)/shard_map/all_to_all | solution.py:425
  113.5 3.2 %shard_map.178 = (bf16[6144,128]{1,0:T(8,128)(2,1)}, bf16[6144,128]{1,0:T(8,128)(2,1)S(1)}) custom-call(bf16[1,2048,256]{2,1,0:T(8,128)(2,1)} %gate_a.1, bf16[1,2048,256]{2,1,0:T(8,128)(2,1)} %up_a.1, bf16[1,256,2048]{2,1,0:T(8,128)(2,1)} %down_a.1), custom_call_target="tpu_custom_call" | custom-call | tf_op jit(solution)/shard_map/pallas_call | solution.py:414
  116.7 1.9 collective-permute-start.7
  118.6 4.6 %collective-permute-start.8 = (bf16[6144,128]{1,0:T(8,128)(2,1)S(1)}, bf16[6144,128]{1,0:T(8,128)(2,1)}, u32[]{:S(2)}, u32[]{:S(2)}) collective-permute-start(bf16[6144,128]{1,0:T(8,128)(2,1)S(1)} %get-tuple-element.21), channel_id=1, source_target_pairs={{0,3},{1,0},{2,1},{3,2},{4,7},{5,4},{6,5},{7,6},{8,11},{9,8},{10,9... | collective-permute-start | bytes 4718600 | tf_op jit(solution)/shard_map/ppermute | solution.py:489
  123.2 6.1 %all-to-all-done.3 = bf16[32,16,128]{2,1,0:T(8,128)(2,1)S(1)} async-done(((bf16[32,16,128]{2,1,0:T(8,128)(2,1)}), bf16[32,16,128]{2,1,0:T(8,128)(2,1)S(1)}, u32[]{:S(2)}, u32[]{:S(2)}) %all-to-all-start.3) | async-done | bytes 131104 | tf_op jit(solution)/shard_map/all_to_all | solution.py:425
  129.4 1.1 broadcast_select_fusion
  130.5 3.7 %all-to-all-start.4 = ((bf16[16,256,128]{2,1,0:T(8,128)(2,1)}), bf16[16,256,128]{2,1,0:T(8,128)(2,1)S(1)}, u32[]{:S(2)}, u32[]{:S(2)}) async-start(bf16[16,256,128]{2,1,0:T(8,128)(2,1)} %broadcast_select_fusion), calls=%async_computation.4 | async-start | bytes 2097152 | tf_op jit(solution)/shard_map/all_to_all | solution.py:425
  134.2 0.0 copy-start.6
  134.2 6.4 %collective-permute-done.7.low = bf16[6144,128]{1,0:T(8,128)(2,1)} collective-permute-done((bf16[6144,128]{1,0:T(8,128)(2,1)}, bf16[6144,128]{1,0:T(8,128)(2,1)}, u32[]{:S(2)}, u32[]{:S(2)}) %collective-permute-start.7) | collective-permute-done | bytes 1572896 | tf_op jit(solution)/shard_map/ppermute | solution.py:488
  140.6 10.5 %collective-permute-done.8.high = bf16[6144,128]{1,0:T(8,128)(2,1)} collective-permute-done((bf16[6144,128]{1,0:T(8,128)(2,1)S(1)}, bf16[6144,128]{1,0:T(8,128)(2,1)}, u32[]{:S(2)}, u32[]{:S(2)}) %collective-permute-start.8) | collective-permute-done | bytes 1572896 | tf_op jit(solution)/shard_map/ppermute | solution.py:489
  151.1 1.5 shard_map.179.gate_w
  152.7 4.6 %shard_map.180 = bf16[16,256,128]{2,1,0:T(8,128)(2,1)S(1)} custom-call(bf16[16,256,128]{2,1,0:T(8,128)(2,1)S(1)} %all-to-all-done.4.got, f32[1,2048]{1,0:T(1,128)S(1)} %bitcast.8, bf16[2048,512]{1,0:T(8,128)(2,1)S(1)} %shard_map.179.gate_w, bf16[1,2048,256]{2,1,0:T(8,128)(2,1)} %up_a.1, bf16[1,256,2048]{2,1,0:T(8,128)(2,1)} %down_a.1, ...), custom_call_target="tpu_custom_call" | custom-call | tf_op jit(solution)/shard_map/pallas_call | solution.py:414
  157.3 18.4 %all_to_all.36.parts = bf16[16,256,128]{2,1,0:T(8,128)(2,1)S(1)} all-to-all(bf16[16,256,128]{2,1,0:T(8,128)(2,1)S(1)} %shard_map.180), channel_id=1, replica_groups=mesh['sp'=32,'tp'=16] {'tp'}, dimensions={0} | all-to-all | bytes 2097152 | tf_op jit(solution)/shard_map/all_to_all | solution.py:425
  175.7 0.8 shard_map.181
  176.5 16.0 %all-to-all-start.6 = ((bf16[32,16,128]{2,1,0:T(8,128)(2,1)}), bf16[32,16,128]{2,1,0:T(8,128)(2,1)S(1)}, u32[]{:S(2)}, u32[]{:S(2)}) async-start(bf16[32,16,128]{2,1,0:T(8,128)(2,1)} %bitcast.5), calls=%async_computation.6 | async-start | bytes 262144 | tf_op jit(solution)/shard_map/all_to_all | solution.py:425
  192.5 0.1 copy.24.weights
  192.6 15.7 %all-to-all-done.6 = bf16[32,16,128]{2,1,0:T(8,128)(2,1)S(1)} async-done(((bf16[32,16,128]{2,1,0:T(8,128)(2,1)}), bf16[32,16,128]{2,1,0:T(8,128)(2,1)S(1)}, u32[]{:S(2)}, u32[]{:S(2)}) %all-to-all-start.6) | async-done | bytes 131104 | tf_op jit(solution)/shard_map/all_to_all | solution.py:425
  208.3 1.2 shard_map.182
  (38 shorter events, 0.1 us)
Async XLA Ops:
  30.4 6.9 %copy-start.13 = (bf16[512,64]{0,1:T(8,128)(2,1)S(1)}, bf16[512,64]{0,1:T(8,128)(2,1)}, u32[]{:S(2)}) copy-start(bf16[512,64]{0,1:T(8,128)(2,1)} %param.24) | copy-start | bytes 196612
  30.4 7.0 %copy-start.14 = (bf16[512,64]{0,1:T(8,128)(2,1)S(1)}, bf16[512,64]{0,1:T(8,128)(2,1)}, u32[]{:S(2)}) copy-start(bf16[512,64]{0,1:T(8,128)(2,1)} %param.25) | copy-start | bytes 196612
  30.4 7.2 %copy-start.15 = (bf16[128,192]{0,1:T(8,128)(2,1)S(1)}, bf16[128,192]{0,1:T(8,128)(2,1)}, u32[]{:S(2)}) copy-start(bf16[128,192]{0,1:T(8,128)(2,1)} %param.18) | copy-start | bytes 147460
  30.4 44.8 %all-to-all-start.1 = ((bf16[16,360,128]{2,1,0:T(8,128)(2,1)}), bf16[16,360,128]{2,1,0:T(8,128)(2,1)S(1)}, u32[]{:S(2)}, u32[]{:S(2)}) async-start(bf16[16,360,128]{2,1,0:T(8,128)(2,1)} %broadcast_in_dim.33), calls=%async_computation.1 | async-start | bytes 2949120 | tf_op jit(solution)/shard_map/all_to_all | solution.py:425
  39.3 0.7 copy-start.1
  40.0 35.1 %copy-start.3 = (bf16[128,640]{1,0:T(8,128)(2,1)}, bf16[128,640]{1,0:T(8,128)(2,1)S(1)}, u32[]{:S(2)}) copy-start(bf16[128,640]{1,0:T(8,128)(2,1)S(1)} %get-tuple-element.16.refs_2_) | copy-start | bytes 491524
  40.0 35.1 %copy-start.4 = (bf16[128,320]{1,0:T(8,128)(2,1)}, bf16[128,320]{1,0:T(8,128)(2,1)S(1)}, u32[]{:S(2)}) copy-start(bf16[128,320]{1,0:T(8,128)(2,1)S(1)} %get-tuple-element.14.q_own_in) | copy-start | bytes 245764
  40.0 44.4 %copy-start = (bf16[128,2048]{1,0:T(8,128)(2,1)S(1)}, bf16[128,2048]{1,0:T(8,128)(2,1)}, u32[]{:S(2)}) copy-start(bf16[128,2048]{1,0:T(8,128)(2,1)} %out_maj.1) | copy-start | bytes 1572868
  40.0 44.4 %copy-start.2 = (bf16[64,2048]{1,0:T(8,128)(2,1)S(1)}, bf16[64,2048]{1,0:T(8,128)(2,1)}, u32[]{:S(2)}) copy-start(bf16[64,2048]{1,0:T(8,128)(2,1)} %out_min.1) | copy-start | bytes 786436
  40.0 16.3 %collective-permute-start = (bf16[128,320]{1,0:T(8,128)(2,1)S(1)}, bf16[128,320]{1,0:T(8,128)(2,1)S(1)}, u32[]{:S(2)}, u32[]{:S(2)}) collective-permute-start(bf16[128,320]{1,0:T(8,128)(2,1)S(1)} %get-tuple-element.14.q_own_in), channel_id=1, source_target_pairs={{0,16},{16,0},{32,48},{48,32},{64,80},{80,64},{96,112},{112,96},{1... | collective-permute-start | bytes 245768 | tf_op jit(solution)/shard_map/ppermute | solution.py:486
  46.7 11.8 %collective-permute-start.1 = (bf16[128,640]{1,0:T(8,128)(2,1)S(1)}, bf16[128,640]{1,0:T(8,128)(2,1)S(1)}, u32[]{:S(2)}, u32[]{:S(2)}) collective-permute-start(bf16[128,640]{1,0:T(8,128)(2,1)S(1)} %get-tuple-element.16.refs_2_), channel_id=1, source_target_pairs={{0,64},{16,80},{32,96},{48,112},{64,128},{80,144},{96,160},{112,17... | collective-permute-start | bytes 491528 | tf_op jit(solution)/shard_map/ppermute | solution.py:487
  50.5 8.1 %collective-permute-start.2 = (bf16[128,640]{1,0:T(8,128)(2,1)S(1)}, bf16[128,640]{1,0:T(8,128)(2,1)S(1)}, u32[]{:S(2)}, u32[]{:S(2)}) collective-permute-start(bf16[128,640]{1,0:T(8,128)(2,1)S(1)} %get-tuple-element.16.refs_2_), channel_id=1, source_target_pairs={{0,32},{16,48},{32,64},{48,80},{64,96},{80,112},{96,128},{112,144}... | collective-permute-start | bytes 491528 | tf_op jit(solution)/shard_map/ppermute | solution.py:487
  53.0 14.9 %collective-permute-start.3 = (bf16[128,640]{1,0:T(8,128)(2,1)S(1)}, bf16[128,640]{1,0:T(8,128)(2,1)S(1)}, u32[]{:S(2)}, u32[]{:S(2)}) collective-permute-start(bf16[128,640]{1,0:T(8,128)(2,1)S(1)} %get-tuple-element.16.refs_2_), channel_id=1, source_target_pairs={{0,480},{16,496},{1,481},{17,497},{2,482},{18,498},{3,483},{19,499... | collective-permute-start | bytes 491528 | tf_op jit(solution)/shard_map/ppermute | solution.py:487
  54.3 17.3 %collective-permute-start.4 = (bf16[128,640]{1,0:T(8,128)(2,1)S(1)}, bf16[128,640]{1,0:T(8,128)(2,1)S(1)}, u32[]{:S(2)}, u32[]{:S(2)}) collective-permute-start(bf16[128,640]{1,0:T(8,128)(2,1)S(1)} %get-tuple-element.16.refs_2_), channel_id=1, source_target_pairs={{0,448},{16,464},{32,480},{48,496},{1,449},{17,465},{33,481},{49,4... | collective-permute-start | bytes 491528 | tf_op jit(solution)/shard_map/ppermute | solution.py:487
  56.4 18.8 %copy-start.12 = (bf16[128,320]{1,0:T(8,128)(2,1)}, bf16[128,320]{1,0:T(8,128)(2,1)S(1)}, u32[]{:S(2)}) copy-start(bf16[128,320]{1,0:T(8,128)(2,1)S(1)} %collective-permute-done.q_other_in) | copy-start | bytes 245764
  56.4 18.8 %collective-permute-start.5 = (bf16[128,640]{1,0:T(8,128)(2,1)S(1)}, bf16[128,640]{1,0:T(8,128)(2,1)S(1)}, u32[]{:S(2)}, u32[]{:S(2)}) collective-permute-start(bf16[128,640]{1,0:T(8,128)(2,1)S(1)} %get-tuple-element.16.refs_2_), channel_id=1, source_target_pairs={{0,416},{16,432},{32,448},{48,464},{64,480},{80,496},{1,417},{17,4... | collective-permute-start | bytes 491528 | tf_op jit(solution)/shard_map/ppermute | solution.py:487
  58.6 16.6 %copy-start.7 = (bf16[128,640]{1,0:T(8,128)(2,1)}, bf16[128,640]{1,0:T(8,128)(2,1)S(1)}, u32[]{:S(2)}) copy-start(bf16[128,640]{1,0:T(8,128)(2,1)S(1)} %collective-permute-done.1.refs_0_) | copy-start | bytes 491524
  58.6 16.6 %copy-start.8 = (bf16[128,640]{1,0:T(8,128)(2,1)}, bf16[128,640]{1,0:T(8,128)(2,1)S(1)}, u32[]{:S(2)}) copy-start(bf16[128,640]{1,0:T(8,128)(2,1)S(1)} %collective-permute-done.2.refs_1_) | copy-start | bytes 491524
  68.0 7.2 %copy-start.9 = (bf16[128,640]{1,0:T(8,128)(2,1)}, bf16[128,640]{1,0:T(8,128)(2,1)S(1)}, u32[]{:S(2)}) copy-start(bf16[128,640]{1,0:T(8,128)(2,1)S(1)} %collective-permute-done.3.refs_3_) | copy-start | bytes 491524
  71.6 3.6 %copy-start.10 = (bf16[128,640]{1,0:T(8,128)(2,1)}, bf16[128,640]{1,0:T(8,128)(2,1)S(1)}, u32[]{:S(2)}) copy-start(bf16[128,640]{1,0:T(8,128)(2,1)S(1)} %collective-permute-done.4.refs_4_) | copy-start | bytes 491524
  75.1 0.7 copy-start.11
  80.4 12.4 %copy-start.16 = (s32[128,2]{0,1:T(2,128)S(1)}, s32[128,2]{0,1:T(2,128)}, u32[]{:S(2)}) copy-start(s32[128,2]{0,1:T(2,128)} %param.30) | copy-start | bytes 3076
  80.4 23.1 %copy-start.5 = (bf16[128,128]{1,0:T(8,128)(2,1)S(1)}, bf16[128,128]{1,0:T(8,128)(2,1)}, u32[]{:S(2)}) copy-start(bf16[128,128]{1,0:T(8,128)(2,1)} %residual.1) | copy-start | bytes 98308
  80.4 4.0 %collective-permute-start.6 = (f32[128,256]{1,0:T(8,128)S(1)}, f32[128,256]{1,0:T(8,128)S(1)}, u32[]{:S(2)}, u32[]{:S(2)}) collective-permute-start(f32[128,256]{1,0:T(8,128)S(1)} %get-tuple-element.18), channel_id=1, source_target_pairs={{0,16},{16,0},{32,48},{48,32},{64,80},{80,64},{96,112},{112,96},{1... | collective-permute-start | bytes 393224 | tf_op jit(solution)/shard_map/ppermute | solution.py:505
  85.8 17.7 %all-to-all-start.2 = ((bf16[16,128,128]{2,1,0:T(8,128)(2,1)}), bf16[16,128,128]{2,1,0:T(8,128)(2,1)S(1)}, u32[]{:S(2)}, u32[]{:S(2)}) async-start(bf16[16,128,128]{2,1,0:T(8,128)(2,1)} %shard_map.176), calls=%async_computation.2 | async-start | bytes 1048576 | tf_op jit(solution)/shard_map/all_to_all | solution.py:425
  104.8 24.5 %all-to-all-start.3 = ((bf16[32,16,128]{2,1,0:T(8,128)(2,1)}), bf16[32,16,128]{2,1,0:T(8,128)(2,1)S(1)}, u32[]{:S(2)}, u32[]{:S(2)}) async-start(bf16[32,16,128]{2,1,0:T(8,128)(2,1)} %bitcast.1), calls=%async_computation.3 | async-start | bytes 262144 | tf_op jit(solution)/shard_map/all_to_all | solution.py:425
  116.7 23.9 %collective-permute-start.7 = (bf16[6144,128]{1,0:T(8,128)(2,1)}, bf16[6144,128]{1,0:T(8,128)(2,1)}, u32[]{:S(2)}, u32[]{:S(2)}) collective-permute-start(bf16[6144,128]{1,0:T(8,128)(2,1)} %get-tuple-element.20), channel_id=1, source_target_pairs={{0,1},{1,2},{2,3},{3,0},{4,5},{5,6},{6,7},{7,4},{8,9},{9,10},{10,1... | collective-permute-start | bytes 4718600 | tf_op jit(solution)/shard_map/ppermute | solution.py:488
  118.6 32.5 %collective-permute-start.8 = (bf16[6144,128]{1,0:T(8,128)(2,1)S(1)}, bf16[6144,128]{1,0:T(8,128)(2,1)}, u32[]{:S(2)}, u32[]{:S(2)}) collective-permute-start(bf16[6144,128]{1,0:T(8,128)(2,1)S(1)} %get-tuple-element.21), channel_id=1, source_target_pairs={{0,3},{1,0},{2,1},{3,2},{4,7},{5,4},{6,5},{7,6},{8,11},{9,8},{10,9... | collective-permute-start | bytes 4718600 | tf_op jit(solution)/shard_map/ppermute | solution.py:489
  130.5 22.1 %all-to-all-start.4 = ((bf16[16,256,128]{2,1,0:T(8,128)(2,1)}), bf16[16,256,128]{2,1,0:T(8,128)(2,1)S(1)}, u32[]{:S(2)}, u32[]{:S(2)}) async-start(bf16[16,256,128]{2,1,0:T(8,128)(2,1)} %broadcast_select_fusion), calls=%async_computation.4 | async-start | bytes 2097152 | tf_op jit(solution)/shard_map/all_to_all | solution.py:425
  134.2 18.5 %copy-start.6 = (f32[2048]{0:T(1024)S(1)}, f32[2048]{0:T(1024)}, u32[]{:S(2)}) copy-start(f32[2048]{0:T(1024)} %param.29) | copy-start | bytes 24580
  157.3 35.2 %copy-start.17 = (f32[128,2]{0,1:T(2,128)S(1)}, f32[128,2]{0,1:T(2,128)}, u32[]{:S(2)}) copy-start(f32[128,2]{0,1:T(2,128)} %param.31) | copy-start | bytes 3076
  176.5 31.8 %all-to-all-start.6 = ((bf16[32,16,128]{2,1,0:T(8,128)(2,1)}), bf16[32,16,128]{2,1,0:T(8,128)(2,1)S(1)}, u32[]{:S(2)}, u32[]{:S(2)}) async-start(bf16[32,16,128]{2,1,0:T(8,128)(2,1)} %bitcast.5), calls=%async_computation.6 | async-start | bytes 262144 | tf_op jit(solution)/shard_map/all_to_all | solution.py:425

commit v9 on v7

--- a/solution.py
+++ b/solution.py
@@ -328,19 +328,24 @@
         c.wait()
 
 
-def assemble_body(gate_a, low, high, gate_w, sems):
-    pairs = [(gate_a.at[0], gate_w.at[:, pl.ds(0, 256)])]
-    for i, packed in enumerate((low, high)):
-        pairs.append((packed.at[pl.ds(0, D)], gate_w.at[:, pl.ds(256 + 128 * i, 128)]))
-    for c in fetch(pairs, sems):
-        c.wait()
-
-
-def expert_body(got, gain, gate_w, up_a, down_a, low, high, parts, up_w, down_w, x, sems):
+def weights_here_body(low, high, out):
+    out[...] = jnp.zeros(out.shape, F32)
+
+
+def halves_body(arrived, here, out):
+    core = lax.axis_index("sp") % 2
+    for d in range(N_TP):
+        half = jnp.where(core == 0, d % 2, d // 4 % 2)
+        out[d] = arrived[pl.ds(pl.multiple_of(half * HALF, HALF), HALF), :]
+
+
+def expert_body(got, gain, gate_a, up_a, down_a, low, high, parts, gate_w, up_w, down_w, x, sems):
     own = pl.ds(0, 256)
-    pairs = [(up_a.at[0], up_w.at[:, own])]
-    for i, packed in enumerate((low, high)):
-        pairs.append((packed.at[pl.ds(D, D)], up_w.at[:, pl.ds(256 + 128 * i, 128)]))
+    pairs = []
+    for at, (mine, w) in enumerate(((gate_a, gate_w), (up_a, up_w))):
+        pairs.append((mine.at[0], w.at[:, own]))
+        for i, packed in enumerate((low, high)):
+            pairs.append((packed.at[pl.ds(at * D, D)], w.at[:, pl.ds(256 + 128 * i, 128)]))
     pairs.append((down_a.at[0], down_w.at[own]))
     for i, packed in enumerate((low, high)):
         for t in range(N_TP):
@@ -348,23 +353,20 @@
             pairs.append((packed.at[pl.ds(2 * D + 128 * t, 128)], down_w.at[mine, cols]))
     copies = fetch(pairs, sems)
     squares = jnp.zeros((HALF, 128), F32)
-    gate = jnp.zeros((HALF, 512), F32)
-    wide = 4
-    for n in range(0, N_TP, wide):
-        for t in range(n, n + wide):
-            cols = slice(128 * t, 128 * (t + 1))
-            v = got[t].astype(F32)
-            squares = squares + v * v
-            x[:, cols] = (v * gain[:, cols]).astype(BF16)
-        cols = slice(128 * n, 128 * (n + wide))
-        gate = gate + dot(x[:, cols], gate_w[cols, :])
+    for t in range(N_TP):
+        cols = slice(128 * t, 128 * (t + 1))
+        v = got[t].astype(F32)
+        squares = squares + v * v
+        x[:, cols] = (v * gain[:, cols]).astype(BF16)
     factor = lax.rsqrt(jnp.sum(squares, axis=1, keepdims=True) / D + NORM_EPS)
     for c in copies[:3]:
         c.wait()
-    gate = gate * factor
+    gate = dot(x[...], gate_w[...]) * factor
+    for c in copies[3:6]:
+        c.wait()
     up = dot(x[...], up_w[...]) * factor
     hidden = (gate / (1.0 + jnp.exp(-gate)) * up).astype(BF16)
-    for c in copies[3:]:
+    for c in copies[6:]:
         c.wait()
     for t in range(0, N_TP, 2):
         value = dot(hidden, down_w[:, 128 * t : 128 * (t + 2)])
@@ -514,19 +516,17 @@
         (head_parts, residual, expert_ids),
         range(3),
     )
-    arrived = to_each(placed.reshape(EXPERTS, CAP, 128), "sp").reshape(2, 1, HALF, 128)
-    peers = jnp.arange(N_TP, dtype=jnp.int32)
-    half_of = jnp.where(lax.axis_index("sp") % 2 == 0, peers % 2, (peers // 4) % 2)
-    half_rows = jnp.where(half_of[:, None, None] == 0, arrived[0], arrived[1])
+    arrived = to_each(placed.reshape(EXPERTS, CAP, 128), "sp").reshape(SLOTS, 128)
+    here = kernel(weights_here_body, shape((8, 128), F32), [], 0, (from_low, from_high))
+    half_rows = kernel(halves_body, shape((N_TP, HALF, 128)), [], 0, (arrived, here), (0,))
     everyone = to_each(half_rows, "tp")
-    gate_w = kernel(assemble_body, shape((D, 512)), [], 3, (gate_proj, from_low, from_high))
     down_parts = kernel(
         expert_body,
         shape((N_TP, HALF, 128)),
-        [room((D, 512)), room((512, D)), room((HALF, D))],
-        4 + 2 * N_TP,
-        (everyone, norm_gain.reshape(1, D), gate_w, up_proj, down_proj, from_low, from_high),
-        (0, 1, 2),
+        [room((D, 512)), room((D, 512)), room((512, D)), room((HALF, D))],
+        7 + 2 * N_TP,
+        (everyone, norm_gain.reshape(1, D), gate_proj, up_proj, down_proj, from_low, from_high),
+        (0, 1),
     )
     down_parts = to_each(down_parts, "tp")
     expert_out = kernel(gather_sum_body, shape((SLOTS, 128)), [], 0, (down_parts,), (0,))

time: 197 us -> 192 us (0.975)
  blocking collectives: 46.1 us -> 62.7 us
  starting transfers between devices: 70.1 us -> 57.9 us
  waiting for transfers between devices: 53.7 us -> 45.8 us
    all_to_all x2 -> x3, blocking collectives: 46.1 us -> 62.7 us  [to_each(): lax.all_to_all(array, axis, 0, 0, tiled=True, axis_index_groups=groups)]
    ppermute x1, waiting for transfers between devices: 10.4 us -> 0.01 us  [per_device(): from_high = lax.ppermute(high, ('sp', 'tp'), ring(-1))]
    all_to_all x5 -> x4, waiting for transfers between devices: 34.8 us -> 41.6 us  [to_each(): lax.all_to_all(array, axis, 0, 0, tiled=True, axis_index_groups=groups)]
    ppermute x1, waiting for transfers between devices: 6.49 us -> 0.01 us  [per_device(): from_low = lax.ppermute(low, ('sp', 'tp'), ring(1))]
    all_to_all x5 -> x4, starting transfers between devices: 40 us -> 33.7 us  [to_each(): lax.all_to_all(array, axis, 0, 0, tiled=True, axis_index_groups=groups)]
    ppermute x1, starting transfers between devices: 8.79 us -> 2.94 us  [per_device(): from_other = lax.ppermute(other, 'sp', OTHER_CORE)]
    ppermute x3, waiting for transfers between devices: 0.01 us -> 3.25 us  [per_device(): lax.ppermute(own_block, 'sp', along_z(-step))]
    ppermute x3, starting transfers between devices: 10.3 us -> 7.58 us  [per_device(): lax.ppermute(own_block, 'sp', along_z(-step))]
  transfers between devices with their start and end apart: 12 -> 11, of which waited for: 8 -> 5; matrix products, arithmetic and copies ran while one was open for 1% -> 0% of each run, Pallas kernels for 3% -> 7%
where the time goes in v9:
time: 192 us; the launch traced here: 191 us
  blocking collectives  62.7 us (33%)
  starting transfers between devices  57.9 us (30%)
  waiting for transfers between devices  45.8 us (24%)
  Pallas kernels  20.6 us (11%)
  local copies, waits for them, and re-layouts  4.13 us (2%)
    all_to_all x3, blocking collectives, to_each(): lax.all_to_all(array, axis, 0, 0, tiled=True, axis_index_groups=groups)  62.7 us
    all_to_all x4, waiting for transfers between devices, to_each(): lax.all_to_all(array, axis, 0, 0, tiled=True, axis_index_groups=groups)  41.6 us
    all_to_all x4, starting transfers between devices, to_each(): lax.all_to_all(array, axis, 0, 0, tiled=True, axis_index_groups=groups)  33.7 us
    pallas_call x12, Pallas kernels, kernel(): pl.pallas_call(body, out_shape=outs, in_specs=[pl.BlockSpec(memory_space=...  20.6 us
    ppermute x3, starting transfers between devices, per_device(): lax.ppermute(own_block, 'sp', along_z(-step))  7.58 us
    ppermute x1, starting transfers between devices, per_device(): q_other = lax.ppermute(q_own, 'sp', OTHER_CORE)  7.23 us
  transfers between devices with their start and end apart: 11, of which 5 were waited for; matrix products, arithmetic and copies ran while one was open for 0% of the time, Pallas kernels for 7%

profile of v9, /device:TPU:1, one launch (start us, length us, event | category | flops | bytes accessed | tf_op | source)
XLA Modules:
  0.0 191.5 jit_solution(11108793878888669021)
XLA Ops:
  0.0 1.2 shard_map.172
  1.2 27.7 %all_to_all.35.got = bf16[16,8,640]{2,1,0:T(8,128)(2,1)S(1)} all-to-all(bf16[16,8,640]{2,1,0:T(8,128)(2,1)S(1)} %shard_map.172), channel_id=1, replica_groups={{0,32,64,96,128,160,192,224,256,288,320,352,384,416,448,480},{16,48,80,..., dimensions={0} | all-to-all | bytes 327680 | tf_op jit(solution)/shard_map/all_to_all | solution.py:421
  28.9 0.1 shard_map.173
  29.0 1.5 broadcast_in_dim.3
  30.5 6.8 %all-to-all-start.1 = ((bf16[16,432,128]{2,1,0:T(8,128)(2,1)}), bf16[16,432,128]{2,1,0:T(8,128)(2,1)S(1)}, u32[]{:S(2)}, u32[]{:S(2)}) async-start(bf16[16,432,128]{2,1,0:T(8,128)(2,1)} %broadcast_in_dim.3), calls=%async_computation.1 | async-start | bytes 3538944 | tf_op jit(solution)/shard_map/all_to_all | solution.py:421
  37.2 0.0 copy-start.12
  37.3 0.0 copy-start.13
  37.3 0.0 copy-start.14
  37.3 3.8 %shard_map.178 = (bf16[6144,128]{1,0:T(8,128)(2,1)}, bf16[6144,128]{1,0:T(8,128)(2,1)}) custom-call(bf16[1,2048,256]{2,1,0:T(8,128)(2,1)} %gate_a.1, bf16[1,2048,256]{2,1,0:T(8,128)(2,1)} %up_a.1, bf16[1,256,2048]{2,1,0:T(8,128)(2,1)} %down_a.1), custom_call_target="tpu_custom_call" | custom-call | tf_op jit(solution)/shard_map/pallas_call | solution.py:410
  41.0 3.3 %collective-permute-start.5 = (bf16[6144,128]{1,0:T(8,128)(2,1)}, bf16[6144,128]{1,0:T(8,128)(2,1)}, u32[]{:S(2)}, u32[]{:S(2)}) collective-permute-start(bf16[6144,128]{1,0:T(8,128)(2,1)} %get-tuple-element.20), channel_id=1, source_target_pairs={{0,1},{1,2},{2,3},{3,0},{4,5},{5,6},{6,7},{7,4},{8,9},{9,10},{10,1... | collective-permute-start | bytes 4718600 | tf_op jit(solution)/shard_map/ppermute | solution.py:484
  44.3 3.2 %collective-permute-start.6 = (bf16[6144,128]{1,0:T(8,128)(2,1)}, bf16[6144,128]{1,0:T(8,128)(2,1)}, u32[]{:S(2)}, u32[]{:S(2)}) collective-permute-start(bf16[6144,128]{1,0:T(8,128)(2,1)} %get-tuple-element.21), channel_id=1, source_target_pairs={{0,3},{1,0},{2,1},{3,2},{4,7},{5,4},{6,5},{7,6},{8,11},{9,8},{10,9... | collective-permute-start | bytes 4718600 | tf_op jit(solution)/shard_map/ppermute | solution.py:485
  47.6 0.1 copy.20.ku_min
  47.7 0.1 copy.21.vu_min
  47.8 0.1 copy.19.maj
  48.0 1.6 shard_map.174
  49.6 0.8 copy-done.1
  50.4 7.2 %collective-permute-start = (bf16[128,320]{1,0:T(8,128)(2,1)S(1)}, bf16[128,320]{1,0:T(8,128)(2,1)S(1)}, u32[]{:S(2)}, u32[]{:S(2)}) collective-permute-start(bf16[128,320]{1,0:T(8,128)(2,1)S(1)} %get-tuple-element.14.q_own_in), channel_id=1, source_target_pairs={{0,16},{16,0},{32,48},{48,32},{64,80},{80,64},{96,112},{112,96},{1... | collective-permute-start | bytes 245768 | tf_op jit(solution)/shard_map/ppermute | solution.py:482
  57.6 3.8 %collective-permute-start.1 = (bf16[128,640]{1,0:T(8,128)(2,1)S(1)}, bf16[128,640]{1,0:T(8,128)(2,1)S(1)}, u32[]{:S(2)}, u32[]{:S(2)}) collective-permute-start(bf16[128,640]{1,0:T(8,128)(2,1)S(1)} %get-tuple-element.16.refs_2_), channel_id=1, source_target_pairs={{0,64},{16,80},{32,96},{48,112},{64,128},{80,144},{96,160},{112,17... | collective-permute-start | bytes 491528 | tf_op jit(solution)/shard_map/ppermute | solution.py:483
  61.4 2.5 %collective-permute-start.2 = (bf16[128,640]{1,0:T(8,128)(2,1)S(1)}, bf16[128,640]{1,0:T(8,128)(2,1)S(1)}, u32[]{:S(2)}, u32[]{:S(2)}) collective-permute-start(bf16[128,640]{1,0:T(8,128)(2,1)S(1)} %get-tuple-element.16.refs_2_), channel_id=1, source_target_pairs={{0,32},{16,48},{32,64},{48,80},{64,96},{80,112},{96,128},{112,144}... | collective-permute-start | bytes 491528 | tf_op jit(solution)/shard_map/ppermute | solution.py:483
  63.9 0.0 collective-permute-done.q_other_in
  63.9 1.3 collective-permute-start.3
  65.3 3.2 %collective-permute-done.2.refs_1_ = bf16[128,640]{1,0:T(8,128)(2,1)S(1)} collective-permute-done((bf16[128,640]{1,0:T(8,128)(2,1)S(1)}, bf16[128,640]{1,0:T(8,128)(2,1)S(1)}, u32[]{:S(2)}, u32[]{:S(2)}) %collective-permute-start.2) | collective-permute-done | bytes 163872 | tf_op jit(solution)/shard_map/ppermute | solution.py:483
  68.6 0.6 copy-done.9
  69.2 0.1 copy-done.10
  69.2 5.0 %shard_map.175 = (f32[128,256]{1,0:T(8,128)S(1)}, f32[128,256]{1,0:T(8,128)S(1)}) custom-call(bf16[16,432,128]{2,1,0:T(8,128)(2,1)S(1)} %all-to-all-done.1.keys, bf16[128,320]{1,0:T(8,128)(2,1)} %copy-done.4, bf16[128,320]{1,0:T(8,128)(2,1)} %copy-done.11, bf16[512,384]{1,0:T(8,128)(2,1)} %copy-done.1, bf16[128,640]{1,0:T(8,128)(2,1)} %copy-done.8, ...), custom_call_target="tpu_custom_call" | custom-call | tf_op jit(solution)/shard_map/pallas_call | solution.py:410
  74.2 0.0 copy-start.15
  74.3 0.0 copy-start.5
  74.3 2.9 %collective-permute-start.4 = (f32[128,256]{1,0:T(8,128)S(1)}, f32[128,256]{1,0:T(8,128)S(1)}, u32[]{:S(2)}, u32[]{:S(2)}) collective-permute-start(f32[128,256]{1,0:T(8,128)S(1)} %get-tuple-element.18), channel_id=1, source_target_pairs={{0,16},{16,0},{32,48},{48,32},{64,80},{80,64},{96,112},{112,96},{1... | collective-permute-start | bytes 393224 | tf_op jit(solution)/shard_map/ppermute | solution.py:501
  77.2 1.0 collective-permute-done.4.b
  78.2 1.4 shard_map.176
  79.5 5.7 %all-to-all-start.2 = ((bf16[16,128,128]{2,1,0:T(8,128)(2,1)}), bf16[16,128,128]{2,1,0:T(8,128)(2,1)S(1)}, u32[]{:S(2)}, u32[]{:S(2)}) async-start(bf16[16,128,128]{2,1,0:T(8,128)(2,1)} %shard_map.176), calls=%async_computation.2 | async-start | bytes 1048576 | tf_op jit(solution)/shard_map/all_to_all | solution.py:421
  85.3 0.1 copy.22.ids
  85.4 10.6 %all-to-all-done.2.parts = bf16[16,128,128]{2,1,0:T(8,128)(2,1)S(1)} async-done(((bf16[16,128,128]{2,1,0:T(8,128)(2,1)}), bf16[16,128,128]{2,1,0:T(8,128)(2,1)S(1)}, u32[]{:S(2)}, u32[]{:S(2)}) %all-to-all-start.2) | async-done | bytes 524320 | tf_op jit(solution)/shard_map/all_to_all | solution.py:421
  96.0 1.3 shard_map.177
  97.3 11.6 %all-to-all-start.3 = ((bf16[32,16,128]{2,1,0:T(8,128)(2,1)}), bf16[32,16,128]{2,1,0:T(8,128)(2,1)S(1)}, u32[]{:S(2)}, u32[]{:S(2)}) async-start(bf16[32,16,128]{2,1,0:T(8,128)(2,1)} %bitcast.1), calls=%async_computation.3 | async-start | bytes 262144 | tf_op jit(solution)/shard_map/all_to_all | solution.py:421
  109.0 0.0 copy-start.6
  109.0 0.6 copy-done.6
  109.6 15.2 %all-to-all-done.3 = bf16[32,16,128]{2,1,0:T(8,128)(2,1)S(1)} async-done(((bf16[32,16,128]{2,1,0:T(8,128)(2,1)}), bf16[32,16,128]{2,1,0:T(8,128)(2,1)S(1)}, u32[]{:S(2)}, u32[]{:S(2)}) %all-to-all-start.3) | async-done | bytes 131104 | tf_op jit(solution)/shard_map/all_to_all | solution.py:421
  124.8 0.1 shard_map.180
  124.9 18.2 %all_to_all.36.got = bf16[16,256,128]{2,1,0:T(8,128)(2,1)S(1)} all-to-all(bf16[16,256,128]{2,1,0:T(8,128)(2,1)S(1)} %shard_map.180), channel_id=1, replica_groups=mesh['sp'=32,'tp'=16] {'tp'}, dimensions={0} | all-to-all | bytes 2097152 | tf_op jit(solution)/shard_map/all_to_all | solution.py:421
  143.1 4.1 %shard_map.181 = bf16[16,256,128]{2,1,0:T(8,128)(2,1)S(1)} custom-call(bf16[16,256,128]{2,1,0:T(8,128)(2,1)S(1)} %all_to_all.36.got, f32[1,2048]{1,0:T(1,128)S(1)} %bitcast.8, bf16[1,2048,256]{2,1,0:T(8,128)(2,1)} %gate_a.1, bf16[1,2048,256]{2,1,0:T(8,128)(2,1)} %up_a.1, bf16[1,256,2048]{2,1,0:T(8,128)(2,1)} %down_a.1, ...), custom_call_target="tpu_custom_call" | custom-call | tf_op jit(solution)/shard_map/pallas_call | solution.py:410
  147.2 0.0 copy-start.16
  147.2 16.8 %all_to_all.37.parts = bf16[16,256,128]{2,1,0:T(8,128)(2,1)S(1)} all-to-all(bf16[16,256,128]{2,1,0:T(8,128)(2,1)S(1)} %shard_map.181), channel_id=1, replica_groups=mesh['sp'=32,'tp'=16] {'tp'}, dimensions={0} | all-to-all | bytes 2097152 | tf_op jit(solution)/shard_map/all_to_all | solution.py:421
  164.0 0.8 shard_map.182
  164.8 9.6 %all-to-all-start.6 = ((bf16[32,16,128]{2,1,0:T(8,128)(2,1)}), bf16[32,16,128]{2,1,0:T(8,128)(2,1)S(1)}, u32[]{:S(2)}, u32[]{:S(2)}) async-start(bf16[32,16,128]{2,1,0:T(8,128)(2,1)} %bitcast.4), calls=%async_computation.6 | async-start | bytes 262144 | tf_op jit(solution)/shard_map/all_to_all | solution.py:421
  174.4 0.1 copy.24.weights
  174.5 15.7 %all-to-all-done.6 = bf16[32,16,128]{2,1,0:T(8,128)(2,1)S(1)} async-done(((bf16[32,16,128]{2,1,0:T(8,128)(2,1)}), bf16[32,16,128]{2,1,0:T(8,128)(2,1)S(1)}, u32[]{:S(2)}, u32[]{:S(2)}) %all-to-all-start.6) | async-done | bytes 131104 | tf_op jit(solution)/shard_map/all_to_all | solution.py:421
  190.2 1.2 shard_map.183
  (29 shorter events, 0.1 us)
Async XLA Ops:
  30.5 38.0 %all-to-all-start.1 = ((bf16[16,432,128]{2,1,0:T(8,128)(2,1)}), bf16[16,432,128]{2,1,0:T(8,128)(2,1)S(1)}, u32[]{:S(2)}, u32[]{:S(2)}) async-start(bf16[16,432,128]{2,1,0:T(8,128)(2,1)} %broadcast_in_dim.3), calls=%async_computation.1 | async-start | bytes 3538944 | tf_op jit(solution)/shard_map/all_to_all | solution.py:421
  37.2 10.3 %copy-start.12 = (bf16[512,64]{0,1:T(8,128)(2,1)S(1)}, bf16[512,64]{0,1:T(8,128)(2,1)}, u32[]{:S(2)}) copy-start(bf16[512,64]{0,1:T(8,128)(2,1)} %param.24) | copy-start | bytes 196612
  37.3 10.4 %copy-start.13 = (bf16[512,64]{0,1:T(8,128)(2,1)S(1)}, bf16[512,64]{0,1:T(8,128)(2,1)}, u32[]{:S(2)}) copy-start(bf16[512,64]{0,1:T(8,128)(2,1)} %param.25) | copy-start | bytes 196612
  37.3 10.6 %copy-start.14 = (bf16[128,192]{0,1:T(8,128)(2,1)S(1)}, bf16[128,192]{0,1:T(8,128)(2,1)}, u32[]{:S(2)}) copy-start(bf16[128,192]{0,1:T(8,128)(2,1)} %param.18) | copy-start | bytes 147460
  41.0 67.9 %collective-permute-start.5 = (bf16[6144,128]{1,0:T(8,128)(2,1)}, bf16[6144,128]{1,0:T(8,128)(2,1)}, u32[]{:S(2)}, u32[]{:S(2)}) collective-permute-start(bf16[6144,128]{1,0:T(8,128)(2,1)} %get-tuple-element.20), channel_id=1, source_target_pairs={{0,1},{1,2},{2,3},{3,0},{4,5},{5,6},{6,7},{7,4},{8,9},{9,10},{10,1... | collective-permute-start | bytes 4718600 | tf_op jit(solution)/shard_map/ppermute | solution.py:484
  44.3 64.6 %collective-permute-start.6 = (bf16[6144,128]{1,0:T(8,128)(2,1)}, bf16[6144,128]{1,0:T(8,128)(2,1)}, u32[]{:S(2)}, u32[]{:S(2)}) collective-permute-start(bf16[6144,128]{1,0:T(8,128)(2,1)} %get-tuple-element.21), channel_id=1, source_target_pairs={{0,3},{1,0},{2,1},{3,2},{4,7},{5,4},{6,5},{7,6},{8,11},{9,8},{10,9... | collective-permute-start | bytes 4718600 | tf_op jit(solution)/shard_map/ppermute | solution.py:485
  49.6 0.8 copy-start.1
  50.4 18.1 %copy-start.3 = (bf16[128,640]{1,0:T(8,128)(2,1)}, bf16[128,640]{1,0:T(8,128)(2,1)S(1)}, u32[]{:S(2)}) copy-start(bf16[128,640]{1,0:T(8,128)(2,1)S(1)} %get-tuple-element.16.refs_2_) | copy-start | bytes 491524
  50.4 18.2 %copy-start.4 = (bf16[128,320]{1,0:T(8,128)(2,1)}, bf16[128,320]{1,0:T(8,128)(2,1)S(1)}, u32[]{:S(2)}) copy-start(bf16[128,320]{1,0:T(8,128)(2,1)S(1)} %get-tuple-element.14.q_own_in) | copy-start | bytes 245764
  50.4 27.8 %copy-start = (bf16[128,2048]{1,0:T(8,128)(2,1)S(1)}, bf16[128,2048]{1,0:T(8,128)(2,1)}, u32[]{:S(2)}) copy-start(bf16[128,2048]{1,0:T(8,128)(2,1)} %out_maj.1) | copy-start | bytes 1572868
  50.4 27.8 %copy-start.2 = (bf16[64,2048]{1,0:T(8,128)(2,1)S(1)}, bf16[64,2048]{1,0:T(8,128)(2,1)}, u32[]{:S(2)}) copy-start(bf16[64,2048]{1,0:T(8,128)(2,1)} %out_min.1) | copy-start | bytes 786436
  50.4 13.5 %collective-permute-start = (bf16[128,320]{1,0:T(8,128)(2,1)S(1)}, bf16[128,320]{1,0:T(8,128)(2,1)S(1)}, u32[]{:S(2)}, u32[]{:S(2)}) collective-permute-start(bf16[128,320]{1,0:T(8,128)(2,1)S(1)} %get-tuple-element.14.q_own_in), channel_id=1, source_target_pairs={{0,16},{16,0},{32,48},{48,32},{64,80},{80,64},{96,112},{112,96},{1... | collective-permute-start | bytes 245768 | tf_op jit(solution)/shard_map/ppermute | solution.py:482
  57.6 7.6 %collective-permute-start.1 = (bf16[128,640]{1,0:T(8,128)(2,1)S(1)}, bf16[128,640]{1,0:T(8,128)(2,1)S(1)}, u32[]{:S(2)}, u32[]{:S(2)}) collective-permute-start(bf16[128,640]{1,0:T(8,128)(2,1)S(1)} %get-tuple-element.16.refs_2_), channel_id=1, source_target_pairs={{0,64},{16,80},{32,96},{48,112},{64,128},{80,144},{96,160},{112,17... | collective-permute-start | bytes 491528 | tf_op jit(solution)/shard_map/ppermute | solution.py:483
  61.4 7.1 %collective-permute-start.2 = (bf16[128,640]{1,0:T(8,128)(2,1)S(1)}, bf16[128,640]{1,0:T(8,128)(2,1)S(1)}, u32[]{:S(2)}, u32[]{:S(2)}) collective-permute-start(bf16[128,640]{1,0:T(8,128)(2,1)S(1)} %get-tuple-element.16.refs_2_), channel_id=1, source_target_pairs={{0,32},{16,48},{32,64},{48,80},{64,96},{80,112},{96,128},{112,144}... | collective-permute-start | bytes 491528 | tf_op jit(solution)/shard_map/ppermute | solution.py:483
  63.9 4.6 %copy-start.11 = (bf16[128,320]{1,0:T(8,128)(2,1)}, bf16[128,320]{1,0:T(8,128)(2,1)S(1)}, u32[]{:S(2)}) copy-start(bf16[128,320]{1,0:T(8,128)(2,1)S(1)} %collective-permute-done.q_other_in) | copy-start | bytes 245764
  63.9 4.6 %collective-permute-start.3 = (bf16[128,640]{1,0:T(8,128)(2,1)S(1)}, bf16[128,640]{1,0:T(8,128)(2,1)S(1)}, u32[]{:S(2)}, u32[]{:S(2)}) collective-permute-start(bf16[128,640]{1,0:T(8,128)(2,1)S(1)} %get-tuple-element.16.refs_2_), channel_id=1, source_target_pairs={{0,480},{16,496},{1,481},{17,497},{2,482},{18,498},{3,483},{19,499... | collective-permute-start | bytes 491528 | tf_op jit(solution)/shard_map/ppermute | solution.py:483
  65.2 3.3 %copy-start.8 = (bf16[128,640]{1,0:T(8,128)(2,1)}, bf16[128,640]{1,0:T(8,128)(2,1)S(1)}, u32[]{:S(2)}) copy-start(bf16[128,640]{1,0:T(8,128)(2,1)S(1)} %collective-permute-done.1.refs_0_) | copy-start | bytes 491524
  68.5 0.7 copy-start.9
  68.5 0.7 copy-start.10
  74.2 11.0 %copy-start.15 = (s32[128,2]{0,1:T(2,128)S(1)}, s32[128,2]{0,1:T(2,128)}, u32[]{:S(2)}) copy-start(s32[128,2]{0,1:T(2,128)} %param.30) | copy-start | bytes 3076
  74.3 21.8 %copy-start.5 = (bf16[128,128]{1,0:T(8,128)(2,1)S(1)}, bf16[128,128]{1,0:T(8,128)(2,1)}, u32[]{:S(2)}) copy-start(bf16[128,128]{1,0:T(8,128)(2,1)} %residual.1) | copy-start | bytes 98308
  74.3 3.9 %collective-permute-start.4 = (f32[128,256]{1,0:T(8,128)S(1)}, f32[128,256]{1,0:T(8,128)S(1)}, u32[]{:S(2)}, u32[]{:S(2)}) collective-permute-start(f32[128,256]{1,0:T(8,128)S(1)} %get-tuple-element.18), channel_id=1, source_target_pairs={{0,16},{16,0},{32,48},{48,32},{64,80},{80,64},{96,112},{112,96},{1... | collective-permute-start | bytes 393224 | tf_op jit(solution)/shard_map/ppermute | solution.py:501
  79.5 16.5 %all-to-all-start.2 = ((bf16[16,128,128]{2,1,0:T(8,128)(2,1)}), bf16[16,128,128]{2,1,0:T(8,128)(2,1)S(1)}, u32[]{:S(2)}, u32[]{:S(2)}) async-start(bf16[16,128,128]{2,1,0:T(8,128)(2,1)} %shard_map.176), calls=%async_computation.2 | async-start | bytes 1048576 | tf_op jit(solution)/shard_map/all_to_all | solution.py:421
  97.3 27.5 %all-to-all-start.3 = ((bf16[32,16,128]{2,1,0:T(8,128)(2,1)}), bf16[32,16,128]{2,1,0:T(8,128)(2,1)S(1)}, u32[]{:S(2)}, u32[]{:S(2)}) async-start(bf16[32,16,128]{2,1,0:T(8,128)(2,1)} %bitcast.1), calls=%async_computation.3 | async-start | bytes 262144 | tf_op jit(solution)/shard_map/all_to_all | solution.py:421
  109.0 0.6 copy-start.6
  124.8 18.3 %copy-start.7 = (f32[2048]{0:T(1024)S(1)}, f32[2048]{0:T(1024)}, u32[]{:S(2)}) copy-start(f32[2048]{0:T(1024)} %param.29) | copy-start | bytes 24580
  147.2 27.2 %copy-start.16 = (f32[128,2]{0,1:T(2,128)S(1)}, f32[128,2]{0,1:T(2,128)}, u32[]{:S(2)}) copy-start(f32[128,2]{0,1:T(2,128)} %param.31) | copy-start | bytes 3076
  164.8 25.4 %all-to-all-start.6 = ((bf16[32,16,128]{2,1,0:T(8,128)(2,1)}), bf16[32,16,128]{2,1,0:T(8,128)(2,1)S(1)}, u32[]{:S(2)}, u32[]{:S(2)}) async-start(bf16[32,16,128]{2,1,0:T(8,128)(2,1)} %bitcast.4), calls=%async_computation.6 | async-start | bytes 262144 | tf_op jit(solution)/shard_map/all_to_all | solution.py:421

commit v10 on v9

--- a/solution.py
+++ b/solution.py
@@ -23,6 +23,7 @@
 ROWS = TOK // N_TP
 KEYS = N_Z * TOK
 MASKED = -1e30
+LOG2_E = float(np.log2(np.e))
 NORM_EPS = 1e-6
 HALF = SLOTS // 2
 NEAR = (-2, -1, 0, 1)
@@ -197,8 +198,8 @@
     core, z = me % 2, me // 2
     row = lax.broadcasted_iota(jnp.int32, (2 * TOK, 1), 0)
     q_pos = jnp.where(row < TOK, me * TOK + row, (me + 1 - 2 * core) * TOK + row - TOK)
-    scale_maj = (NOPE_MAJOR + ROPE) ** -0.5
-    scale_min = (NOPE_MINOR + ROPE) ** -0.5
+    scale_maj = (NOPE_MAJOR + ROPE) ** -0.5 * LOG2_E
+    scale_min = (NOPE_MINOR + ROPE) ** -0.5 * LOG2_E
     tops = [jnp.full((2 * TOK, 128), MASKED, F32)] * 2
     for c in copies[:3]:
         c.wait()
@@ -254,8 +255,8 @@
     o_min = jnp.zeros((2 * TOK, 64), F32)
     step = 512
     for at in range(0, KEYS, step):
-        p = jnp.exp(s_maj[:, at : at + step] - m_maj)
-        r = jnp.exp(s_min[:, at : at + step] - m_min)
+        p = jnp.exp2(s_maj[:, at : at + step] - m_maj)
+        r = jnp.exp2(s_min[:, at : at + step] - m_min)
         for k in range(step // 128):
             sum_maj = sum_maj + p[:, 128 * k : 128 * (k + 1)]
             sum_min = sum_min + r[:, 128 * k : 128 * (k + 1)]
@@ -280,7 +281,7 @@
         m_a, m_b = a[:, m_at : m_at + 1], b[:, m_at : m_at + 1]
         l_a, l_b = a[:, m_at + 1 : m_at + 2], b[:, m_at + 1 : m_at + 2]
         top = jnp.maximum(m_a, m_b)
-        f_a, f_b = jnp.exp(m_a - top), jnp.exp(m_b - top)
+        f_a, f_b = jnp.exp2(m_a - top), jnp.exp2(m_b - top)
         total = l_a * f_a + l_b * f_b
         return ((a[:, lo:hi] * f_a + b[:, lo:hi] * f_b) / total).astype(BF16)
 
@@ -304,7 +305,7 @@
     return ids[:, 0:1] * CAP + rank_0, ids[:, 1:2] * CAP + rank_1
 
 
-def place_body(parts, residual, ids, stream, placed):
+def place_body(parts, residual, ids, weights, stream, placed):
     slot_0, slot_1 = slot_columns(ids[...])
     lane = lax.broadcasted_iota(jnp.int32, (TOK, SLOTS), 1)
     select = ((lane == slot_0) | (lane == slot_1)).astype(BF16)
@@ -513,8 +514,8 @@
         (shape((TOK, 128)), shape((SLOTS, 128))),
         [],
         0,
-        (head_parts, residual, expert_ids),
-        range(3),
+        (head_parts, residual, expert_ids, expert_weights),
+        range(4),
     )
     arrived = to_each(placed.reshape(EXPERTS, CAP, 128), "sp").reshape(SLOTS, 128)
     here = kernel(weights_here_body, shape((8, 128), F32), [], 0, (from_low, from_high))

time: 192 us -> 192 us (level)
  blocking collectives: 62.7 us -> 87.9 us
  waiting for transfers between devices: 45.8 us -> 32.4 us
  starting transfers between devices: 57.9 us -> 47 us
    all_to_all x3 -> x4, blocking collectives: 62.7 us -> 87.9 us  [to_each(): lax.all_to_all(array, axis, 0, 0, tiled=True, axis_index_groups=groups)]
    all_to_all x4 -> x3, waiting for transfers between devices: 41.6 us -> 25.7 us  [to_each(): lax.all_to_all(array, axis, 0, 0, tiled=True, axis_index_groups=groups)]
    all_to_all x4 -> x3, starting transfers between devices: 33.7 us -> 23.2 us  [to_each(): lax.all_to_all(array, axis, 0, 0, tiled=True, axis_index_groups=groups)]
    ppermute x3, waiting for transfers between devices: 3.25 us -> 5.74 us  [per_device(): lax.ppermute(own_block, 'sp', along_z(-step))]
  transfers between devices with their start and end apart: 11 -> 10, of which waited for: 5 -> 6; matrix products, arithmetic and copies ran while one was open for 0% -> 0% of each run, Pallas kernels for 7% -> 7%
where the time goes in v10:
time: 192 us
  blocking collectives  87.9 us (46%)
  starting transfers between devices  47 us (24%)
  waiting for transfers between devices  32.4 us (17%)
  Pallas kernels  19.9 us (10%)
  local copies, waits for them, and re-layouts  4.06 us (2%)
    all_to_all x4, blocking collectives, to_each(): lax.all_to_all(array, axis, 0, 0, tiled=True, axis_index_groups=groups)  87.9 us
    all_to_all x3, waiting for transfers between devices, to_each(): lax.all_to_all(array, axis, 0, 0, tiled=True, axis_index_groups=groups)  25.7 us
    all_to_all x3, starting transfers between devices, to_each(): lax.all_to_all(array, axis, 0, 0, tiled=True, axis_index_groups=groups)  23.2 us
    pallas_call x12, Pallas kernels, kernel(): pl.pallas_call(body, out_shape=outs, in_specs=[pl.BlockSpec(memory_space=...  19.9 us
    ppermute x1, starting transfers between devices, per_device(): q_other = lax.ppermute(q_own, 'sp', OTHER_CORE)  7.23 us
    ppermute x3, starting transfers between devices, per_device(): lax.ppermute(own_block, 'sp', along_z(-step))  7.13 us
    ppermute x3, waiting for transfers between devices, per_device(): lax.ppermute(own_block, 'sp', along_z(-step))  5.74 us
  transfers between devices with their start and end apart: 10, of which 6 were waited for; matrix products, arithmetic and copies ran while one was open for 0% of the time, Pallas kernels for 7%

profile of v10, /device:TPU:1, one launch (start us, length us, event | category | flops | bytes accessed | tf_op | source)
XLA Modules:
  0.0 191.6 jit_solution(13590035039239633643)
XLA Ops:
  0.0 1.2 shard_map.172
  1.2 27.7 %all_to_all.35.got = bf16[16,8,640]{2,1,0:T(8,128)(2,1)S(1)} all-to-all(bf16[16,8,640]{2,1,0:T(8,128)(2,1)S(1)} %shard_map.172), channel_id=1, replica_groups={{0,32,64,96,128,160,192,224,256,288,320,352,384,416,448,480},{16,48,80,..., dimensions={0} | all-to-all | bytes 327680 | tf_op jit(solution)/shard_map/all_to_all | solution.py:422
  28.9 0.1 shard_map.173
  29.0 1.5 broadcast_in_dim.3
  30.5 6.8 %all-to-all-start.1 = ((bf16[16,432,128]{2,1,0:T(8,128)(2,1)}), bf16[16,432,128]{2,1,0:T(8,128)(2,1)S(1)}, u32[]{:S(2)}, u32[]{:S(2)}) async-start(bf16[16,432,128]{2,1,0:T(8,128)(2,1)} %broadcast_in_dim.3), calls=%async_computation.1 | async-start | bytes 3538944 | tf_op jit(solution)/shard_map/all_to_all | solution.py:422
  37.2 0.0 copy-start.14
  37.2 0.0 copy-start.12
  37.3 0.0 copy-start.13
  37.3 3.8 %shard_map.178 = (bf16[6144,128]{1,0:T(8,128)(2,1)}, bf16[6144,128]{1,0:T(8,128)(2,1)}) custom-call(bf16[1,2048,256]{2,1,0:T(8,128)(2,1)} %gate_a.1, bf16[1,2048,256]{2,1,0:T(8,128)(2,1)} %up_a.1, bf16[1,256,2048]{2,1,0:T(8,128)(2,1)} %down_a.1), custom_call_target="tpu_custom_call" | custom-call | tf_op jit(solution)/shard_map/pallas_call | solution.py:411
  41.0 3.3 %collective-permute-start.5 = (bf16[6144,128]{1,0:T(8,128)(2,1)}, bf16[6144,128]{1,0:T(8,128)(2,1)}, u32[]{:S(2)}, u32[]{:S(2)}) collective-permute-start(bf16[6144,128]{1,0:T(8,128)(2,1)} %get-tuple-element.20), channel_id=1, source_target_pairs={{0,1},{1,2},{2,3},{3,0},{4,5},{5,6},{6,7},{7,4},{8,9},{9,10},{10,1... | collective-permute-start | bytes 4718600 | tf_op jit(solution)/shard_map/ppermute | solution.py:485
  44.3 3.2 %collective-permute-start.6 = (bf16[6144,128]{1,0:T(8,128)(2,1)}, bf16[6144,128]{1,0:T(8,128)(2,1)}, u32[]{:S(2)}, u32[]{:S(2)}) collective-permute-start(bf16[6144,128]{1,0:T(8,128)(2,1)} %get-tuple-element.21), channel_id=1, source_target_pairs={{0,3},{1,0},{2,1},{3,2},{4,7},{5,4},{6,5},{7,6},{8,11},{9,8},{10,9... | collective-permute-start | bytes 4718600 | tf_op jit(solution)/shard_map/ppermute | solution.py:486
  47.6 0.1 copy.19.maj
  47.7 0.1 copy.20.ku_min
  47.8 0.1 copy.21.vu_min
  48.0 1.6 shard_map.174
  49.6 0.8 copy-done.1
  50.4 7.2 %collective-permute-start = (bf16[128,320]{1,0:T(8,128)(2,1)S(1)}, bf16[128,320]{1,0:T(8,128)(2,1)S(1)}, u32[]{:S(2)}, u32[]{:S(2)}) collective-permute-start(bf16[128,320]{1,0:T(8,128)(2,1)S(1)} %get-tuple-element.14.q_own_in), channel_id=1, source_target_pairs={{0,16},{16,0},{32,48},{48,32},{64,80},{80,64},{96,112},{112,96},{1... | collective-permute-start | bytes 245768 | tf_op jit(solution)/shard_map/ppermute | solution.py:483
  57.6 4.5 %collective-permute-start.3 = (bf16[128,640]{1,0:T(8,128)(2,1)S(1)}, bf16[128,640]{1,0:T(8,128)(2,1)S(1)}, u32[]{:S(2)}, u32[]{:S(2)}) collective-permute-start(bf16[128,640]{1,0:T(8,128)(2,1)S(1)} %get-tuple-element.16.refs_2_), channel_id=1, source_target_pairs={{0,480},{16,496},{1,481},{17,497},{2,482},{18,498},{3,483},{19,499... | collective-permute-start | bytes 491528 | tf_op jit(solution)/shard_map/ppermute | solution.py:484
  62.2 1.3 collective-permute-start.2
  63.5 1.3 collective-permute-start.1
  64.8 0.9 collective-permute-done.3.refs_3_
  65.7 1.3 collective-permute-done.2.refs_1_
  67.0 3.6 %collective-permute-done.1.refs_0_ = bf16[128,640]{1,0:T(8,128)(2,1)S(1)} collective-permute-done((bf16[128,640]{1,0:T(8,128)(2,1)S(1)}, bf16[128,640]{1,0:T(8,128)(2,1)S(1)}, u32[]{:S(2)}, u32[]{:S(2)}) %collective-permute-start.1) | collective-permute-done | bytes 163872 | tf_op jit(solution)/shard_map/ppermute | solution.py:484
  70.6 0.6 copy-done.10
  71.2 4.9 %shard_map.175 = (f32[128,256]{1,0:T(8,128)S(1)}, f32[128,256]{1,0:T(8,128)S(1)}) custom-call(bf16[16,432,128]{2,1,0:T(8,128)(2,1)S(1)} %all-to-all-done.1.keys, bf16[128,320]{1,0:T(8,128)(2,1)} %copy-done.4, bf16[128,320]{1,0:T(8,128)(2,1)} %copy-done.11, bf16[512,384]{1,0:T(8,128)(2,1)} %copy-done.1, bf16[128,640]{1,0:T(8,128)(2,1)} %copy-done.10, ...), custom_call_target="tpu_custom_call" | custom-call | tf_op jit(solution)/shard_map/pallas_call | solution.py:411
  76.1 0.0 copy-start.15
  76.1 0.0 copy-start.16
  76.1 0.0 copy-start.5
  76.1 2.9 %collective-permute-start.4 = (f32[128,256]{1,0:T(8,128)S(1)}, f32[128,256]{1,0:T(8,128)S(1)}, u32[]{:S(2)}, u32[]{:S(2)}) collective-permute-start(f32[128,256]{1,0:T(8,128)S(1)} %get-tuple-element.18), channel_id=1, source_target_pairs={{0,16},{16,0},{32,48},{48,32},{64,80},{80,64},{96,112},{112,96},{1... | collective-permute-start | bytes 393224 | tf_op jit(solution)/shard_map/ppermute | solution.py:502
  79.1 1.0 collective-permute-done.4.b
  80.0 1.4 shard_map.176
  81.4 5.7 %all-to-all-start.2 = ((bf16[16,128,128]{2,1,0:T(8,128)(2,1)}), bf16[16,128,128]{2,1,0:T(8,128)(2,1)S(1)}, u32[]{:S(2)}, u32[]{:S(2)}) async-start(bf16[16,128,128]{2,1,0:T(8,128)(2,1)} %shard_map.176), calls=%async_computation.2 | async-start | bytes 1048576 | tf_op jit(solution)/shard_map/all_to_all | solution.py:422
  87.1 0.1 copy.22.ids
  87.2 0.1 copy.23.weights
  87.4 10.5 %all-to-all-done.2.parts = bf16[16,128,128]{2,1,0:T(8,128)(2,1)S(1)} async-done(((bf16[16,128,128]{2,1,0:T(8,128)(2,1)}), bf16[16,128,128]{2,1,0:T(8,128)(2,1)S(1)}, u32[]{:S(2)}, u32[]{:S(2)}) %all-to-all-start.2) | async-done | bytes 524320 | tf_op jit(solution)/shard_map/all_to_all | solution.py:422
  97.9 1.3 shard_map.177
  99.2 10.7 %all-to-all-start.3 = ((bf16[32,16,128]{2,1,0:T(8,128)(2,1)}), bf16[32,16,128]{2,1,0:T(8,128)(2,1)S(1)}, u32[]{:S(2)}, u32[]{:S(2)}) async-start(bf16[32,16,128]{2,1,0:T(8,128)(2,1)} %bitcast.1), calls=%async_computation.3 | async-start | bytes 262144 | tf_op jit(solution)/shard_map/all_to_all | solution.py:422
  109.9 0.0 collective-permute-done.5.low
  109.9 0.0 copy-start.6
  110.0 0.6 copy-done.6
  110.5 15.2 %all-to-all-done.3 = bf16[32,16,128]{2,1,0:T(8,128)(2,1)S(1)} async-done(((bf16[32,16,128]{2,1,0:T(8,128)(2,1)}), bf16[32,16,128]{2,1,0:T(8,128)(2,1)S(1)}, u32[]{:S(2)}, u32[]{:S(2)}) %all-to-all-start.3) | async-done | bytes 131104 | tf_op jit(solution)/shard_map/all_to_all | solution.py:422
  125.8 0.1 shard_map.180
  125.9 18.2 %all_to_all.36.got = bf16[16,256,128]{2,1,0:T(8,128)(2,1)S(1)} all-to-all(bf16[16,256,128]{2,1,0:T(8,128)(2,1)S(1)} %shard_map.180), channel_id=1, replica_groups=mesh['sp'=32,'tp'=16] {'tp'}, dimensions={0} | all-to-all | bytes 2097152 | tf_op jit(solution)/shard_map/all_to_all | solution.py:422
  144.1 4.1 %shard_map.181 = bf16[16,256,128]{2,1,0:T(8,128)(2,1)S(1)} custom-call(bf16[16,256,128]{2,1,0:T(8,128)(2,1)S(1)} %all_to_all.36.got, f32[1,2048]{1,0:T(1,128)S(1)} %bitcast.9, bf16[1,2048,256]{2,1,0:T(8,128)(2,1)} %gate_a.1, bf16[1,2048,256]{2,1,0:T(8,128)(2,1)} %up_a.1, bf16[1,256,2048]{2,1,0:T(8,128)(2,1)} %down_a.1, ...), custom_call_target="tpu_custom_call" | custom-call | tf_op jit(solution)/shard_map/pallas_call | solution.py:411
  148.2 16.8 %all_to_all.37.parts = bf16[16,256,128]{2,1,0:T(8,128)(2,1)S(1)} all-to-all(bf16[16,256,128]{2,1,0:T(8,128)(2,1)S(1)} %shard_map.181), channel_id=1, replica_groups=mesh['sp'=32,'tp'=16] {'tp'}, dimensions={0} | all-to-all | bytes 2097152 | tf_op jit(solution)/shard_map/all_to_all | solution.py:422
  165.0 0.1 shard_map.182
  165.1 25.2 %all_to_all.38 = bf16[32,16,128]{2,1,0:T(8,128)(2,1)S(1)} all-to-all(bf16[32,16,128]{2,1,0:T(8,128)(2,1)S(1)} %bitcast.7), channel_id=1, replica_groups=mesh['sp'=32,'tp'=16] {'sp'}, dimensions={0} | all-to-all | bytes 262144 | tf_op jit(solution)/shard_map/all_to_all | solution.py:422
  190.4 1.2 shard_map.183
  (28 shorter events, 0.1 us)
Async XLA Ops:
  30.5 40.1 %all-to-all-start.1 = ((bf16[16,432,128]{2,1,0:T(8,128)(2,1)}), bf16[16,432,128]{2,1,0:T(8,128)(2,1)S(1)}, u32[]{:S(2)}, u32[]{:S(2)}) async-start(bf16[16,432,128]{2,1,0:T(8,128)(2,1)} %broadcast_in_dim.3), calls=%async_computation.1 | async-start | bytes 3538944 | tf_op jit(solution)/shard_map/all_to_all | solution.py:422
  37.2 10.3 %copy-start.14 = (bf16[128,192]{0,1:T(8,128)(2,1)S(1)}, bf16[128,192]{0,1:T(8,128)(2,1)}, u32[]{:S(2)}) copy-start(bf16[128,192]{0,1:T(8,128)(2,1)} %param.18) | copy-start | bytes 147460
  37.2 10.4 %copy-start.12 = (bf16[512,64]{0,1:T(8,128)(2,1)S(1)}, bf16[512,64]{0,1:T(8,128)(2,1)}, u32[]{:S(2)}) copy-start(bf16[512,64]{0,1:T(8,128)(2,1)} %param.24) | copy-start | bytes 196612
  37.3 10.6 %copy-start.13 = (bf16[512,64]{0,1:T(8,128)(2,1)S(1)}, bf16[512,64]{0,1:T(8,128)(2,1)}, u32[]{:S(2)}) copy-start(bf16[512,64]{0,1:T(8,128)(2,1)} %param.25) | copy-start | bytes 196612
  41.0 68.9 %collective-permute-start.5 = (bf16[6144,128]{1,0:T(8,128)(2,1)}, bf16[6144,128]{1,0:T(8,128)(2,1)}, u32[]{:S(2)}, u32[]{:S(2)}) collective-permute-start(bf16[6144,128]{1,0:T(8,128)(2,1)} %get-tuple-element.20), channel_id=1, source_target_pairs={{0,1},{1,2},{2,3},{3,0},{4,5},{5,6},{6,7},{7,4},{8,9},{9,10},{10,1... | collective-permute-start | bytes 4718600 | tf_op jit(solution)/shard_map/ppermute | solution.py:485
  44.3 65.6 %collective-permute-start.6 = (bf16[6144,128]{1,0:T(8,128)(2,1)}, bf16[6144,128]{1,0:T(8,128)(2,1)}, u32[]{:S(2)}, u32[]{:S(2)}) collective-permute-start(bf16[6144,128]{1,0:T(8,128)(2,1)} %get-tuple-element.21), channel_id=1, source_target_pairs={{0,3},{1,0},{2,1},{3,2},{4,7},{5,4},{6,5},{7,6},{8,11},{9,8},{10,9... | collective-permute-start | bytes 4718600 | tf_op jit(solution)/shard_map/ppermute | solution.py:486
  49.6 0.8 copy-start.1
  50.4 20.2 %copy-start.3 = (bf16[128,640]{1,0:T(8,128)(2,1)}, bf16[128,640]{1,0:T(8,128)(2,1)S(1)}, u32[]{:S(2)}) copy-start(bf16[128,640]{1,0:T(8,128)(2,1)S(1)} %get-tuple-element.16.refs_2_) | copy-start | bytes 491524
  50.4 20.2 %copy-start.4 = (bf16[128,320]{1,0:T(8,128)(2,1)}, bf16[128,320]{1,0:T(8,128)(2,1)S(1)}, u32[]{:S(2)}) copy-start(bf16[128,320]{1,0:T(8,128)(2,1)S(1)} %get-tuple-element.14.q_own_in) | copy-start | bytes 245764
  50.4 29.7 %copy-start = (bf16[128,2048]{1,0:T(8,128)(2,1)S(1)}, bf16[128,2048]{1,0:T(8,128)(2,1)}, u32[]{:S(2)}) copy-start(bf16[128,2048]{1,0:T(8,128)(2,1)} %out_maj.1) | copy-start | bytes 1572868
  50.4 29.7 %copy-start.2 = (bf16[64,2048]{1,0:T(8,128)(2,1)S(1)}, bf16[64,2048]{1,0:T(8,128)(2,1)}, u32[]{:S(2)}) copy-start(bf16[64,2048]{1,0:T(8,128)(2,1)} %out_min.1) | copy-start | bytes 786436
  50.4 13.1 %collective-permute-start = (bf16[128,320]{1,0:T(8,128)(2,1)S(1)}, bf16[128,320]{1,0:T(8,128)(2,1)S(1)}, u32[]{:S(2)}, u32[]{:S(2)}) collective-permute-start(bf16[128,320]{1,0:T(8,128)(2,1)S(1)} %get-tuple-element.14.q_own_in), channel_id=1, source_target_pairs={{0,16},{16,0},{32,48},{48,32},{64,80},{80,64},{96,112},{112,96},{1... | collective-permute-start | bytes 245768 | tf_op jit(solution)/shard_map/ppermute | solution.py:483
  57.6 8.1 %collective-permute-start.3 = (bf16[128,640]{1,0:T(8,128)(2,1)S(1)}, bf16[128,640]{1,0:T(8,128)(2,1)S(1)}, u32[]{:S(2)}, u32[]{:S(2)}) collective-permute-start(bf16[128,640]{1,0:T(8,128)(2,1)S(1)} %get-tuple-element.16.refs_2_), channel_id=1, source_target_pairs={{0,480},{16,496},{1,481},{17,497},{2,482},{18,498},{3,483},{19,499... | collective-permute-start | bytes 491528 | tf_op jit(solution)/shard_map/ppermute | solution.py:484
  62.2 4.8 %collective-permute-start.2 = (bf16[128,640]{1,0:T(8,128)(2,1)S(1)}, bf16[128,640]{1,0:T(8,128)(2,1)S(1)}, u32[]{:S(2)}, u32[]{:S(2)}) collective-permute-start(bf16[128,640]{1,0:T(8,128)(2,1)S(1)} %get-tuple-element.16.refs_2_), channel_id=1, source_target_pairs={{0,32},{16,48},{32,64},{48,80},{64,96},{80,112},{96,128},{112,144}... | collective-permute-start | bytes 491528 | tf_op jit(solution)/shard_map/ppermute | solution.py:484
  63.5 7.1 %copy-start.11 = (bf16[128,320]{1,0:T(8,128)(2,1)}, bf16[128,320]{1,0:T(8,128)(2,1)S(1)}, u32[]{:S(2)}) copy-start(bf16[128,320]{1,0:T(8,128)(2,1)S(1)} %collective-permute-done.q_other_in) | copy-start | bytes 245764
  63.5 7.0 %collective-permute-start.1 = (bf16[128,640]{1,0:T(8,128)(2,1)S(1)}, bf16[128,640]{1,0:T(8,128)(2,1)S(1)}, u32[]{:S(2)}, u32[]{:S(2)}) collective-permute-start(bf16[128,640]{1,0:T(8,128)(2,1)S(1)} %get-tuple-element.16.refs_2_), channel_id=1, source_target_pairs={{0,64},{16,80},{32,96},{48,112},{64,128},{80,144},{96,160},{112,17... | collective-permute-start | bytes 491528 | tf_op jit(solution)/shard_map/ppermute | solution.py:484
  65.7 4.9 %copy-start.8 = (bf16[128,640]{1,0:T(8,128)(2,1)}, bf16[128,640]{1,0:T(8,128)(2,1)S(1)}, u32[]{:S(2)}) copy-start(bf16[128,640]{1,0:T(8,128)(2,1)S(1)} %collective-permute-done.3.refs_3_) | copy-start | bytes 491524
  67.0 3.6 %copy-start.9 = (bf16[128,640]{1,0:T(8,128)(2,1)}, bf16[128,640]{1,0:T(8,128)(2,1)S(1)}, u32[]{:S(2)}) copy-start(bf16[128,640]{1,0:T(8,128)(2,1)S(1)} %collective-permute-done.2.refs_1_) | copy-start | bytes 491524
  70.5 0.7 copy-start.10
  76.1 11.0 %copy-start.15 = (s32[128,2]{0,1:T(2,128)S(1)}, s32[128,2]{0,1:T(2,128)}, u32[]{:S(2)}) copy-start(s32[128,2]{0,1:T(2,128)} %param.30) | copy-start | bytes 3076
  76.1 11.1 %copy-start.16 = (f32[128,2]{0,1:T(2,128)S(1)}, f32[128,2]{0,1:T(2,128)}, u32[]{:S(2)}) copy-start(f32[128,2]{0,1:T(2,128)} %param.31) | copy-start | bytes 3076
  76.1 21.7 %copy-start.5 = (bf16[128,128]{1,0:T(8,128)(2,1)S(1)}, bf16[128,128]{1,0:T(8,128)(2,1)}, u32[]{:S(2)}) copy-start(bf16[128,128]{1,0:T(8,128)(2,1)} %residual.1) | copy-start | bytes 98308
  76.1 3.9 %collective-permute-start.4 = (f32[128,256]{1,0:T(8,128)S(1)}, f32[128,256]{1,0:T(8,128)S(1)}, u32[]{:S(2)}, u32[]{:S(2)}) collective-permute-start(f32[128,256]{1,0:T(8,128)S(1)} %get-tuple-element.18), channel_id=1, source_target_pairs={{0,16},{16,0},{32,48},{48,32},{64,80},{80,64},{96,112},{112,96},{1... | collective-permute-start | bytes 393224 | tf_op jit(solution)/shard_map/ppermute | solution.py:502
  81.4 16.5 %all-to-all-start.2 = ((bf16[16,128,128]{2,1,0:T(8,128)(2,1)}), bf16[16,128,128]{2,1,0:T(8,128)(2,1)S(1)}, u32[]{:S(2)}, u32[]{:S(2)}) async-start(bf16[16,128,128]{2,1,0:T(8,128)(2,1)} %shard_map.176), calls=%async_computation.2 | async-start | bytes 1048576 | tf_op jit(solution)/shard_map/all_to_all | solution.py:422
  99.2 26.6 %all-to-all-start.3 = ((bf16[32,16,128]{2,1,0:T(8,128)(2,1)}), bf16[32,16,128]{2,1,0:T(8,128)(2,1)S(1)}, u32[]{:S(2)}, u32[]{:S(2)}) async-start(bf16[32,16,128]{2,1,0:T(8,128)(2,1)} %bitcast.1), calls=%async_computation.3 | async-start | bytes 262144 | tf_op jit(solution)/shard_map/all_to_all | solution.py:422
  109.9 0.6 copy-start.6
  125.8 18.3 %copy-start.7 = (f32[2048]{0:T(1024)S(1)}, f32[2048]{0:T(1024)}, u32[]{:S(2)}) copy-start(f32[2048]{0:T(1024)} %param.29) | copy-start | bytes 24580

commit v11 on v10

--- a/solution.py
+++ b/solution.py
@@ -190,8 +190,7 @@
             (up_in, up_weights),
             (q_own_in, q_all.at[pl.ds(0, TOK)]),
             (q_other_in, q_all.at[pl.ds(TOK, TOK)]),
-        )
-        + tuple((b, near.at[pl.ds(TOK * i, TOK)]) for i, b in enumerate(near_in)),
+        ),
         sems,
     )
     me = lax.axis_index("sp")
@@ -201,8 +200,12 @@
     scale_maj = (NOPE_MAJOR + ROPE) ** -0.5 * LOG2_E
     scale_min = (NOPE_MINOR + ROPE) ** -0.5 * LOG2_E
     tops = [jnp.full((2 * TOK, 128), MASKED, F32)] * 2
-    for c in copies[:3]:
-        c.wait()
+    for c in copies:
+        c.wait()
+    blocks = fetch(
+        [(b, near.at[pl.ds(TOK * i, TOK)]) for i, b in enumerate(near_in)],
+        sems.at[pl.ds(3, len(NEAR))],
+    )
     weights = up_weights[...]
     q_maj, q_min = q_all[:, :192], q_all[:, 192:320]
 
@@ -241,7 +244,7 @@
         k_z = (z + NEAR[-1] + 1 + inner // ROWS) % N_Z
         k_pos = (2 * k_z + core) * TOK + ROWS * (n * PER + col // FAR_ROWS) + inner % ROWS
         tops = scored(CHUNK * n, CHUNK, lat, rope, k_pos, tops)
-    for c in copies[3:]:
+    for c in blocks:
         c.wait()
     col = lax.broadcasted_iota(jnp.int32, (1, len(NEAR) * TOK), 1)
     k_pos = (2 * ((z + NEAR[0] + N_Z + col // TOK) % N_Z) + core) * TOK + col % TOK
@@ -348,8 +351,8 @@
         for i, packed in enumerate((low, high)):
             pairs.append((packed.at[pl.ds(at * D, D)], w.at[:, pl.ds(256 + 128 * i, 128)]))
     pairs.append((down_a.at[0], down_w.at[own]))
-    for i, packed in enumerate((low, high)):
-        for t in range(N_TP):
+    for t in range(N_TP):
+        for i, packed in enumerate((low, high)):
             mine, cols = pl.ds(256 + 128 * i, 128), pl.ds(128 * t, 128)
             pairs.append((packed.at[pl.ds(2 * D + 128 * t, 128)], down_w.at[mine, cols]))
     copies = fetch(pairs, sems)
@@ -367,9 +370,10 @@
         c.wait()
     up = dot(x[...], up_w[...]) * factor
     hidden = (gate / (1.0 + jnp.exp(-gate)) * up).astype(BF16)
-    for c in copies[6:]:
-        c.wait()
+    copies[6].wait()
     for t in range(0, N_TP, 2):
+        for c in copies[7 + 2 * t : 11 + 2 * t]:
+            c.wait()
         value = dot(hidden, down_w[:, 128 * t : 128 * (t + 2)])
         parts[t] = value[:, :128].astype(BF16)
         parts[t + 1] = value[:, 128:].astype(BF16)

time: 192 us -> 195 us (1.016)
  Pallas kernels: 19.9 us -> 22.4 us
    pallas_call x12, Pallas kernels: 19.9 us -> 22.4 us  [kernel(): pl.pallas_call(body, out_shape=outs, in_specs=[pl.BlockSpec(memory_space=...]
where the time goes in v11:
time: 195 us; the launch traced here: 194 us
  blocking collectives  87.9 us (45%)
  starting transfers between devices  47 us (24%)
  waiting for transfers between devices  32.4 us (17%)
  Pallas kernels  22.4 us (11%)
  local copies, waits for them, and re-layouts  4.06 us (2%)
    all_to_all x4, blocking collectives, to_each(): lax.all_to_all(array, axis, 0, 0, tiled=True, axis_index_groups=groups)  87.9 us
    all_to_all x3, waiting for transfers between devices, to_each(): lax.all_to_all(array, axis, 0, 0, tiled=True, axis_index_groups=groups)  25.7 us
    all_to_all x3, starting transfers between devices, to_each(): lax.all_to_all(array, axis, 0, 0, tiled=True, axis_index_groups=groups)  23.2 us
    pallas_call x12, Pallas kernels, kernel(): pl.pallas_call(body, out_shape=outs, in_specs=[pl.BlockSpec(memory_space=...  22.4 us
    ppermute x1, starting transfers between devices, per_device(): q_other = lax.ppermute(q_own, 'sp', OTHER_CORE)  7.23 us
    ppermute x3, starting transfers between devices, per_device(): lax.ppermute(own_block, 'sp', along_z(-step))  7.13 us
    ppermute x3, waiting for transfers between devices, per_device(): lax.ppermute(own_block, 'sp', along_z(-step))  5.74 us
  transfers between devices with their start and end apart: 10, of which 6 were waited for; matrix products, arithmetic and copies ran while one was open for 0% of the time, Pallas kernels for 7%

profile of v11, /device:TPU:1, one launch (start us, length us, event | category | flops | bytes accessed | tf_op | source)
XLA Modules:
  0.0 194.1 jit_solution(14116293855640943877)
XLA Ops:
  0.0 1.2 shard_map.172
  1.2 27.7 %all_to_all.35.got = bf16[16,8,640]{2,1,0:T(8,128)(2,1)S(1)} all-to-all(bf16[16,8,640]{2,1,0:T(8,128)(2,1)S(1)} %shard_map.172), channel_id=1, replica_groups={{0,32,64,96,128,160,192,224,256,288,320,352,384,416,448,480},{16,48,80,..., dimensions={0} | all-to-all | bytes 327680 | tf_op jit(solution)/shard_map/all_to_all | solution.py:426
  28.9 0.1 shard_map.173
  29.0 1.5 broadcast_in_dim.3
  30.5 6.8 %all-to-all-start.1 = ((bf16[16,432,128]{2,1,0:T(8,128)(2,1)}), bf16[16,432,128]{2,1,0:T(8,128)(2,1)S(1)}, u32[]{:S(2)}, u32[]{:S(2)}) async-start(bf16[16,432,128]{2,1,0:T(8,128)(2,1)} %broadcast_in_dim.3), calls=%async_computation.1 | async-start | bytes 3538944 | tf_op jit(solution)/shard_map/all_to_all | solution.py:426
  37.2 0.0 copy-start.14
  37.2 0.0 copy-start.12
  37.3 0.0 copy-start.13
  37.3 3.8 %shard_map.178 = (bf16[6144,128]{1,0:T(8,128)(2,1)}, bf16[6144,128]{1,0:T(8,128)(2,1)}) custom-call(bf16[1,2048,256]{2,1,0:T(8,128)(2,1)} %gate_a.1, bf16[1,2048,256]{2,1,0:T(8,128)(2,1)} %up_a.1, bf16[1,256,2048]{2,1,0:T(8,128)(2,1)} %down_a.1), custom_call_target="tpu_custom_call" | custom-call | tf_op jit(solution)/shard_map/pallas_call | solution.py:415
  41.0 3.3 %collective-permute-start.5 = (bf16[6144,128]{1,0:T(8,128)(2,1)}, bf16[6144,128]{1,0:T(8,128)(2,1)}, u32[]{:S(2)}, u32[]{:S(2)}) collective-permute-start(bf16[6144,128]{1,0:T(8,128)(2,1)} %get-tuple-element.20), channel_id=1, source_target_pairs={{0,1},{1,2},{2,3},{3,0},{4,5},{5,6},{6,7},{7,4},{8,9},{9,10},{10,1... | collective-permute-start | bytes 4718600 | tf_op jit(solution)/shard_map/ppermute | solution.py:489
  44.3 3.2 %collective-permute-start.6 = (bf16[6144,128]{1,0:T(8,128)(2,1)}, bf16[6144,128]{1,0:T(8,128)(2,1)}, u32[]{:S(2)}, u32[]{:S(2)}) collective-permute-start(bf16[6144,128]{1,0:T(8,128)(2,1)} %get-tuple-element.21), channel_id=1, source_target_pairs={{0,3},{1,0},{2,1},{3,2},{4,7},{5,4},{6,5},{7,6},{8,11},{9,8},{10,9... | collective-permute-start | bytes 4718600 | tf_op jit(solution)/shard_map/ppermute | solution.py:490
  47.6 0.1 copy.19.maj
  47.7 0.1 copy.20.ku_min
  47.8 0.1 copy.21.vu_min
  48.0 1.6 shard_map.174
  49.6 0.8 copy-done.1
  50.4 7.2 %collective-permute-start = (bf16[128,320]{1,0:T(8,128)(2,1)S(1)}, bf16[128,320]{1,0:T(8,128)(2,1)S(1)}, u32[]{:S(2)}, u32[]{:S(2)}) collective-permute-start(bf16[128,320]{1,0:T(8,128)(2,1)S(1)} %get-tuple-element.14.q_own_in), channel_id=1, source_target_pairs={{0,16},{16,0},{32,48},{48,32},{64,80},{80,64},{96,112},{112,96},{1... | collective-permute-start | bytes 245768 | tf_op jit(solution)/shard_map/ppermute | solution.py:487
  57.6 4.5 %collective-permute-start.3 = (bf16[128,640]{1,0:T(8,128)(2,1)S(1)}, bf16[128,640]{1,0:T(8,128)(2,1)S(1)}, u32[]{:S(2)}, u32[]{:S(2)}) collective-permute-start(bf16[128,640]{1,0:T(8,128)(2,1)S(1)} %get-tuple-element.16.refs_2_), channel_id=1, source_target_pairs={{0,480},{16,496},{1,481},{17,497},{2,482},{18,498},{3,483},{19,499... | collective-permute-start | bytes 491528 | tf_op jit(solution)/shard_map/ppermute | solution.py:488
  62.2 1.3 collective-permute-start.2
  63.5 1.3 collective-permute-start.1
  64.8 0.9 collective-permute-done.3.refs_3_
  65.7 1.3 collective-permute-done.2.refs_1_
  67.0 3.6 %collective-permute-done.1.refs_0_ = bf16[128,640]{1,0:T(8,128)(2,1)S(1)} collective-permute-done((bf16[128,640]{1,0:T(8,128)(2,1)S(1)}, bf16[128,640]{1,0:T(8,128)(2,1)S(1)}, u32[]{:S(2)}, u32[]{:S(2)}) %collective-permute-start.1) | collective-permute-done | bytes 163872 | tf_op jit(solution)/shard_map/ppermute | solution.py:488
  70.6 0.6 copy-done.10
  71.2 5.8 %shard_map.175 = (f32[128,256]{1,0:T(8,128)S(1)}, f32[128,256]{1,0:T(8,128)S(1)}) custom-call(bf16[16,432,128]{2,1,0:T(8,128)(2,1)S(1)} %all-to-all-done.1.keys, bf16[128,320]{1,0:T(8,128)(2,1)} %copy-done.4, bf16[128,320]{1,0:T(8,128)(2,1)} %copy-done.11, bf16[512,384]{1,0:T(8,128)(2,1)} %copy-done.1, bf16[128,640]{1,0:T(8,128)(2,1)} %copy-done.10, ...), custom_call_target="tpu_custom_call" | custom-call | tf_op jit(solution)/shard_map/pallas_call | solution.py:415
  77.0 0.0 copy-start.15
  77.0 0.0 copy-start.16
  77.0 0.0 copy-start.5
  77.0 2.9 %collective-permute-start.4 = (f32[128,256]{1,0:T(8,128)S(1)}, f32[128,256]{1,0:T(8,128)S(1)}, u32[]{:S(2)}, u32[]{:S(2)}) collective-permute-start(f32[128,256]{1,0:T(8,128)S(1)} %get-tuple-element.18), channel_id=1, source_target_pairs={{0,16},{16,0},{32,48},{48,32},{64,80},{80,64},{96,112},{112,96},{1... | collective-permute-start | bytes 393224 | tf_op jit(solution)/shard_map/ppermute | solution.py:506
  79.9 1.0 collective-permute-done.4.b
  80.9 1.4 shard_map.176
  82.3 5.7 %all-to-all-start.2 = ((bf16[16,128,128]{2,1,0:T(8,128)(2,1)}), bf16[16,128,128]{2,1,0:T(8,128)(2,1)S(1)}, u32[]{:S(2)}, u32[]{:S(2)}) async-start(bf16[16,128,128]{2,1,0:T(8,128)(2,1)} %shard_map.176), calls=%async_computation.2 | async-start | bytes 1048576 | tf_op jit(solution)/shard_map/all_to_all | solution.py:426
  88.0 0.1 copy.22.ids
  88.1 0.1 copy.23.weights
  88.2 10.5 %all-to-all-done.2.parts = bf16[16,128,128]{2,1,0:T(8,128)(2,1)S(1)} async-done(((bf16[16,128,128]{2,1,0:T(8,128)(2,1)}), bf16[16,128,128]{2,1,0:T(8,128)(2,1)S(1)}, u32[]{:S(2)}, u32[]{:S(2)}) %all-to-all-start.2) | async-done | bytes 524320 | tf_op jit(solution)/shard_map/all_to_all | solution.py:426
  98.7 1.3 shard_map.177
  100.1 10.7 %all-to-all-start.3 = ((bf16[32,16,128]{2,1,0:T(8,128)(2,1)}), bf16[32,16,128]{2,1,0:T(8,128)(2,1)S(1)}, u32[]{:S(2)}, u32[]{:S(2)}) async-start(bf16[32,16,128]{2,1,0:T(8,128)(2,1)} %bitcast.1), calls=%async_computation.3 | async-start | bytes 262144 | tf_op jit(solution)/shard_map/all_to_all | solution.py:426
  110.8 0.0 collective-permute-done.5.low
  110.8 0.0 copy-start.6
  110.8 0.6 copy-done.6
  111.4 15.2 %all-to-all-done.3 = bf16[32,16,128]{2,1,0:T(8,128)(2,1)S(1)} async-done(((bf16[32,16,128]{2,1,0:T(8,128)(2,1)}), bf16[32,16,128]{2,1,0:T(8,128)(2,1)S(1)}, u32[]{:S(2)}, u32[]{:S(2)}) %all-to-all-start.3) | async-done | bytes 131104 | tf_op jit(solution)/shard_map/all_to_all | solution.py:426
  126.6 0.1 shard_map.180
  126.8 18.2 %all_to_all.36.got = bf16[16,256,128]{2,1,0:T(8,128)(2,1)S(1)} all-to-all(bf16[16,256,128]{2,1,0:T(8,128)(2,1)S(1)} %shard_map.180), channel_id=1, replica_groups=mesh['sp'=32,'tp'=16] {'tp'}, dimensions={0} | all-to-all | bytes 2097152 | tf_op jit(solution)/shard_map/all_to_all | solution.py:426
  145.0 5.7 %shard_map.181 = bf16[16,256,128]{2,1,0:T(8,128)(2,1)S(1)} custom-call(bf16[16,256,128]{2,1,0:T(8,128)(2,1)S(1)} %all_to_all.36.got, f32[1,2048]{1,0:T(1,128)S(1)} %bitcast.9, bf16[1,2048,256]{2,1,0:T(8,128)(2,1)} %gate_a.1, bf16[1,2048,256]{2,1,0:T(8,128)(2,1)} %up_a.1, bf16[1,256,2048]{2,1,0:T(8,128)(2,1)} %down_a.1, ...), custom_call_target="tpu_custom_call" | custom-call | tf_op jit(solution)/shard_map/pallas_call | solution.py:415
  150.6 16.8 %all_to_all.37.parts = bf16[16,256,128]{2,1,0:T(8,128)(2,1)S(1)} all-to-all(bf16[16,256,128]{2,1,0:T(8,128)(2,1)S(1)} %shard_map.181), channel_id=1, replica_groups=mesh['sp'=32,'tp'=16] {'tp'}, dimensions={0} | all-to-all | bytes 2097152 | tf_op jit(solution)/shard_map/all_to_all | solution.py:426
  167.4 0.1 shard_map.182
  167.6 25.2 %all_to_all.38 = bf16[32,16,128]{2,1,0:T(8,128)(2,1)S(1)} all-to-all(bf16[32,16,128]{2,1,0:T(8,128)(2,1)S(1)} %bitcast.7), channel_id=1, replica_groups=mesh['sp'=32,'tp'=16] {'sp'}, dimensions={0} | all-to-all | bytes 262144 | tf_op jit(solution)/shard_map/all_to_all | solution.py:426
  192.8 1.2 shard_map.183
  (28 shorter events, 0.1 us)
Async XLA Ops:
  30.5 40.1 %all-to-all-start.1 = ((bf16[16,432,128]{2,1,0:T(8,128)(2,1)}), bf16[16,432,128]{2,1,0:T(8,128)(2,1)S(1)}, u32[]{:S(2)}, u32[]{:S(2)}) async-start(bf16[16,432,128]{2,1,0:T(8,128)(2,1)} %broadcast_in_dim.3), calls=%async_computation.1 | async-start | bytes 3538944 | tf_op jit(solution)/shard_map/all_to_all | solution.py:426
  37.2 10.3 %copy-start.14 = (bf16[128,192]{0,1:T(8,128)(2,1)S(1)}, bf16[128,192]{0,1:T(8,128)(2,1)}, u32[]{:S(2)}) copy-start(bf16[128,192]{0,1:T(8,128)(2,1)} %param.18) | copy-start | bytes 147460
  37.2 10.4 %copy-start.12 = (bf16[512,64]{0,1:T(8,128)(2,1)S(1)}, bf16[512,64]{0,1:T(8,128)(2,1)}, u32[]{:S(2)}) copy-start(bf16[512,64]{0,1:T(8,128)(2,1)} %param.24) | copy-start | bytes 196612
  37.3 10.6 %copy-start.13 = (bf16[512,64]{0,1:T(8,128)(2,1)S(1)}, bf16[512,64]{0,1:T(8,128)(2,1)}, u32[]{:S(2)}) copy-start(bf16[512,64]{0,1:T(8,128)(2,1)} %param.25) | copy-start | bytes 196612
  41.0 69.7 %collective-permute-start.5 = (bf16[6144,128]{1,0:T(8,128)(2,1)}, bf16[6144,128]{1,0:T(8,128)(2,1)}, u32[]{:S(2)}, u32[]{:S(2)}) collective-permute-start(bf16[6144,128]{1,0:T(8,128)(2,1)} %get-tuple-element.20), channel_id=1, source_target_pairs={{0,1},{1,2},{2,3},{3,0},{4,5},{5,6},{6,7},{7,4},{8,9},{9,10},{10,1... | collective-permute-start | bytes 4718600 | tf_op jit(solution)/shard_map/ppermute | solution.py:489
  44.3 66.5 %collective-permute-start.6 = (bf16[6144,128]{1,0:T(8,128)(2,1)}, bf16[6144,128]{1,0:T(8,128)(2,1)}, u32[]{:S(2)}, u32[]{:S(2)}) collective-permute-start(bf16[6144,128]{1,0:T(8,128)(2,1)} %get-tuple-element.21), channel_id=1, source_target_pairs={{0,3},{1,0},{2,1},{3,2},{4,7},{5,4},{6,5},{7,6},{8,11},{9,8},{10,9... | collective-permute-start | bytes 4718600 | tf_op jit(solution)/shard_map/ppermute | solution.py:490
  49.6 0.8 copy-start.1
  50.4 20.2 %copy-start.3 = (bf16[128,640]{1,0:T(8,128)(2,1)}, bf16[128,640]{1,0:T(8,128)(2,1)S(1)}, u32[]{:S(2)}) copy-start(bf16[128,640]{1,0:T(8,128)(2,1)S(1)} %get-tuple-element.16.refs_2_) | copy-start | bytes 491524
  50.4 20.2 %copy-start.4 = (bf16[128,320]{1,0:T(8,128)(2,1)}, bf16[128,320]{1,0:T(8,128)(2,1)S(1)}, u32[]{:S(2)}) copy-start(bf16[128,320]{1,0:T(8,128)(2,1)S(1)} %get-tuple-element.14.q_own_in) | copy-start | bytes 245764
  50.4 30.5 %copy-start = (bf16[128,2048]{1,0:T(8,128)(2,1)S(1)}, bf16[128,2048]{1,0:T(8,128)(2,1)}, u32[]{:S(2)}) copy-start(bf16[128,2048]{1,0:T(8,128)(2,1)} %out_maj.1) | copy-start | bytes 1572868
  50.4 30.5 %copy-start.2 = (bf16[64,2048]{1,0:T(8,128)(2,1)S(1)}, bf16[64,2048]{1,0:T(8,128)(2,1)}, u32[]{:S(2)}) copy-start(bf16[64,2048]{1,0:T(8,128)(2,1)} %out_min.1) | copy-start | bytes 786436
  50.4 13.1 %collective-permute-start = (bf16[128,320]{1,0:T(8,128)(2,1)S(1)}, bf16[128,320]{1,0:T(8,128)(2,1)S(1)}, u32[]{:S(2)}, u32[]{:S(2)}) collective-permute-start(bf16[128,320]{1,0:T(8,128)(2,1)S(1)} %get-tuple-element.14.q_own_in), channel_id=1, source_target_pairs={{0,16},{16,0},{32,48},{48,32},{64,80},{80,64},{96,112},{112,96},{1... | collective-permute-start | bytes 245768 | tf_op jit(solution)/shard_map/ppermute | solution.py:487
  57.6 8.1 %collective-permute-start.3 = (bf16[128,640]{1,0:T(8,128)(2,1)S(1)}, bf16[128,640]{1,0:T(8,128)(2,1)S(1)}, u32[]{:S(2)}, u32[]{:S(2)}) collective-permute-start(bf16[128,640]{1,0:T(8,128)(2,1)S(1)} %get-tuple-element.16.refs_2_), channel_id=1, source_target_pairs={{0,480},{16,496},{1,481},{17,497},{2,482},{18,498},{3,483},{19,499... | collective-permute-start | bytes 491528 | tf_op jit(solution)/shard_map/ppermute | solution.py:488
  62.2 4.8 %collective-permute-start.2 = (bf16[128,640]{1,0:T(8,128)(2,1)S(1)}, bf16[128,640]{1,0:T(8,128)(2,1)S(1)}, u32[]{:S(2)}, u32[]{:S(2)}) collective-permute-start(bf16[128,640]{1,0:T(8,128)(2,1)S(1)} %get-tuple-element.16.refs_2_), channel_id=1, source_target_pairs={{0,32},{16,48},{32,64},{48,80},{64,96},{80,112},{96,128},{112,144}... | collective-permute-start | bytes 491528 | tf_op jit(solution)/shard_map/ppermute | solution.py:488
  63.5 7.1 %copy-start.11 = (bf16[128,320]{1,0:T(8,128)(2,1)}, bf16[128,320]{1,0:T(8,128)(2,1)S(1)}, u32[]{:S(2)}) copy-start(bf16[128,320]{1,0:T(8,128)(2,1)S(1)} %collective-permute-done.q_other_in) | copy-start | bytes 245764
  63.5 7.0 %collective-permute-start.1 = (bf16[128,640]{1,0:T(8,128)(2,1)S(1)}, bf16[128,640]{1,0:T(8,128)(2,1)S(1)}, u32[]{:S(2)}, u32[]{:S(2)}) collective-permute-start(bf16[128,640]{1,0:T(8,128)(2,1)S(1)} %get-tuple-element.16.refs_2_), channel_id=1, source_target_pairs={{0,64},{16,80},{32,96},{48,112},{64,128},{80,144},{96,160},{112,17... | collective-permute-start | bytes 491528 | tf_op jit(solution)/shard_map/ppermute | solution.py:488
  65.7 4.9 %copy-start.8 = (bf16[128,640]{1,0:T(8,128)(2,1)}, bf16[128,640]{1,0:T(8,128)(2,1)S(1)}, u32[]{:S(2)}) copy-start(bf16[128,640]{1,0:T(8,128)(2,1)S(1)} %collective-permute-done.3.refs_3_) | copy-start | bytes 491524
  67.0 3.6 %copy-start.9 = (bf16[128,640]{1,0:T(8,128)(2,1)}, bf16[128,640]{1,0:T(8,128)(2,1)S(1)}, u32[]{:S(2)}) copy-start(bf16[128,640]{1,0:T(8,128)(2,1)S(1)} %collective-permute-done.2.refs_1_) | copy-start | bytes 491524
  70.5 0.7 copy-start.10
  77.0 11.0 %copy-start.15 = (s32[128,2]{0,1:T(2,128)S(1)}, s32[128,2]{0,1:T(2,128)}, u32[]{:S(2)}) copy-start(s32[128,2]{0,1:T(2,128)} %param.30) | copy-start | bytes 3076
  77.0 11.1 %copy-start.16 = (f32[128,2]{0,1:T(2,128)S(1)}, f32[128,2]{0,1:T(2,128)}, u32[]{:S(2)}) copy-start(f32[128,2]{0,1:T(2,128)} %param.31) | copy-start | bytes 3076
  77.0 21.7 %copy-start.5 = (bf16[128,128]{1,0:T(8,128)(2,1)S(1)}, bf16[128,128]{1,0:T(8,128)(2,1)}, u32[]{:S(2)}) copy-start(bf16[128,128]{1,0:T(8,128)(2,1)} %residual.1) | copy-start | bytes 98308
  77.0 3.9 %collective-permute-start.4 = (f32[128,256]{1,0:T(8,128)S(1)}, f32[128,256]{1,0:T(8,128)S(1)}, u32[]{:S(2)}, u32[]{:S(2)}) collective-permute-start(f32[128,256]{1,0:T(8,128)S(1)} %get-tuple-element.18), channel_id=1, source_target_pairs={{0,16},{16,0},{32,48},{48,32},{64,80},{80,64},{96,112},{112,96},{1... | collective-permute-start | bytes 393224 | tf_op jit(solution)/shard_map/ppermute | solution.py:506
  82.3 16.5 %all-to-all-start.2 = ((bf16[16,128,128]{2,1,0:T(8,128)(2,1)}), bf16[16,128,128]{2,1,0:T(8,128)(2,1)S(1)}, u32[]{:S(2)}, u32[]{:S(2)}) async-start(bf16[16,128,128]{2,1,0:T(8,128)(2,1)} %shard_map.176), calls=%async_computation.2 | async-start | bytes 1048576 | tf_op jit(solution)/shard_map/all_to_all | solution.py:426
  100.1 26.6 %all-to-all-start.3 = ((bf16[32,16,128]{2,1,0:T(8,128)(2,1)}), bf16[32,16,128]{2,1,0:T(8,128)(2,1)S(1)}, u32[]{:S(2)}, u32[]{:S(2)}) async-start(bf16[32,16,128]{2,1,0:T(8,128)(2,1)} %bitcast.1), calls=%async_computation.3 | async-start | bytes 262144 | tf_op jit(solution)/shard_map/all_to_all | solution.py:426
  110.8 0.6 copy-start.6
  126.6 18.3 %copy-start.7 = (f32[2048]{0:T(1024)S(1)}, f32[2048]{0:T(1024)}, u32[]{:S(2)}) copy-start(f32[2048]{0:T(1024)} %param.29) | copy-start | bytes 24580
